TPU v7x, 256 devices: a 8x8x2 block of a 8x8x16 slice. The times are simulated.
256 devices in a mesh: grp: 2 (over z), sp: 16 (over y, core), tp: 8 (over x).
Axes of the slice: x: 8, y: 8, z: 2, core: 2. Of those that a mesh axis runs over, the one named last changes fastest.
The devices are a block of a 8x8x16 slice.
Arguments:
- layer_input: bfloat16 [32, 4096, 2048], P(('grp', 'tp'), 'sp'), parts along dimension 0, may hold values from -6 to 6
- norm_gain: bfloat16 [2048], replicated, may hold values from 0.099609375 to 1.8984375
- key_weight: bfloat16 [2048, 1024], replicated, may hold values from -0.125 to 0.125
- value_weight: bfloat16 [2048, 1024], replicated, may hold values from -0.125 to 0.125
- input_gate_weight: bfloat16 [2048, 8], replicated, may hold values from -0.125 to 0.125
- forget_gate_weight: bfloat16 [2048, 8], replicated, may hold values from -0.125 to 0.125
- conv_weight: float32 [4, 1024], replicated, may hold values from -3 to 3
- input_shift: float32 [32, 8, 4096], P(('grp', 'sp'), 'tp'), parts along dimension 0, may hold values from -4 to 302
- forget_shift: float32 [32, 8, 4096], P(('grp', 'sp'), 'tp'), parts along dimension 0, may hold values from 0 to 10.1
- new_query: bfloat16 [32, 8, 128], P(('grp', 'sp'), 'tp'), parts along dimension 0, may hold values from 0.1 to 2
- new_key: bfloat16 [32, 8, 128], P(('grp', 'sp'), 'tp'), parts along dimension 0, may hold values from -6 to 6
- new_value: bfloat16 [32, 8, 128], P(('grp', 'sp'), 'tp'), parts along dimension 0, may hold values from -6 to 6
- new_input: float32 [32, 8], P(('grp', 'sp'), 'tp'), parts along dimension 0, may hold values from 2 to 6
- new_forget: float32 [32, 8], P(('grp', 'sp'), 'tp'), parts along dimension 0, may hold values from -1 to 3
Outputs:
- key_cache: bfloat16 [32, 8, 4096, 128], P(('grp', 'sp'), 'tp'), parts along dimension 0
- value_cache: bfloat16 [32, 8, 4096, 128], P(('grp', 'sp'), 'tp'), parts along dimension 0
- weight_cache: float32 [32, 8, 4096], P(('grp', 'sp'), 'tp'), parts along dimension 0
- first_read: bfloat16 [32, 8, 128], P(('grp', 'sp'), 'tp'), parts along dimension 0
There are 2 independent parts, one for each index of `grp`. A program takes and returns all parts, laid end to end along the dimension named above; an argument that names none is the same for every part. Nothing has to cross between parts.
All inputs are finite; a program needn't handle non-finite values.
Results may differ from a plain program's by a relative error of at most 0.012.
Values may be sent and summed in bfloat16 or wider, within the bound.
No kernel may reach another device: no remote copies, remote signals or barrier semaphores. Data moves between devices by JAX's collectives and lax.ppermute only.
A program may use at most 64 MiB of HBM per device.

v0:
```python
import math

import jax
import jax.numpy as jnp
from jax import lax
from jax.sharding import PartitionSpec as P

HEADS = 8
DK = 128
CONV = 4


epsilon = 1e-06


def shifted(block, axis, distance):
    devices = range(lax.axis_size(axis))
    route = [(i - distance, i) for i in devices if i - distance in devices]
    return lax.ppermute(block, axis, route)


def side_by_side(arrays, axis, split_dim, concat_dim, along):
    widths = [math.prod(a.shape[along:]) for a in arrays]
    both = jnp.concatenate(
        [a.reshape(*a.shape[:along], w) for a, w in zip(arrays, widths)], axis=along
    )
    whole = lax.all_to_all(both, axis, split_axis=split_dim, concat_axis=concat_dim, tiled=True)
    blocks = jnp.split(whole, [sum(widths[:k]) for k in range(1, len(widths))], axis=along)
    return tuple(
        (b.reshape(*whole.shape[:along], *a.shape[along:]) for a, b in zip(arrays, blocks))
    )


def project_rows(
    token_rows, norm_gain, key_weight, value_weight, input_gate_weight, forget_gate_weight
):
    widened = token_rows.astype(jnp.float32)
    normed = (
        widened
        * lax.rsqrt(jnp.mean(widened * widened, axis=-1, keepdims=True) + epsilon)
        * norm_gain.astype(jnp.float32)
    ).astype(jnp.bfloat16)
    key_matrix = key_weight.reshape(key_weight.shape[0], HEADS, DK)
    value_matrix = value_weight.reshape(value_weight.shape[0], HEADS, DK)
    key_linear = jnp.einsum(
        "apd,dhk->ahpk", normed, key_matrix, preferred_element_type=jnp.float32
    ).astype(jnp.bfloat16)
    values = jnp.einsum(
        "apd,dhk->ahpk", normed, value_matrix, preferred_element_type=jnp.float32
    ).astype(jnp.bfloat16)
    input_linear = jnp.einsum(
        "apd,dh->ahp", normed, input_gate_weight, preferred_element_type=jnp.float32
    ).astype(jnp.bfloat16)
    forget_linear = jnp.einsum(
        "apd,dh->ahp", normed, forget_gate_weight, preferred_element_type=jnp.float32
    ).astype(jnp.bfloat16)
    return (key_linear, values, input_linear, forget_linear)


def convolve(key_linear, previous, conv_weight):
    extended = jnp.concatenate([previous, key_linear], axis=2).astype(jnp.float32)
    length = key_linear.shape[2]
    tap_weight = conv_weight.reshape(CONV, HEADS, 1, DK)
    summed = extended[:, :, 0:length, :] * tap_weight[0]
    for offset in range(1, CONV):
        summed = summed + extended[:, :, offset : offset + length, :] * tap_weight[offset]
    return jax.nn.silu(summed).astype(jnp.bfloat16)


def read_cache(
    keys,
    values,
    input_linear,
    forget_linear,
    input_shift,
    forget_shift,
    new_query,
    new_key,
    new_value,
    new_input,
    new_forget,
):
    scaling = DK ** (-0.5)
    log_forget = jax.nn.log_sigmoid(forget_linear.astype(jnp.float32) + forget_shift)
    suffix = lax.cumsum(log_forget, axis=2, reverse=True) - log_forget
    new_decay = jax.nn.log_sigmoid(new_forget)
    log_weight = input_linear.astype(jnp.float32) + input_shift + suffix + new_decay[:, :, None]
    largest = jnp.maximum(jnp.max(log_weight, axis=2), new_input)
    weight_cache = jnp.exp(log_weight - largest[:, :, None])
    new_weight = jnp.exp(new_input - largest)
    matched = jnp.einsum("bhlk,bhk->bhl", keys, new_query, preferred_element_type=jnp.float32)
    scores = (weight_cache * matched * scaling).astype(jnp.bfloat16)
    fresh_match = jnp.sum(new_key.astype(jnp.float32) * new_query.astype(jnp.float32), axis=2)
    new_score = (new_weight * fresh_match * scaling).astype(jnp.bfloat16)
    denominator = jnp.sum(scores.astype(jnp.float32), axis=2) + new_score.astype(jnp.float32)
    numerator = jnp.einsum("bhl,bhlk->bhk", scores, values, preferred_element_type=jnp.float32)
    numerator = numerator + new_score.astype(jnp.float32)[:, :, None] * new_value.astype(
        jnp.float32
    )
    first_read = (numerator / jnp.maximum(jnp.abs(denominator), 1.0)[:, :, None]).astype(
        jnp.bfloat16
    )
    return (weight_cache, first_read)


def shards(
    layer_input,
    norm_gain,
    key_weight,
    value_weight,
    input_gate_weight,
    forget_gate_weight,
    conv_weight,
    input_shift,
    forget_shift,
    new_query,
    new_key,
    new_value,
    new_input,
    new_forget,
):
    token_rows = lax.all_to_all(layer_input, "tp", split_axis=1, concat_axis=0, tiled=True)
    key_linear, values, input_linear, forget_linear = project_rows(
        token_rows, norm_gain, key_weight, value_weight, input_gate_weight, forget_gate_weight
    )
    previous = shifted(key_linear[:, :, -(CONV - 1) :, :], ("sp", "tp"), 1)
    keys = convolve(key_linear, previous, conv_weight)
    groups = lax.axis_size("tp")
    seq_count = keys.shape[0]
    per_group = HEADS // groups

    def regroup(source):
        return source.reshape((seq_count * groups, per_group) + source.shape[2:])

    keys, values, input_linear, forget_linear = side_by_side(
        (regroup(keys), regroup(values), regroup(input_linear), regroup(forget_linear)),
        ("sp", "tp"),
        0,
        2,
        3,
    )
    weight_cache, first_read = read_cache(
        keys,
        values,
        input_linear,
        forget_linear,
        input_shift,
        forget_shift,
        new_query,
        new_key,
        new_value,
        new_input,
        new_forget,
    )
    return (keys, values, weight_cache, first_read)


def solution(mesh):
    in_specs = (
        P(("grp", "tp"), "sp", None),
        P(),
        P(),
        P(),
        P(),
        P(),
        P(),
        P(("grp", "sp"), "tp", None),
        P(("grp", "sp"), "tp", None),
        P(("grp", "sp"), "tp", None),
        P(("grp", "sp"), "tp", None),
        P(("grp", "sp"), "tp", None),
        P(("grp", "sp"), "tp"),
        P(("grp", "sp"), "tp"),
    )
    out_specs = (
        P(("grp", "sp"), "tp", None, None),
        P(("grp", "sp"), "tp", None, None),
        P(("grp", "sp"), "tp", None),
        P(("grp", "sp"), "tp", None),
    )
    return jax.shard_map(shards, mesh=mesh, in_specs=in_specs, out_specs=out_specs, check_vma=False)
```

profile of v0, /device:TPU:513, one launch (start us, length us, event | category | flops | bytes accessed | tf_op | source)
XLA Modules:
  0.0 194.7 jit_solution(17202118483127337060)
XLA Ops:
  0.6 5.1 %copy.61 = bf16[2,256,2048]{2,0,1:T(2,128)(2,1)} copy(bf16[2,256,2048]{2,1,0:T(8,128)(2,1)} %param.14) | data formatting | bytes 4194304 | tf_op args[0]
  5.8 8.0 %all-to-all-start = ((bf16[2,256,2048]{2,0,1:T(2,128)(2,1)}), bf16[2,256,2048]{2,0,1:T(2,128)(2,1)S(1)}, u32[]{:S(2)}, u32[]{:S(2)}) async-start(bf16[2,256,2048]{2,0,1:T(2,128)(2,1)} %copy.61), calls=%async_computation | async-start | bytes 4194304 | tf_op jit(solution)/shard_map/all_to_all | solution.py:122
  13.8 37.6 %all-to-all-done = bf16[2,256,2048]{2,0,1:T(2,128)(2,1)S(1)} async-done(((bf16[2,256,2048]{2,0,1:T(2,128)(2,1)}), bf16[2,256,2048]{2,0,1:T(2,128)(2,1)S(1)}, u32[]{:S(2)}, u32[]{:S(2)}) %all-to-all-start) | async-done | bytes 2097184 | tf_op jit(solution)/shard_map/all_to_all | solution.py:122
  51.3 0.9 bitcast_convert_fusion
  52.7 1.3 fusion.11
  53.9 0.9 copy-done.10
  54.8 2.4 %fusion.17 = bf16[16,8,32,128]{3,2,1,0:T(8,128)(2,1)S(1)} fusion(bf16[16,32,2048,1]{2,1,3,0:T(8,128)(2,1)S(1)} %bitcast.148, bf16[2048,1024]{1,0:T(8,128)(2,1)S(1)} %copy-done.10), kind=kOutput, calls=%fused_computation.31 | convolution fusion | flops 2148007936 | bytes 7340032 | tf_op jit(solution)/shard_map/apd,dhk->ahpk/dot_general | solution.py:45
  57.3 2.1 %collective-permute-start = (bf16[16,8,3,128]{3,2,1,0:T(4,128)(2,1)S(1)}, bf16[16,8,3,128]{3,2,1,0:T(4,128)(2,1)S(1)}, u32[]{:S(2)}, u32[]{:S(2)}) collective-permute-start(bf16[16,8,3,128]{3,2,1,0:T(4,128)(2,1)S(1)} %slice.48), channel_id=1, source_target_pairs={{0,1},{1,2},{2,3},{3,4},{4,5},{5,6},{6,7},{7,8},{8,9},{9,10},{10,1... | collective-permute-start | bytes 294920 | tf_op jit(solution)/shard_map/ppermute | solution.py:19
  59.4 0.9 copy.62
  60.8 1.7 copy-done.11
  62.5 3.3 %fusion.16 = bf16[16,32,8,128]{3,1,2,0:T(8,128)(2,1)} fusion(bf16[16,32,2048,1]{2,1,3,0:T(8,128)(2,1)S(1)} %bitcast.149, bf16[2048,1024]{1,0:T(8,128)(2,1)S(1)} %copy-done.11), kind=kOutput, calls=%fused_computation.30 | convolution fusion | flops 2148007936 | bytes 7340032 | tf_op jit(solution)/shard_map/apd,dhk->ahpk/dot_general | solution.py:48
  66.2 1.5 fusion.18
  67.7 1.5 fusion.19
  69.2 0.9 copy.71
  70.9 3.4 %collective-permute-done = bf16[16,8,3,128]{3,2,1,0:T(4,128)(2,1)S(1)} collective-permute-done((bf16[16,8,3,128]{3,2,1,0:T(4,128)(2,1)S(1)}, bf16[16,8,3,128]{3,2,1,0:T(4,128)(2,1)S(1)}, u32[]{:S(2)}, u32[]{:S(2)}) %collective-permute-start) | collective-permute-done | bytes 98336 | tf_op jit(solution)/shard_map/ppermute | solution.py:19
  74.9 1.3 multiply_convert_fusion
  76.2 2.6 %pad_maximum_fusion = bf16[128,1,32,258]{3,2,1,0:T(8,128)(2,1)} fusion(bf16[128,1,32,1]{3,2,1,0:T(8,128)(2,1)S(1)} %copy.72, bf16[128,1,32,1]{3,2,1,0:T(8,128)(2,1)S(1)} %copy.71, bf16[128,1,32,128]{3,2,1,0:T(8,128)(2,1)S(1)} %bitcast.150, bf16[128,1,32,128]{3,2,1,0:T(8,128)(2,1)S(1)} %bitcast.147), kind=kLoop, calls=%fused_computation.18 | loop fusion | flops 8454144 | bytes 4227072 | tf_op jit(solution)/shard_map/concatenate | solution.py:24
  78.8 30.9 %all-to-all-start.1 = ((bf16[128,1,32,258]{3,2,1,0:T(8,128)(2,1)}), bf16[128,1,32,258]{3,2,1,0:T(8,128)(2,1)S(1)}, u32[]{:S(2)}, u32[]{:S(2)}) async-start(bf16[128,1,32,258]{3,2,1,0:T(8,128)(2,1)} %pad_maximum_fusion), calls=%async_computation.1 | async-start | bytes 6291456 | tf_op jit(solution)/shard_map/all_to_all | solution.py:27
  111.7 71.8 %all-to-all-done.1 = bf16[128,1,32,258]{3,2,1,0:T(8,128)(2,1)S(1)} async-done(((bf16[128,1,32,258]{3,2,1,0:T(8,128)(2,1)}), bf16[128,1,32,258]{3,2,1,0:T(8,128)(2,1)S(1)}, u32[]{:S(2)}, u32[]{:S(2)}) %all-to-all-start.1) | async-done | bytes 2113568 | tf_op jit(solution)/shard_map/all_to_all | solution.py:27
  183.5 1.0 convert_reduce_fusion.1
  184.6 1.5 fusion.33
  186.1 1.2 reduce-window.6
  189.8 2.2 %convert_reduce_fusion.2 = (f32[]{:T(128)}, bf16[1,1,4096]{2,1,0:T(2,128)(2,1)S(1)}) fusion(f32[1,1,4096]{2,1,0:T(1,128)S(1)} %subtract_exponential_fusion, bf16[1,1,128]{2,1,0:T(2,128)(2,1)S(1)} %copy-done.8, bf16[1,1,4096,128]{3,2,1,0:T(8,128)(2,1)} %get-tuple-element.9), kind=kOutput, calls=%fused_computation.49 | convolution fusion | flops 1069055 | bytes 1073412 | tf_op jit(solution)/shard_map/bhlk,bhk->bhl/dot_general | solution.py:91
  192.7 2.0 %fusion.22 = bf16[1,1,128]{2,1,0:T(2,128)(2,1)} fusion(bf16[1,1,4096,128]{3,2,1,0:T(8,128)(2,1)} %get-tuple-element.8, bf16[1,1,4096]{2,1,0:T(2,128)(2,1)S(1)} %get-tuple-element.15, bf16[1,1,128]{2,1,0:T(2,128)(2,1)S(1)} %copy-done.9, f32[]{:T(128)} %bitcast.46, f32[]{:T(128)} %bitcast.44), kind=kOutput, calls=%fused_computation.40 | convolution fusion | flops 1049216 | bytes 1057288 | tf_op jit(solution)/shard_map/bhl,bhlk->bhk/dot_general | solution.py:96
  (42 shorter events, 4.7 us)
Async XLA Ops:
  0.6 65.6 %copy-start = (bf16[2048,8]{0,1:T(8,128)(2,1)S(1)}, bf16[2048,8]{0,1:T(8,128)(2,1)}, u32[]{:S(2)}) copy-start(bf16[2048,8]{0,1:T(8,128)(2,1)} %param.18) | copy-start | bytes 98308
  5.8 8.0 %copy-start.7 = (bf16[2048]{0:T(1024)(128)(2,1)S(1)}, bf16[2048]{0:T(1024)(128)(2,1)}, u32[]{:S(2)}) copy-start(bf16[2048]{0:T(1024)(128)(2,1)} %param.15) | copy-start | bytes 12292
  5.8 8.0 %copy-start.6 = (f32[4,1024]{1,0:T(4,128)S(1)}, f32[4,1024]{1,0:T(4,128)}, u32[]{:S(2)}) copy-start(f32[4,1024]{1,0:T(4,128)} %param.20) | copy-start | bytes 49156
  5.8 45.6 %all-to-all-start = ((bf16[2,256,2048]{2,0,1:T(2,128)(2,1)}), bf16[2,256,2048]{2,0,1:T(2,128)(2,1)S(1)}, u32[]{:S(2)}, u32[]{:S(2)}) async-start(bf16[2,256,2048]{2,0,1:T(2,128)(2,1)} %copy.61), calls=%async_computation | async-start | bytes 4194304 | tf_op jit(solution)/shard_map/all_to_all | solution.py:122
  52.6 2.2 %copy-start.10 = (bf16[2048,1024]{1,0:T(8,128)(2,1)S(1)}, bf16[2048,1024]{1,0:T(8,128)(2,1)}, u32[]{:S(2)}) copy-start(bf16[2048,1024]{1,0:T(8,128)(2,1)} %param.16) | copy-start | bytes 12582916
  57.3 17.1 %collective-permute-start = (bf16[16,8,3,128]{3,2,1,0:T(4,128)(2,1)S(1)}, bf16[16,8,3,128]{3,2,1,0:T(4,128)(2,1)S(1)}, u32[]{:S(2)}, u32[]{:S(2)}) collective-permute-start(bf16[16,8,3,128]{3,2,1,0:T(4,128)(2,1)S(1)} %slice.48), channel_id=1, source_target_pairs={{0,1},{1,2},{2,3},{3,4},{4,5},{5,6},{6,7},{7,8},{8,9},{9,10},{10,1... | collective-permute-start | bytes 294920 | tf_op jit(solution)/shard_map/ppermute | solution.py:19
  60.3 2.2 %copy-start.11 = (bf16[2048,1024]{1,0:T(8,128)(2,1)S(1)}, bf16[2048,1024]{1,0:T(8,128)(2,1)}, u32[]{:S(2)}) copy-start(bf16[2048,1024]{1,0:T(8,128)(2,1)} %param.17) | copy-start | bytes 12582916
  65.8 1.9 copy-start.3
  74.9 1.3 copy-start.1
  78.8 32.3 %copy-start.8 = (bf16[1,1,128]{2,1,0:T(2,128)(2,1)S(1)}, bf16[1,1,128]{2,1,0:T(2,128)(2,1)}, u32[]{:S(2)}) copy-start(bf16[1,1,128]{2,1,0:T(2,128)(2,1)} %param.23) | copy-start | bytes 772
  78.8 32.3 %copy-start.12 = (bf16[1,1,128]{2,1,0:T(2,128)(2,1)S(1)}, bf16[1,1,128]{2,1,0:T(2,128)(2,1)}, u32[]{:S(2)}) copy-start(bf16[1,1,128]{2,1,0:T(2,128)(2,1)} %param.24) | copy-start | bytes 772
  78.8 104.7 %all-to-all-start.1 = ((bf16[128,1,32,258]{3,2,1,0:T(8,128)(2,1)}), bf16[128,1,32,258]{3,2,1,0:T(8,128)(2,1)S(1)}, u32[]{:S(2)}, u32[]{:S(2)}) async-start(bf16[128,1,32,258]{3,2,1,0:T(8,128)(2,1)} %pad_maximum_fusion), calls=%async_computation.1 | async-start | bytes 6291456 | tf_op jit(solution)/shard_map/all_to_all | solution.py:27
  184.5 1.5 copy-start.4
  184.5 3.3 %copy-start.5 = (f32[1,1,4096]{2,1,0:T(1,128)S(1)}, f32[1,1,4096]{2,1,0:T(1,128)}, u32[]{:S(2)}) copy-start(f32[1,1,4096]{2,1,0:T(1,128)} %param.21) | copy-start | bytes 49156
  184.6 8.1 %copy-start.9 = (bf16[1,1,128]{2,1,0:T(2,128)(2,1)S(1)}, bf16[1,1,128]{2,1,0:T(2,128)(2,1)}, u32[]{:S(2)}) copy-start(bf16[1,1,128]{2,1,0:T(2,128)(2,1)} %param.25) | copy-start | bytes 772
  189.8 4.9 %copy-start.2 = (f32[1,1,4096]{2,1,0:T(1,128)}, f32[1,1,4096]{2,1,0:T(1,128)S(1)}, u32[]{:S(2)}) copy-start(f32[1,1,4096]{2,1,0:T(1,128)S(1)} %subtract_exponential_fusion) | copy-start | bytes 49156
where the time goes:
time: 195 us
  waiting for transfers between devices  113 us (58%)
  starting transfers between devices  41 us (21%)
  matrix products  12.8 us (7%)
  local copies, waits for them, and re-layouts  12.7 us (7%)
  other arithmetic  11.2 us (6%)
  between operations  4.17 us (2%)
    all_to_all x1, waiting for transfers between devices, side_by_side(): lax.all_to_all(both, axis, split_axis=split_dim, concat_axis=concat_dim,...  71.8 us
    all_to_all x1, waiting for transfers between devices, shards(): lax.all_to_all(layer_input, 'tp', split_axis=1, concat_axis=0, tiled=True)  37.6 us
    all_to_all x1, starting transfers between devices, side_by_side(): lax.all_to_all(both, axis, split_axis=split_dim, concat_axis=concat_dim,...  30.9 us
    all_to_all x1, starting transfers between devices, shards(): lax.all_to_all(layer_input, 'tp', split_axis=1, concat_axis=0, tiled=True)  7.99 us
    unnamed x27, local copies, waits for them, and re-layouts  7.71 us
  transfers between devices with their start and end apart: 3, of which 3 were waited for; matrix products, arithmetic and copies ran while one was open for 5% of the time, Pallas kernels for 0%

commit v1 on v0

v1 whole, which is shorter than its diff:
```python
import jax
import jax.numpy as jnp
from jax import lax
from jax.sharding import PartitionSpec as P

HEADS = 8
DK = 128
CONV = 4


epsilon = 1e-06


def normalise(token_rows, norm_gain):
    widened = token_rows.astype(jnp.float32)
    return (
        widened
        * lax.rsqrt(jnp.mean(widened * widened, axis=-1, keepdims=True) + epsilon)
        * norm_gain.astype(jnp.float32)
    ).astype(jnp.bfloat16)


def project(normed, weight):
    matrix = weight.reshape(weight.shape[0], HEADS, DK)
    return jnp.einsum(
        "apd,dhk->hapk", normed, matrix, preferred_element_type=jnp.float32
    ).astype(jnp.bfloat16)


def gate(normed, weight):
    linear = jnp.einsum("apd,dh->hap", normed, weight, preferred_element_type=jnp.float32)
    return linear.astype(jnp.bfloat16)


def convolve(key_linear, tap_weight):
    length = key_linear.shape[0]
    extended = jnp.pad(key_linear.astype(jnp.float32), ((CONV - 1, 0), (0, 0)))
    summed = extended[0:length] * tap_weight[0]
    for offset in range(1, CONV):
        summed = summed + extended[offset : offset + length] * tap_weight[offset]
    return jax.nn.silu(summed).astype(jnp.bfloat16)


def read_cache(
    keys,
    values,
    input_linear,
    forget_linear,
    input_shift,
    forget_shift,
    new_query,
    new_key,
    new_value,
    new_input,
    new_forget,
):
    scaling = DK ** (-0.5)
    log_forget = jax.nn.log_sigmoid(forget_linear.astype(jnp.float32) + forget_shift)
    suffix = lax.cumsum(log_forget, axis=2, reverse=True) - log_forget
    new_decay = jax.nn.log_sigmoid(new_forget)
    log_weight = input_linear.astype(jnp.float32) + input_shift + suffix + new_decay[:, :, None]
    largest = jnp.maximum(jnp.max(log_weight, axis=2), new_input)
    weight_cache = jnp.exp(log_weight - largest[:, :, None])
    new_weight = jnp.exp(new_input - largest)
    matched = jnp.einsum("bhlk,bhk->bhl", keys, new_query, preferred_element_type=jnp.float32)
    scores = (weight_cache * matched * scaling).astype(jnp.bfloat16)
    fresh_match = jnp.sum(new_key.astype(jnp.float32) * new_query.astype(jnp.float32), axis=2)
    new_score = (new_weight * fresh_match * scaling).astype(jnp.bfloat16)
    denominator = jnp.sum(scores.astype(jnp.float32), axis=2) + new_score.astype(jnp.float32)
    numerator = jnp.einsum("bhl,bhlk->bhk", scores, values, preferred_element_type=jnp.float32)
    numerator = numerator + new_score.astype(jnp.float32)[:, :, None] * new_value.astype(
        jnp.float32
    )
    first_read = (numerator / jnp.maximum(jnp.abs(denominator), 1.0)[:, :, None]).astype(
        jnp.bfloat16
    )
    return (weight_cache, first_read)


def shards(
    layer_input,
    norm_gain,
    key_weight,
    value_weight,
    input_gate_weight,
    forget_gate_weight,
    conv_weight,
    input_shift,
    forget_shift,
    new_query,
    new_key,
    new_value,
    new_input,
    new_forget,
):
    seqs, rows, _ = layer_input.shape
    lines = rows // DK
    normed = normalise(layer_input, norm_gain)
    gates = jnp.stack(
        [gate(normed, input_gate_weight), gate(normed, forget_gate_weight)], axis=2
    ).reshape(HEADS, seqs, 2 * lines, DK)
    gates = jnp.pad(gates, ((0, 0), (0, 0), (0, 8 - 2 * lines), (0, 0)))
    block = jnp.concatenate(
        [project(normed, key_weight), project(normed, value_weight), gates], axis=2
    )
    by_head = lax.all_to_all(block, "tp", split_axis=0, concat_axis=0, tiled=True)
    by_head = by_head.reshape(-1, *block.shape[2:])
    mine = lax.all_to_all(by_head, "sp", split_axis=0, concat_axis=0, tiled=True)
    blocks = mine.shape[0]
    length = blocks * rows
    key_linear = mine[:, :rows].reshape(length, DK)
    values = mine[:, rows : 2 * rows].reshape(1, 1, length, DK)
    input_linear = mine[:, 2 * rows : 2 * rows + lines].reshape(1, 1, length)
    forget_linear = mine[:, 2 * rows + lines : 2 * rows + 2 * lines].reshape(1, 1, length)
    head = lax.axis_index("tp")
    tap_weight = lax.dynamic_slice(conv_weight, (0, head * DK), (CONV, DK))
    keys = convolve(key_linear, tap_weight).reshape(1, 1, length, DK)
    weight_cache, first_read = read_cache(
        keys,
        values,
        input_linear,
        forget_linear,
        input_shift,
        forget_shift,
        new_query,
        new_key,
        new_value,
        new_input,
        new_forget,
    )
    return (keys, values, weight_cache, first_read)


def solution(mesh):
    in_specs = (
        P(("grp", "tp"), "sp", None),
        P(),
        P(),
        P(),
        P(),
        P(),
        P(),
        P(("grp", "sp"), "tp", None),
        P(("grp", "sp"), "tp", None),
        P(("grp", "sp"), "tp", None),
        P(("grp", "sp"), "tp", None),
        P(("grp", "sp"), "tp", None),
        P(("grp", "sp"), "tp"),
        P(("grp", "sp"), "tp"),
    )
    out_specs = (
        P(("grp", "sp"), "tp", None, None),
        P(("grp", "sp"), "tp", None, None),
        P(("grp", "sp"), "tp", None),
        P(("grp", "sp"), "tp", None),
    )
    return jax.shard_map(shards, mesh=mesh, in_specs=in_specs, out_specs=out_specs, check_vma=False)
```

time: 195 us -> 147 us (0.75)
  waiting for transfers between devices: 113 us -> 47 us
  blocking collectives: 0 us -> 43 us
  local copies, waits for them, and re-layouts: 12.7 us -> 1.91 us
  starting transfers between devices: 41 us -> 30.9 us
  other arithmetic: 11.2 us -> 8.45 us
    all_to_all x2 -> x1, waiting for transfers between devices: 109 us -> 47 us  [shards(): lax.all_to_all(by_head, 'sp', split_axis=0, concat_axis=0, tiled=True)]
    all_to_all x0 -> x1, blocking collectives: none -> 43 us  [shards(): lax.all_to_all(block, 'tp', split_axis=0, concat_axis=0, tiled=True)]
    all_to_all x2 -> x1, starting transfers between devices: 38.9 us -> 30.9 us  [shards(): lax.all_to_all(by_head, 'sp', split_axis=0, concat_axis=0, tiled=True)]
    unnamed x27 -> x22, local copies, waits for them, and re-layouts: 7.71 us -> 0.51 us
    ppermute x1 -> x0, waiting for transfers between devices: 3.43 us -> none  [shifted(): return lax.ppermute(block, axis, route)]
    convert_element_type x6 -> x2, other arithmetic: 4.43 us -> 1.04 us  [the longest x1 0.84 us: normalise(): norm_gain.astype(jnp.float32)]
    concatenate x1, other arithmetic: 2.62 us -> 0.18 us  [shards(): jnp.concatenate([project(normed, key_weight), project(normed, value_weigh...]
    reshape x0 -> x1, other arithmetic: none -> 2.27 us  [shards(): keys = convolve(key_linear, tap_weight).reshape(1, 1, length, DK)]
  transfers between devices with their start and end apart: 3 -> 1, of which waited for: 3 -> 1; matrix products, arithmetic and copies ran while one was open for 5% -> 1% of each run, Pallas kernels for 0% -> 0%
where the time goes in v1:
time: 147 us
  waiting for transfers between devices  47 us (32%)
  blocking collectives  43 us (29%)
  starting transfers between devices  30.9 us (21%)
  matrix products  11.3 us (8%)
  other arithmetic  8.45 us (6%)
  between operations  4.2 us (3%)
  local copies, waits for them, and re-layouts  1.91 us (1%)
    all_to_all x1, waiting for transfers between devices, shards(): lax.all_to_all(by_head, 'sp', split_axis=0, concat_axis=0, tiled=True)  47 us
    all_to_all x1, blocking collectives, shards(): lax.all_to_all(block, 'tp', split_axis=0, concat_axis=0, tiled=True)  43 us
    all_to_all x1, starting transfers between devices, shards(): lax.all_to_all(by_head, 'sp', split_axis=0, concat_axis=0, tiled=True)  30.9 us
    dot_general x2, matrix products, project(): jnp.einsum('apd,dhk->hapk', normed, matrix, preferred_element_type=jnp.fl...  7.09 us
  transfers between devices with their start and end apart: 1, of which 1 were waited for; matrix products, arithmetic and copies ran while one was open for 1% of the time, Pallas kernels for 0%

profile of v1, /device:TPU:513, one launch (start us, length us, event | category | flops | bytes accessed | tf_op | source)
XLA Modules:
  0.0 146.8 jit_solution(9058349963306154619)
XLA Ops:
  0.7 0.8 convert_element_type.100
  1.5 2.1 %fusion.4 = f32[2,256]{1,0:T(2,128)S(1)} fusion(bf16[2,256,2048]{2,1,0:T(8,128)(2,1)} %param.14), kind=kLoop, calls=%fused_computation.8 | loop fusion | flops 3145216 | bytes 2099200 | tf_op jit(solution)/shard_map/reduce_sum | solution.py:18
  3.6 0.7 fusion.27
  4.3 0.7 fusion.28
  5.1 4.7 %fusion.21 = bf16[8,2,256,128]{3,2,0,1:T(8,128)(2,1)S(1)} fusion(bf16[2,256,2048]{2,1,0:T(8,128)(2,1)S(1)} %copy-done.2, f32[2048]{0:T(1024)S(1)} %convert_element_type.100, f32[2,256]{1,0:T(2,128)S(1)} %add_rsqrt_fusion, bf16[2048,1024]{1,0:T(8,128)(2,1)} %param.17), kind=kOutput, calls=%fused_computation.25 | convolution fusion | flops 2152202240 | bytes 7350272 | tf_op jit(solution)/shard_map/apd,dhk->hapk/dot_general | solution.py:25
  9.9 2.4 %fusion.24 = bf16[8,2,256,128]{3,2,0,1:T(8,128)(2,1)S(1)} fusion(bf16[2,256,2048]{2,1,0:T(8,128)(2,1)S(1)} %copy-done.2, f32[2048]{0:T(1024)S(1)} %convert_element_type.100, f32[2,256]{1,0:T(2,128)S(1)} %add_rsqrt_fusion, bf16[2048,1024]{1,0:T(8,128)(2,1)S(1)} %copy-done.7), kind=kOutput, calls=%fused_computation.26 | convolution fusion | flops 2152202240 | bytes 7350272 | tf_op jit(solution)/shard_map/apd,dhk->hapk/dot_general | solution.py:25
  12.3 0.2 fusion.11
  12.4 0.1 copy.28
  12.6 43.0 %all_to_all.10 = bf16[8,2,520,128]{3,2,1,0:T(8,128)(2,1)} all-to-all(bf16[8,2,520,128]{3,2,1,0:T(8,128)(2,1)S(1)} %copy.28), channel_id=1, replica_groups=mesh['grp'=2,'sp'=16,'tp'=8] {'tp'}, dimensions={0} | all-to-all | bytes 4259840 | tf_op jit(solution)/shard_map/all_to_all | solution.py:106
  55.6 30.9 %all-to-all-start.1 = ((bf16[16,520,128]{2,1,0:T(8,128)(2,1)}), bf16[16,520,128]{2,1,0:T(8,128)(2,1)S(1)}, u32[]{:S(2)}, u32[]{:S(2)}) async-start(bf16[16,520,128]{2,1,0:T(8,128)(2,1)} %bitcast.13), calls=%async_computation.1 | async-start | bytes 4259840 | tf_op jit(solution)/shard_map/all_to_all | solution.py:108
  87.9 0.7 constant_dynamic-slice_fusion
  88.6 0.6 multiply_reduce_fusion
  89.2 47.0 %all-to-all-done.1 = bf16[16,520,128]{2,1,0:T(8,128)(2,1)S(1)} async-done(((bf16[16,520,128]{2,1,0:T(8,128)(2,1)}), bf16[16,520,128]{2,1,0:T(8,128)(2,1)S(1)}, u32[]{:S(2)}, u32[]{:S(2)}) %all-to-all-start.1) | async-done | bytes 2129952 | tf_op jit(solution)/shard_map/all_to_all | solution.py:108
  136.3 0.1 fusion.38
  136.4 1.2 reduce-window.6
  137.6 0.1 slice_reduce_fusion
  137.7 0.2 reduce-window.9
  138.1 0.3 fusion.42
  138.3 0.2 bitcast_convert_fusion
  138.6 0.4 copy-done.4
  139.1 0.6 fusion.41
  140.4 2.3 %fusion.45 = bf16[1,1,4096,128]{3,2,1,0:T(8,128)(2,1)} fusion(f32[4096,128]{1,0:T(8,128)S(1)} %bitcast_convert_fusion, f32[128]{0:T(128)S(1)} %get-tuple-element.11, f32[128]{0:T(128)S(1)} %get-tuple-element.12, f32[128]{0:T(128)S(1)} %get-tuple-element.13, f32[128]{0:T(128)S(1)} %get-tuple-element.10), kind=kLoop, calls=%fused_computation.59 | loop fusion | flops 6291456 | bytes 3147776 | tf_op jit(solution)/shard_map/reshape | solution.py:117
  142.7 2.0 %convert_reduce_fusion = (f32[]{:T(128)}, bf16[1,1,4096]{2,1,0:T(2,128)(2,1)S(1)}) fusion(f32[1,1,4096]{2,1,0:T(1,128)S(1)} %subtract_exponential_fusion, bf16[1,1,128]{2,1,0:T(2,128)(2,1)S(1)} %copy-done.10, f32[4096,128]{1,0:T(8,128)S(1)} %bitcast_convert_fusion, f32[128]{0:T(128)S(1)} %get-tuple-element.11, f32[128]{0:T(128)S(1)} %get-tuple-element.12, ...), kind=kOutput, calls=%fused_computation.43 | convolution fusion | flops 7360511 | bytes 2124036 | tf_op jit(solution)/shard_map/bhlk,bhk->bhl/dot_general | solution.py:65
  146.0 0.8 fusion.31
  (30 shorter events, 0.3 us)
Async XLA Ops:
  0.6 3.0 %copy-start = (bf16[2048,8]{0,1:T(8,128)(2,1)S(1)}, bf16[2048,8]{0,1:T(8,128)(2,1)}, u32[]{:S(2)}) copy-start(bf16[2048,8]{0,1:T(8,128)(2,1)} %param.18) | copy-start | bytes 98308
  0.6 3.0 %copy-start.2 = (bf16[2,256,2048]{2,1,0:T(8,128)(2,1)S(1)}, bf16[2,256,2048]{2,1,0:T(8,128)(2,1)}, u32[]{:S(2)}) copy-start(bf16[2,256,2048]{2,1,0:T(8,128)(2,1)} %param.14) | copy-start | bytes 6291460
  3.6 0.8 copy-start.8
  5.1 4.7 %copy-start.7 = (bf16[2048,1024]{1,0:T(8,128)(2,1)S(1)}, bf16[2048,1024]{1,0:T(8,128)(2,1)}, u32[]{:S(2)}) copy-start(bf16[2048,1024]{1,0:T(8,128)(2,1)} %param.16) | copy-start | bytes 12582916
  55.6 33.0 %copy-start.9 = (bf16[1,1,128]{2,1,0:T(2,128)(2,1)S(1)}, bf16[1,1,128]{2,1,0:T(2,128)(2,1)}, u32[]{:S(2)}) copy-start(bf16[1,1,128]{2,1,0:T(2,128)(2,1)} %param.24) | copy-start | bytes 772
  55.6 33.0 %copy-start.10 = (bf16[1,1,128]{2,1,0:T(2,128)(2,1)S(1)}, bf16[1,1,128]{2,1,0:T(2,128)(2,1)}, u32[]{:S(2)}) copy-start(bf16[1,1,128]{2,1,0:T(2,128)(2,1)} %param.23) | copy-start | bytes 772
  55.6 80.7 %copy-start.3 = (f32[1,1,4096]{2,1,0:T(1,128)S(1)}, f32[1,1,4096]{2,1,0:T(1,128)}, u32[]{:S(2)}) copy-start(f32[1,1,4096]{2,1,0:T(1,128)} %param.22) | copy-start | bytes 49156
  55.6 80.6 %all-to-all-start.1 = ((bf16[16,520,128]{2,1,0:T(8,128)(2,1)}), bf16[16,520,128]{2,1,0:T(8,128)(2,1)S(1)}, u32[]{:S(2)}, u32[]{:S(2)}) async-start(bf16[16,520,128]{2,1,0:T(8,128)(2,1)} %bitcast.13), calls=%async_computation.1 | async-start | bytes 4259840 | tf_op jit(solution)/shard_map/all_to_all | solution.py:108
  138.3 7.7 %copy-start.1 = (bf16[16,256,128]{2,1,0:T(8,128)(2,1)}, bf16[16,256,128]{2,1,0:T(8,128)(2,1)S(1)}, u32[]{:S(2)}) copy-start(bf16[16,256,128]{2,1,0:T(8,128)(2,1)S(1)} %get-tuple-element.8) | copy-start | bytes 3145732
  138.3 0.7 copy-start.4
  140.4 4.3 %copy-start.5 = (f32[1,1,4096]{2,1,0:T(1,128)}, f32[1,1,4096]{2,1,0:T(1,128)S(1)}, u32[]{:S(2)}) copy-start(f32[1,1,4096]{2,1,0:T(1,128)S(1)} %subtract_exponential_fusion) | copy-start | bytes 49156
  142.7 3.3 %copy-start.6 = (bf16[1,1,128]{2,1,0:T(2,128)(2,1)S(1)}, bf16[1,1,128]{2,1,0:T(2,128)(2,1)}, u32[]{:S(2)}) copy-start(bf16[1,1,128]{2,1,0:T(2,128)(2,1)} %param.25) | copy-start | bytes 772

commit v2 on v1

--- a/solution.py
+++ b/solution.py
@@ -2,6 +2,7 @@
 import jax.numpy as jnp
 from jax import lax
 from jax.sharding import PartitionSpec as P
+
 
 HEADS = 8
 DK = 128
@@ -23,12 +24,12 @@
 def project(normed, weight):
     matrix = weight.reshape(weight.shape[0], HEADS, DK)
     return jnp.einsum(
-        "apd,dhk->hapk", normed, matrix, preferred_element_type=jnp.float32
+        "pd,dhk->hpk", normed, matrix, preferred_element_type=jnp.float32
     ).astype(jnp.bfloat16)
 
 
 def gate(normed, weight):
-    linear = jnp.einsum("apd,dh->hap", normed, weight, preferred_element_type=jnp.float32)
+    linear = jnp.einsum("pd,dh->hp", normed, weight, preferred_element_type=jnp.float32)
     return linear.astype(jnp.bfloat16)
 
 
@@ -77,7 +78,48 @@
     return (weight_cache, first_read)
 
 
-def shards(
+def gather_sequence(layer_input):
+    pair, rows, width = layer_input.shape
+    core = lax.axis_index("sp") % pair
+    own = lax.dynamic_index_in_dim(layer_input, core, 0, keepdims=False)
+    other = lax.dynamic_index_in_dim(layer_input, 1 - core, 0, keepdims=False)
+    route = [(i, i ^ 1) for i in range(lax.axis_size("sp"))]
+    got = lax.ppermute(other, "sp", route)
+    first = core == 0
+    return jnp.stack([jnp.where(first, own, got), jnp.where(first, got, own)]).reshape(
+        pair * rows, width
+    )
+
+
+def rotate(block):
+    ring = lax.axis_size("tp")
+    here = lax.axis_index("tp")
+    got = []
+    for step in range(ring):
+        mine = lax.dynamic_index_in_dim(block, (here + step) % ring, 0, keepdims=False)
+        if step:
+            route = [(i, (i + step) % ring) for i in range(ring)]
+            mine = lax.ppermute(mine, "tp", route)
+        got.append(mine)
+    return jnp.stack(got)
+
+
+def spread(stack):
+    ring, chips = lax.axis_size("sp"), stack.shape[0]
+    pair = ring // chips
+    column, chip = lax.axis_index("tp"), lax.axis_index("sp") // pair
+    whole = jnp.zeros_like(stack)
+    for step in range(chips):
+        target = (chip + step) % chips
+        mine = lax.dynamic_index_in_dim(stack, (column - target) % chips, 0, keepdims=False)
+        if step:
+            route = [(i, (i // pair + step) % chips * pair + i % pair) for i in range(ring)]
+            mine = lax.ppermute(mine, "sp", route)
+        whole = lax.dynamic_update_index_in_dim(whole, mine, (chip - step) % chips, 0)
+    return whole
+
+
+def layer(
     layer_input,
     norm_gain,
     key_weight,
@@ -93,25 +135,21 @@
     new_input,
     new_forget,
 ):
-    seqs, rows, _ = layer_input.shape
+    normed = normalise(gather_sequence(layer_input), norm_gain)
+    rows = normed.shape[0]
     lines = rows // DK
-    normed = normalise(layer_input, norm_gain)
-    gates = jnp.stack(
-        [gate(normed, input_gate_weight), gate(normed, forget_gate_weight)], axis=2
-    ).reshape(HEADS, seqs, 2 * lines, DK)
-    gates = jnp.pad(gates, ((0, 0), (0, 0), (0, 8 - 2 * lines), (0, 0)))
-    block = jnp.concatenate(
-        [project(normed, key_weight), project(normed, value_weight), gates], axis=2
-    )
-    by_head = lax.all_to_all(block, "tp", split_axis=0, concat_axis=0, tiled=True)
-    by_head = by_head.reshape(-1, *block.shape[2:])
-    mine = lax.all_to_all(by_head, "sp", split_axis=0, concat_axis=0, tiled=True)
-    blocks = mine.shape[0]
-    length = blocks * rows
+    gates = jnp.stack([gate(normed, input_gate_weight), gate(normed, forget_gate_weight)], axis=1)
+    gates = gates.reshape(HEADS, 2 * lines, DK)
+    key_block = jnp.concatenate([project(normed, key_weight), gates], axis=1)
+    normed, key_block = lax.optimization_barrier((normed, key_block))
+    value_block = project(normed, value_weight)
+    mine = spread(rotate(key_block))
+    values = spread(rotate(value_block))
+    length = mine.shape[0] * rows
     key_linear = mine[:, :rows].reshape(length, DK)
-    values = mine[:, rows : 2 * rows].reshape(1, 1, length, DK)
-    input_linear = mine[:, 2 * rows : 2 * rows + lines].reshape(1, 1, length)
-    forget_linear = mine[:, 2 * rows + lines : 2 * rows + 2 * lines].reshape(1, 1, length)
+    values = values.reshape(1, 1, length, DK)
+    input_linear = mine[:, rows : rows + lines].reshape(1, 1, length)
+    forget_linear = mine[:, rows + lines : rows + 2 * lines].reshape(1, 1, length)
     head = lax.axis_index("tp")
     tap_weight = lax.dynamic_slice(conv_weight, (0, head * DK), (CONV, DK))
     keys = convolve(key_linear, tap_weight).reshape(1, 1, length, DK)
@@ -154,4 +192,4 @@
         P(("grp", "sp"), "tp", None),
         P(("grp", "sp"), "tp", None),
     )
-    return jax.shard_map(shards, mesh=mesh, in_specs=in_specs, out_specs=out_specs, check_vma=False)
+    return jax.shard_map(layer, mesh=mesh, in_specs=in_specs, out_specs=out_specs, check_vma=False)

time: 147 us -> 190 us (1.29)
  the two profiles are of different devices: /device:TPU:513 before, /device:TPU:640 now
where the time goes in v2:
time: 190 us; the launch traced here: 189 us
  starting transfers between devices  82.5 us (43%)
  waiting for transfers between devices  76.8 us (40%)
  matrix products  11.7 us (6%)
  other arithmetic  8.71 us (5%)
  local copies, waits for them, and re-layouts  4.86 us (3%)
  between operations  4.81 us (3%)
    ppermute x14, waiting for transfers between devices, rotate(): mine = lax.ppermute(mine, 'tp', route)  58 us
    ppermute x14, starting transfers between devices, spread(): mine = lax.ppermute(mine, 'sp', route)  49 us
    ppermute x14, starting transfers between devices, rotate(): mine = lax.ppermute(mine, 'tp', route)  33.6 us
    ppermute x14, waiting for transfers between devices, spread(): mine = lax.ppermute(mine, 'sp', route)  18.8 us
    dot_general x2, matrix products, project(): jnp.einsum('pd,dhk->hpk', normed, matrix, preferred_element_type=jnp.floa...  7.66 us
  transfers between devices with their start and end apart: 29, of which 13 were waited for; matrix products, arithmetic and copies ran while one was open for 1% of the time, Pallas kernels for 0%

profile of v2, /device:TPU:640, one launch (start us, length us, event | category | flops | bytes accessed | tf_op | source)
XLA Modules:
  0.0 189.5 jit_solution(14388480143404821493)
XLA Ops:
  10.9 5.3 %fusion.21 = bf16[8,512,128]{2,1,0:T(8,128)(2,1)S(1)} fusion(bf16[512,2048,1]{1,0,2:T(8,128)(2,1)} %bitcast.243, bf16[2048,1024]{1,0:T(8,128)(2,1)} %param.16), kind=kOutput, calls=%fused_computation.22 | convolution fusion | flops 2148007936 | bytes 7340032 | tf_op jit(solution)/shard_map/pd,dhk->hpk/dot_general | solution.py:26
  22.3 3.9 %collective-permute-start.2 = (bf16[520,128]{1,0:T(8,128)(2,1)S(1)}, bf16[520,128]{1,0:T(8,128)(2,1)S(1)}, u32[]{:S(2)}, u32[]{:S(2)}) collective-permute-start(bf16[520,128]{1,0:T(8,128)(2,1)S(1)} %get-tuple-element.27), channel_id=1, source_target_pairs={{0,2},{1,3},{2,4},{3,5},{4,6},{5,7},{6,0},{7,1},{8,10},{9,11},{10,... | collective-permute-start | bytes 399368 | tf_op jit(solution)/shard_map/ppermute | solution.py:102
  29.8 3.3 %collective-permute-start.16 = (bf16[512,128]{1,0:T(8,128)(2,1)S(1)}, bf16[512,128]{1,0:T(8,128)(2,1)S(1)}, u32[]{:S(2)}, u32[]{:S(2)}) collective-permute-start(bf16[512,128]{1,0:T(8,128)(2,1)S(1)} %get-tuple-element.43), channel_id=1, source_target_pairs={{0,2},{1,3},{2,4},{3,5},{4,6},{5,7},{6,0},{7,1},{8,10},{9,11},{10,... | collective-permute-start | bytes 393224 | tf_op jit(solution)/shard_map/ppermute | solution.py:102
  33.2 21.5 %collective-permute-done.16 = bf16[512,128]{1,0:T(8,128)(2,1)S(1)} collective-permute-done((bf16[512,128]{1,0:T(8,128)(2,1)S(1)}, bf16[512,128]{1,0:T(8,128)(2,1)S(1)}, u32[]{:S(2)}, u32[]{:S(2)}) %collective-permute-start.16) | collective-permute-done | bytes 131104 | tf_op jit(solution)/shard_map/ppermute | solution.py:102
  57.3 11.5 %collective-permute-done.17 = bf16[512,128]{1,0:T(8,128)(2,1)S(1)} collective-permute-done((bf16[512,128]{1,0:T(8,128)(2,1)S(1)}, bf16[512,128]{1,0:T(8,128)(2,1)S(1)}, u32[]{:S(2)}, u32[]{:S(2)}) %collective-permute-start.17) | collective-permute-done | bytes 131104 | tf_op jit(solution)/shard_map/ppermute | solution.py:102
  68.8 2.9 %collective-permute-start.18 = (bf16[512,128]{1,0:T(8,128)(2,1)S(1)}, bf16[512,128]{1,0:T(8,128)(2,1)S(1)}, u32[]{:S(2)}, u32[]{:S(2)}) collective-permute-start(bf16[512,128]{1,0:T(8,128)(2,1)S(1)} %get-tuple-element.41), channel_id=1, source_target_pairs={{0,4},{1,5},{2,6},{3,7},{4,0},{5,1},{6,2},{7,3},{8,12},{9,13},{10,... | collective-permute-start | bytes 393224 | tf_op jit(solution)/shard_map/ppermute | solution.py:102
  71.7 7.8 %collective-permute-done.18 = bf16[512,128]{1,0:T(8,128)(2,1)S(1)} collective-permute-done((bf16[512,128]{1,0:T(8,128)(2,1)S(1)}, bf16[512,128]{1,0:T(8,128)(2,1)S(1)}, u32[]{:S(2)}, u32[]{:S(2)}) %collective-permute-start.18) | collective-permute-done | bytes 131104 | tf_op jit(solution)/shard_map/ppermute | solution.py:102
  79.5 3.3 %collective-permute-start.19 = (bf16[512,128]{1,0:T(8,128)(2,1)S(1)}, bf16[512,128]{1,0:T(8,128)(2,1)S(1)}, u32[]{:S(2)}, u32[]{:S(2)}) collective-permute-start(bf16[512,128]{1,0:T(8,128)(2,1)S(1)} %get-tuple-element.40), channel_id=1, source_target_pairs={{0,5},{1,6},{2,7},{3,0},{4,1},{5,2},{6,3},{7,4},{8,13},{9,14},{10,... | collective-permute-start | bytes 393224 | tf_op jit(solution)/shard_map/ppermute | solution.py:102
  82.8 8.2 %collective-permute-done.19 = bf16[512,128]{1,0:T(8,128)(2,1)S(1)} collective-permute-done((bf16[512,128]{1,0:T(8,128)(2,1)S(1)}, bf16[512,128]{1,0:T(8,128)(2,1)S(1)}, u32[]{:S(2)}, u32[]{:S(2)}) %collective-permute-start.19) | collective-permute-done | bytes 131104 | tf_op jit(solution)/shard_map/ppermute | solution.py:102
  92.0 6.5 %collective-permute-done.20 = bf16[512,128]{1,0:T(8,128)(2,1)S(1)} collective-permute-done((bf16[512,128]{1,0:T(8,128)(2,1)S(1)}, bf16[512,128]{1,0:T(8,128)(2,1)S(1)}, u32[]{:S(2)}, u32[]{:S(2)}) %collective-permute-start.20) | collective-permute-done | bytes 131104 | tf_op jit(solution)/shard_map/ppermute | solution.py:102
  98.5 3.1 %collective-permute-start.21 = (bf16[512,128]{1,0:T(8,128)(2,1)S(1)}, bf16[512,128]{1,0:T(8,128)(2,1)S(1)}, u32[]{:S(2)}, u32[]{:S(2)}) collective-permute-start(bf16[512,128]{1,0:T(8,128)(2,1)S(1)} %get-tuple-element.38), channel_id=1, source_target_pairs={{0,7},{1,0},{2,1},{3,2},{4,3},{5,4},{6,5},{7,6},{8,15},{9,8},{10,9... | collective-permute-start | bytes 393224 | tf_op jit(solution)/shard_map/ppermute | solution.py:102
  107.1 3.5 %collective-permute-start.6 = (bf16[520,128]{1,0:T(8,128)(2,1)S(1)}, bf16[520,128]{1,0:T(8,128)(2,1)S(1)}, u32[]{:S(2)}, u32[]{:S(2)}) collective-permute-start(bf16[520,128]{1,0:T(8,128)(2,1)S(1)} %get-tuple-element.23), channel_id=1, source_target_pairs={{0,6},{1,7},{2,0},{3,1},{4,2},{5,3},{6,4},{7,5},{8,14},{9,15},{10,... | collective-permute-start | bytes 399368 | tf_op jit(solution)/shard_map/ppermute | solution.py:102
  110.9 2.9 %collective-permute-start.22 = (bf16[512,128]{1,0:T(8,128)(2,1)S(1)}, bf16[512,128]{1,0:T(8,128)(2,1)S(1)}, u32[]{:S(2)}, u32[]{:S(2)}) collective-permute-start(bf16[512,128]{1,0:T(8,128)(2,1)S(1)} %get-tuple-element.36), channel_id=1, source_target_pairs={{0,16},{8,24},{16,32},{24,40},{32,48},{40,56},{48,64},{56,72},{64,... | collective-permute-start | bytes 393224 | tf_op jit(solution)/shard_map/ppermute | solution.py:117
  113.8 5.1 %collective-permute-start.23 = (bf16[512,128]{1,0:T(8,128)(2,1)S(1)}, bf16[512,128]{1,0:T(8,128)(2,1)S(1)}, u32[]{:S(2)}, u32[]{:S(2)}) collective-permute-start(bf16[512,128]{1,0:T(8,128)(2,1)S(1)} %get-tuple-element.35), channel_id=1, source_target_pairs={{0,32},{8,40},{16,48},{24,56},{32,64},{40,72},{48,80},{56,88},{64,... | collective-permute-start | bytes 393224 | tf_op jit(solution)/shard_map/ppermute | solution.py:117
  118.9 6.7 %collective-permute-start.24 = (bf16[512,128]{1,0:T(8,128)(2,1)S(1)}, bf16[512,128]{1,0:T(8,128)(2,1)S(1)}, u32[]{:S(2)}, u32[]{:S(2)}) collective-permute-start(bf16[512,128]{1,0:T(8,128)(2,1)S(1)} %get-tuple-element.34), channel_id=1, source_target_pairs={{0,48},{8,56},{16,64},{24,72},{32,80},{40,88},{48,96},{56,104},{64... | collective-permute-start | bytes 393224 | tf_op jit(solution)/shard_map/ppermute | solution.py:117
  125.7 7.5 %collective-permute-start.25 = (bf16[512,128]{1,0:T(8,128)(2,1)S(1)}, bf16[512,128]{1,0:T(8,128)(2,1)S(1)}, u32[]{:S(2)}, u32[]{:S(2)}) collective-permute-start(bf16[512,128]{1,0:T(8,128)(2,1)S(1)} %get-tuple-element.33), channel_id=1, source_target_pairs={{0,64},{8,72},{16,80},{24,88},{32,96},{40,104},{48,112},{56,120},{... | collective-permute-start | bytes 393224 | tf_op jit(solution)/shard_map/ppermute | solution.py:117
  135.4 5.6 %collective-permute-start.27 = (bf16[512,128]{1,0:T(8,128)(2,1)S(1)}, bf16[512,128]{1,0:T(8,128)(2,1)S(1)}, u32[]{:S(2)}, u32[]{:S(2)}) collective-permute-start(bf16[512,128]{1,0:T(8,128)(2,1)S(1)} %get-tuple-element.31), channel_id=1, source_target_pairs={{0,96},{8,104},{16,112},{24,120},{32,0},{40,8},{48,16},{56,24},{64... | collective-permute-start | bytes 393224 | tf_op jit(solution)/shard_map/ppermute | solution.py:117
  141.7 4.3 %collective-permute-start.8 = (bf16[520,128]{1,0:T(8,128)(2,1)S(1)}, bf16[520,128]{1,0:T(8,128)(2,1)S(1)}, u32[]{:S(2)}, u32[]{:S(2)}) collective-permute-start(bf16[520,128]{1,0:T(8,128)(2,1)S(1)} %get-tuple-element.20), channel_id=1, source_target_pairs={{0,16},{8,24},{16,32},{24,40},{32,48},{40,56},{48,64},{56,72},{64,... | collective-permute-start | bytes 399368 | tf_op jit(solution)/shard_map/ppermute | solution.py:117
  148.5 2.8 %collective-permute-done.26 = bf16[512,128]{1,0:T(8,128)(2,1)S(1)} collective-permute-done((bf16[512,128]{1,0:T(8,128)(2,1)S(1)}, bf16[512,128]{1,0:T(8,128)(2,1)S(1)}, u32[]{:S(2)}, u32[]{:S(2)}) %collective-permute-start.26) | collective-permute-done | bytes 131104 | tf_op jit(solution)/shard_map/ppermute | solution.py:117
  152.9 3.8 %collective-permute-start.11 = (bf16[520,128]{1,0:T(8,128)(2,1)S(1)}, bf16[520,128]{1,0:T(8,128)(2,1)S(1)}, u32[]{:S(2)}, u32[]{:S(2)}) collective-permute-start(bf16[520,128]{1,0:T(8,128)(2,1)S(1)} %get-tuple-element.17), channel_id=1, source_target_pairs={{0,64},{8,72},{16,80},{24,88},{32,96},{40,104},{48,112},{56,120},{... | collective-permute-start | bytes 399368 | tf_op jit(solution)/shard_map/ppermute | solution.py:117
  158.9 4.4 %collective-permute-start.13 = (bf16[520,128]{1,0:T(8,128)(2,1)S(1)}, bf16[520,128]{1,0:T(8,128)(2,1)S(1)}, u32[]{:S(2)}, u32[]{:S(2)}) collective-permute-start(bf16[520,128]{1,0:T(8,128)(2,1)S(1)} %get-tuple-element.15), channel_id=1, source_target_pairs={{0,96},{8,104},{16,112},{24,120},{32,0},{40,8},{48,16},{56,24},{64... | collective-permute-start | bytes 399368 | tf_op jit(solution)/shard_map/ppermute | solution.py:117
  164.0 6.5 %collective-permute-done.10 = bf16[520,128]{1,0:T(8,128)(2,1)S(1)} collective-permute-done((bf16[520,128]{1,0:T(8,128)(2,1)S(1)}, bf16[520,128]{1,0:T(8,128)(2,1)S(1)}, u32[]{:S(2)}, u32[]{:S(2)}) %collective-permute-start.10) | collective-permute-done | bytes 133152 | tf_op jit(solution)/shard_map/ppermute | solution.py:117
  170.6 4.1 %collective-permute-done.12 = bf16[520,128]{1,0:T(8,128)(2,1)S(1)} collective-permute-done((bf16[520,128]{1,0:T(8,128)(2,1)S(1)}, bf16[520,128]{1,0:T(8,128)(2,1)S(1)}, u32[]{:S(2)}, u32[]{:S(2)}) %collective-permute-start.12) | collective-permute-done | bytes 133152 | tf_op jit(solution)/shard_map/ppermute | solution.py:117
  174.8 3.3 %collective-permute-done.13 = bf16[520,128]{1,0:T(8,128)(2,1)S(1)} collective-permute-done((bf16[520,128]{1,0:T(8,128)(2,1)S(1)}, bf16[520,128]{1,0:T(8,128)(2,1)S(1)}, u32[]{:S(2)}, u32[]{:S(2)}) %collective-permute-start.13) | collective-permute-done | bytes 133152 | tf_op jit(solution)/shard_map/ppermute | solution.py:117
  (127 shorter events, 46.8 us)
Async XLA Ops:
  20.5 86.6 %collective-permute-start.1 = (bf16[520,128]{1,0:T(8,128)(2,1)S(1)}, bf16[520,128]{1,0:T(8,128)(2,1)S(1)}, u32[]{:S(2)}, u32[]{:S(2)}) collective-permute-start(bf16[520,128]{1,0:T(8,128)(2,1)S(1)} %get-tuple-element.28), channel_id=1, source_target_pairs={{0,1},{1,2},{2,3},{3,4},{4,5},{5,6},{6,7},{7,0},{8,9},{9,10},{10,1... | collective-permute-start | bytes 399368 | tf_op jit(solution)/shard_map/ppermute | solution.py:102
  22.3 88.4 %collective-permute-start.2 = (bf16[520,128]{1,0:T(8,128)(2,1)S(1)}, bf16[520,128]{1,0:T(8,128)(2,1)S(1)}, u32[]{:S(2)}, u32[]{:S(2)}) collective-permute-start(bf16[520,128]{1,0:T(8,128)(2,1)S(1)} %get-tuple-element.27), channel_id=1, source_target_pairs={{0,2},{1,3},{2,4},{3,5},{4,6},{5,7},{6,0},{7,1},{8,10},{9,11},{10,... | collective-permute-start | bytes 399368 | tf_op jit(solution)/shard_map/ppermute | solution.py:102
  26.2 84.7 %collective-permute-start.3 = (bf16[520,128]{1,0:T(8,128)(2,1)S(1)}, bf16[520,128]{1,0:T(8,128)(2,1)S(1)}, u32[]{:S(2)}, u32[]{:S(2)}) collective-permute-start(bf16[520,128]{1,0:T(8,128)(2,1)S(1)} %get-tuple-element.26), channel_id=1, source_target_pairs={{0,3},{1,4},{2,5},{3,6},{4,7},{5,0},{6,1},{7,2},{8,11},{9,12},{10,... | collective-permute-start | bytes 399368 | tf_op jit(solution)/shard_map/ppermute | solution.py:102
  27.2 86.6 %collective-permute-start.4 = (bf16[520,128]{1,0:T(8,128)(2,1)S(1)}, bf16[520,128]{1,0:T(8,128)(2,1)S(1)}, u32[]{:S(2)}, u32[]{:S(2)}) collective-permute-start(bf16[520,128]{1,0:T(8,128)(2,1)S(1)} %get-tuple-element.25), channel_id=1, source_target_pairs={{0,4},{1,5},{2,6},{3,7},{4,0},{5,1},{6,2},{7,3},{8,12},{9,13},{10,... | collective-permute-start | bytes 399368 | tf_op jit(solution)/shard_map/ppermute | solution.py:102
  29.8 24.8 %collective-permute-start.16 = (bf16[512,128]{1,0:T(8,128)(2,1)S(1)}, bf16[512,128]{1,0:T(8,128)(2,1)S(1)}, u32[]{:S(2)}, u32[]{:S(2)}) collective-permute-start(bf16[512,128]{1,0:T(8,128)(2,1)S(1)} %get-tuple-element.43), channel_id=1, source_target_pairs={{0,2},{1,3},{2,4},{3,5},{4,6},{5,7},{6,0},{7,1},{8,10},{9,11},{10,... | collective-permute-start | bytes 393224 | tf_op jit(solution)/shard_map/ppermute | solution.py:102
  54.7 14.1 %collective-permute-start.17 = (bf16[512,128]{1,0:T(8,128)(2,1)S(1)}, bf16[512,128]{1,0:T(8,128)(2,1)S(1)}, u32[]{:S(2)}, u32[]{:S(2)}) collective-permute-start(bf16[512,128]{1,0:T(8,128)(2,1)S(1)} %get-tuple-element.42), channel_id=1, source_target_pairs={{0,3},{1,4},{2,5},{3,6},{4,7},{5,0},{6,1},{7,2},{8,11},{9,12},{10,... | collective-permute-start | bytes 393224 | tf_op jit(solution)/shard_map/ppermute | solution.py:102
  79.5 11.5 %collective-permute-start.19 = (bf16[512,128]{1,0:T(8,128)(2,1)S(1)}, bf16[512,128]{1,0:T(8,128)(2,1)S(1)}, u32[]{:S(2)}, u32[]{:S(2)}) collective-permute-start(bf16[512,128]{1,0:T(8,128)(2,1)S(1)} %get-tuple-element.40), channel_id=1, source_target_pairs={{0,5},{1,6},{2,7},{3,0},{4,1},{5,2},{6,3},{7,4},{8,13},{9,14},{10,... | collective-permute-start | bytes 393224 | tf_op jit(solution)/shard_map/ppermute | solution.py:102
  104.1 14.8 %collective-permute-start.5 = (bf16[520,128]{1,0:T(8,128)(2,1)S(1)}, bf16[520,128]{1,0:T(8,128)(2,1)S(1)}, u32[]{:S(2)}, u32[]{:S(2)}) collective-permute-start(bf16[520,128]{1,0:T(8,128)(2,1)S(1)} %get-tuple-element.24), channel_id=1, source_target_pairs={{0,5},{1,6},{2,7},{3,0},{4,1},{5,2},{6,3},{7,4},{8,13},{9,14},{10,... | collective-permute-start | bytes 399368 | tf_op jit(solution)/shard_map/ppermute | solution.py:102
  107.1 18.5 %collective-permute-start.6 = (bf16[520,128]{1,0:T(8,128)(2,1)S(1)}, bf16[520,128]{1,0:T(8,128)(2,1)S(1)}, u32[]{:S(2)}, u32[]{:S(2)}) collective-permute-start(bf16[520,128]{1,0:T(8,128)(2,1)S(1)} %get-tuple-element.23), channel_id=1, source_target_pairs={{0,6},{1,7},{2,0},{3,1},{4,2},{5,3},{6,4},{7,5},{8,14},{9,15},{10,... | collective-permute-start | bytes 399368 | tf_op jit(solution)/shard_map/ppermute | solution.py:102
  110.7 22.5 %collective-permute-start.7 = (bf16[520,128]{1,0:T(8,128)(2,1)S(1)}, bf16[520,128]{1,0:T(8,128)(2,1)S(1)}, u32[]{:S(2)}, u32[]{:S(2)}) collective-permute-start(bf16[520,128]{1,0:T(8,128)(2,1)S(1)} %get-tuple-element.22), channel_id=1, source_target_pairs={{0,7},{1,0},{2,1},{3,2},{4,3},{5,4},{6,5},{7,6},{8,15},{9,8},{10,9... | collective-permute-start | bytes 399368 | tf_op jit(solution)/shard_map/ppermute | solution.py:102
  110.9 24.6 %collective-permute-start.22 = (bf16[512,128]{1,0:T(8,128)(2,1)S(1)}, bf16[512,128]{1,0:T(8,128)(2,1)S(1)}, u32[]{:S(2)}, u32[]{:S(2)}) collective-permute-start(bf16[512,128]{1,0:T(8,128)(2,1)S(1)} %get-tuple-element.36), channel_id=1, source_target_pairs={{0,16},{8,24},{16,32},{24,40},{32,48},{40,56},{48,64},{56,72},{64,... | collective-permute-start | bytes 393224 | tf_op jit(solution)/shard_map/ppermute | solution.py:117
  113.8 27.2 %collective-permute-start.23 = (bf16[512,128]{1,0:T(8,128)(2,1)S(1)}, bf16[512,128]{1,0:T(8,128)(2,1)S(1)}, u32[]{:S(2)}, u32[]{:S(2)}) collective-permute-start(bf16[512,128]{1,0:T(8,128)(2,1)S(1)} %get-tuple-element.35), channel_id=1, source_target_pairs={{0,32},{8,40},{16,48},{24,56},{32,64},{40,72},{48,80},{56,88},{64,... | collective-permute-start | bytes 393224 | tf_op jit(solution)/shard_map/ppermute | solution.py:117
  118.9 22.8 %collective-permute-start.24 = (bf16[512,128]{1,0:T(8,128)(2,1)S(1)}, bf16[512,128]{1,0:T(8,128)(2,1)S(1)}, u32[]{:S(2)}, u32[]{:S(2)}) collective-permute-start(bf16[512,128]{1,0:T(8,128)(2,1)S(1)} %get-tuple-element.34), channel_id=1, source_target_pairs={{0,48},{8,56},{16,64},{24,72},{32,80},{40,88},{48,96},{56,104},{64... | collective-permute-start | bytes 393224 | tf_op jit(solution)/shard_map/ppermute | solution.py:117
  125.7 20.4 %collective-permute-start.25 = (bf16[512,128]{1,0:T(8,128)(2,1)S(1)}, bf16[512,128]{1,0:T(8,128)(2,1)S(1)}, u32[]{:S(2)}, u32[]{:S(2)}) collective-permute-start(bf16[512,128]{1,0:T(8,128)(2,1)S(1)} %get-tuple-element.33), channel_id=1, source_target_pairs={{0,64},{8,72},{16,80},{24,88},{32,96},{40,104},{48,112},{56,120},{... | collective-permute-start | bytes 393224 | tf_op jit(solution)/shard_map/ppermute | solution.py:117
  133.2 18.0 %collective-permute-start.26 = (bf16[512,128]{1,0:T(8,128)(2,1)S(1)}, bf16[512,128]{1,0:T(8,128)(2,1)S(1)}, u32[]{:S(2)}, u32[]{:S(2)}) collective-permute-start(bf16[512,128]{1,0:T(8,128)(2,1)S(1)} %get-tuple-element.32), channel_id=1, source_target_pairs={{0,80},{8,88},{16,96},{24,104},{32,112},{40,120},{48,0},{56,8},{64... | collective-permute-start | bytes 393224 | tf_op jit(solution)/shard_map/ppermute | solution.py:117
  135.4 17.5 %collective-permute-start.27 = (bf16[512,128]{1,0:T(8,128)(2,1)S(1)}, bf16[512,128]{1,0:T(8,128)(2,1)S(1)}, u32[]{:S(2)}, u32[]{:S(2)}) collective-permute-start(bf16[512,128]{1,0:T(8,128)(2,1)S(1)} %get-tuple-element.31), channel_id=1, source_target_pairs={{0,96},{8,104},{16,112},{24,120},{32,0},{40,8},{48,16},{56,24},{64... | collective-permute-start | bytes 393224 | tf_op jit(solution)/shard_map/ppermute | solution.py:117
  141.1 16.1 %collective-permute-start.28 = (bf16[512,128]{1,0:T(8,128)(2,1)S(1)}, bf16[512,128]{1,0:T(8,128)(2,1)S(1)}, u32[]{:S(2)}, u32[]{:S(2)}) collective-permute-start(bf16[512,128]{1,0:T(8,128)(2,1)S(1)} %get-tuple-element.30), channel_id=1, source_target_pairs={{0,112},{8,120},{16,0},{24,8},{32,16},{40,24},{48,32},{56,40},{64,... | collective-permute-start | bytes 393224 | tf_op jit(solution)/shard_map/ppermute | solution.py:117
  141.7 17.2 %collective-permute-start.8 = (bf16[520,128]{1,0:T(8,128)(2,1)S(1)}, bf16[520,128]{1,0:T(8,128)(2,1)S(1)}, u32[]{:S(2)}, u32[]{:S(2)}) collective-permute-start(bf16[520,128]{1,0:T(8,128)(2,1)S(1)} %get-tuple-element.20), channel_id=1, source_target_pairs={{0,16},{8,24},{16,32},{24,40},{32,48},{40,56},{48,64},{56,72},{64,... | collective-permute-start | bytes 399368 | tf_op jit(solution)/shard_map/ppermute | solution.py:117
  146.1 17.3 %collective-permute-start.9 = (bf16[520,128]{1,0:T(8,128)(2,1)S(1)}, bf16[520,128]{1,0:T(8,128)(2,1)S(1)}, u32[]{:S(2)}, u32[]{:S(2)}) collective-permute-start(bf16[520,128]{1,0:T(8,128)(2,1)S(1)} %get-tuple-element.19), channel_id=1, source_target_pairs={{0,32},{8,40},{16,48},{24,56},{32,64},{40,72},{48,80},{56,88},{64,... | collective-permute-start | bytes 399368 | tf_op jit(solution)/shard_map/ppermute | solution.py:117
  151.3 19.3 %collective-permute-start.10 = (bf16[520,128]{1,0:T(8,128)(2,1)S(1)}, bf16[520,128]{1,0:T(8,128)(2,1)S(1)}, u32[]{:S(2)}, u32[]{:S(2)}) collective-permute-start(bf16[520,128]{1,0:T(8,128)(2,1)S(1)} %get-tuple-element.18), channel_id=1, source_target_pairs={{0,48},{8,56},{16,64},{24,72},{32,80},{40,88},{48,96},{56,104},{64... | collective-permute-start | bytes 399368 | tf_op jit(solution)/shard_map/ppermute | solution.py:117
  152.9 17.7 %collective-permute-start.11 = (bf16[520,128]{1,0:T(8,128)(2,1)S(1)}, bf16[520,128]{1,0:T(8,128)(2,1)S(1)}, u32[]{:S(2)}, u32[]{:S(2)}) collective-permute-start(bf16[520,128]{1,0:T(8,128)(2,1)S(1)} %get-tuple-element.17), channel_id=1, source_target_pairs={{0,64},{8,72},{16,80},{24,88},{32,96},{40,104},{48,112},{56,120},{... | collective-permute-start | bytes 399368 | tf_op jit(solution)/shard_map/ppermute | solution.py:117
  157.2 17.6 %collective-permute-start.12 = (bf16[520,128]{1,0:T(8,128)(2,1)S(1)}, bf16[520,128]{1,0:T(8,128)(2,1)S(1)}, u32[]{:S(2)}, u32[]{:S(2)}) collective-permute-start(bf16[520,128]{1,0:T(8,128)(2,1)S(1)} %get-tuple-element.16), channel_id=1, source_target_pairs={{0,80},{8,88},{16,96},{24,104},{32,112},{40,120},{48,0},{56,8},{64... | collective-permute-start | bytes 399368 | tf_op jit(solution)/shard_map/ppermute | solution.py:117
  158.9 19.1 %collective-permute-start.13 = (bf16[520,128]{1,0:T(8,128)(2,1)S(1)}, bf16[520,128]{1,0:T(8,128)(2,1)S(1)}, u32[]{:S(2)}, u32[]{:S(2)}) collective-permute-start(bf16[520,128]{1,0:T(8,128)(2,1)S(1)} %get-tuple-element.15), channel_id=1, source_target_pairs={{0,96},{8,104},{16,112},{24,120},{32,0},{40,8},{48,16},{56,24},{64... | collective-permute-start | bytes 399368 | tf_op jit(solution)/shard_map/ppermute | solution.py:117
  163.3 16.1 %collective-permute-start.14 = (bf16[520,128]{1,0:T(8,128)(2,1)S(1)}, bf16[520,128]{1,0:T(8,128)(2,1)S(1)}, u32[]{:S(2)}, u32[]{:S(2)}) collective-permute-start(bf16[520,128]{1,0:T(8,128)(2,1)S(1)} %get-tuple-element.14), channel_id=1, source_target_pairs={{0,112},{8,120},{16,0},{24,8},{32,16},{40,24},{48,32},{56,40},{64,... | collective-permute-start | bytes 399368 | tf_op jit(solution)/shard_map/ppermute | solution.py:117
  (17 other events, 132.8 us)

commit v3 on v2

--- a/solution.py
+++ b/solution.py
@@ -24,12 +24,12 @@
 def project(normed, weight):
     matrix = weight.reshape(weight.shape[0], HEADS, DK)
     return jnp.einsum(
-        "pd,dhk->hpk", normed, matrix, preferred_element_type=jnp.float32
+        "apd,dhk->hapk", normed, matrix, preferred_element_type=jnp.float32
     ).astype(jnp.bfloat16)
 
 
 def gate(normed, weight):
-    linear = jnp.einsum("pd,dh->hp", normed, weight, preferred_element_type=jnp.float32)
+    linear = jnp.einsum("apd,dh->hap", normed, weight, preferred_element_type=jnp.float32)
     return linear.astype(jnp.bfloat16)
 
 
@@ -59,15 +59,17 @@
     log_forget = jax.nn.log_sigmoid(forget_linear.astype(jnp.float32) + forget_shift)
     suffix = lax.cumsum(log_forget, axis=2, reverse=True) - log_forget
     new_decay = jax.nn.log_sigmoid(new_forget)
-    log_weight = input_linear.astype(jnp.float32) + input_shift + suffix + new_decay[:, :, None]
+    base = lax.optimization_barrier(input_shift + new_decay[:, :, None])
+    log_weight = input_linear.astype(jnp.float32) + base + suffix
     largest = jnp.maximum(jnp.max(log_weight, axis=2), new_input)
     weight_cache = jnp.exp(log_weight - largest[:, :, None])
     new_weight = jnp.exp(new_input - largest)
+    fresh_match = jnp.sum(new_key.astype(jnp.float32) * new_query.astype(jnp.float32), axis=2)
+    new_score = (new_weight * fresh_match * scaling).astype(jnp.bfloat16)
     matched = jnp.einsum("bhlk,bhk->bhl", keys, new_query, preferred_element_type=jnp.float32)
     scores = (weight_cache * matched * scaling).astype(jnp.bfloat16)
-    fresh_match = jnp.sum(new_key.astype(jnp.float32) * new_query.astype(jnp.float32), axis=2)
-    new_score = (new_weight * fresh_match * scaling).astype(jnp.bfloat16)
-    denominator = jnp.sum(scores.astype(jnp.float32), axis=2) + new_score.astype(jnp.float32)
+    denominator = jnp.sum(scores.astype(jnp.float32), axis=2)
+    denominator = denominator + new_score.astype(jnp.float32)
     numerator = jnp.einsum("bhl,bhlk->bhk", scores, values, preferred_element_type=jnp.float32)
     numerator = numerator + new_score.astype(jnp.float32)[:, :, None] * new_value.astype(
         jnp.float32
@@ -78,17 +80,15 @@
     return (weight_cache, first_read)
 
 
-def gather_sequence(layer_input):
-    pair, rows, width = layer_input.shape
+def trade(block):
+    pair = block.shape[1]
     core = lax.axis_index("sp") % pair
-    own = lax.dynamic_index_in_dim(layer_input, core, 0, keepdims=False)
-    other = lax.dynamic_index_in_dim(layer_input, 1 - core, 0, keepdims=False)
+    own = lax.dynamic_index_in_dim(block, core, 1, keepdims=False)
+    other = lax.dynamic_index_in_dim(block, 1 - core, 1, keepdims=False)
     route = [(i, i ^ 1) for i in range(lax.axis_size("sp"))]
     got = lax.ppermute(other, "sp", route)
     first = core == 0
-    return jnp.stack([jnp.where(first, own, got), jnp.where(first, got, own)]).reshape(
-        pair * rows, width
-    )
+    return jnp.stack([jnp.where(first, own, got), jnp.where(first, got, own)], axis=1)
 
 
 def rotate(block):
@@ -135,15 +135,19 @@
     new_input,
     new_forget,
 ):
-    normed = normalise(gather_sequence(layer_input), norm_gain)
-    rows = normed.shape[0]
+    seqs, rows, _ = layer_input.shape
     lines = rows // DK
-    gates = jnp.stack([gate(normed, input_gate_weight), gate(normed, forget_gate_weight)], axis=1)
-    gates = gates.reshape(HEADS, 2 * lines, DK)
-    key_block = jnp.concatenate([project(normed, key_weight), gates], axis=1)
+    normed = normalise(layer_input, norm_gain)
+    gates = jnp.stack(
+        [gate(normed, input_gate_weight), gate(normed, forget_gate_weight)], axis=2
+    ).reshape(HEADS, seqs, 2 * lines, DK)
+    gates = jnp.pad(gates, ((0, 0), (0, 0), (0, 8 - 2 * lines), (0, 0)))
+    key_block = jnp.concatenate([project(normed, key_weight), gates], axis=2)
     normed, key_block = lax.optimization_barrier((normed, key_block))
     value_block = project(normed, value_weight)
-    mine = spread(rotate(key_block))
+    value_block = trade(value_block).reshape(HEADS, seqs * rows, DK)
+    mine = trade(spread(rotate(key_block)))
+    mine = mine.reshape((-1,) + mine.shape[2:])
     values = spread(rotate(value_block))
     length = mine.shape[0] * rows
     key_linear = mine[:, :rows].reshape(length, DK)

time: 190 us -> 166 us (0.87)
  the two profiles are of different devices: /device:TPU:640 before, /device:TPU:513 now
where the time goes in v3:
time: 166 us; the launch traced here: 164 us
  starting transfers between devices  72.7 us (44%)
  waiting for transfers between devices  49.7 us (30%)
  matrix products  14.2 us (9%)
  local copies, waits for them, and re-layouts  11.3 us (7%)
  other arithmetic  11 us (7%)
  between operations  4.82 us (3%)
    ppermute x14, starting transfers between devices, rotate(): mine = lax.ppermute(mine, 'tp', route)  32.7 us
    ppermute x14, waiting for transfers between devices, spread(): mine = lax.ppermute(mine, 'sp', route)  32.3 us
    ppermute x14, starting transfers between devices, spread(): mine = lax.ppermute(mine, 'sp', route)  22 us
    ppermute x2, starting transfers between devices, trade(): got = lax.ppermute(other, 'sp', route)  17.9 us
    ppermute x14, waiting for transfers between devices, rotate(): mine = lax.ppermute(mine, 'tp', route)  17.5 us
    dot_general x2, matrix products, project(): jnp.einsum('apd,dhk->hapk', normed, matrix, preferred_element_type=jnp.fl...  10.1 us
    unnamed x36, local copies, waits for them, and re-layouts  5.45 us
  transfers between devices with their start and end apart: 30, of which 12 were waited for; matrix products, arithmetic and copies ran while one was open for 11% of the time, Pallas kernels for 0%

profile of v3, /device:TPU:513, one launch (start us, length us, event | category | flops | bytes accessed | tf_op | source)
XLA Modules:
  0.0 163.7 jit_solution(3708598894867962436)
XLA Ops:
  5.7 4.5 %fusion.20 = bf16[8,2,256,128]{3,2,0,1:T(8,128)(2,1)S(1)} fusion(bf16[2,256,2048]{2,1,0:T(8,128)(2,1)S(1)} %fusion.5, bf16[2048,1024]{1,0:T(8,128)(2,1)} %param.16), kind=kOutput, calls=%fused_computation.24 | convolution fusion | flops 2148007936 | bytes 7340032 | tf_op jit(solution)/shard_map/apd,dhk->hapk/dot_general | solution.py:26
  13.6 2.4 %collective-permute-start.1 = (bf16[2,264,128]{2,1,0:T(8,128)(2,1)}, bf16[2,264,128]{2,1,0:T(8,128)(2,1)}, u32[]{:S(2)}, u32[]{:S(2)}) collective-permute-start(bf16[2,264,128]{2,1,0:T(8,128)(2,1)} %get-tuple-element.29), channel_id=1, source_target_pairs={{0,2},{1,3},{2,4},{3,5},{4,6},{5,7},{6,0},{7,1},{8,10},{9,11},{10,... | collective-permute-start | bytes 405512 | tf_op jit(solution)/shard_map/ppermute | solution.py:102
  16.0 2.9 %collective-permute-start.2 = (bf16[2,264,128]{2,1,0:T(8,128)(2,1)}, bf16[2,264,128]{2,1,0:T(8,128)(2,1)}, u32[]{:S(2)}, u32[]{:S(2)}) collective-permute-start(bf16[2,264,128]{2,1,0:T(8,128)(2,1)} %get-tuple-element.28), channel_id=1, source_target_pairs={{0,3},{1,4},{2,5},{3,6},{4,7},{5,0},{6,1},{7,2},{8,11},{9,12},{10,... | collective-permute-start | bytes 405512 | tf_op jit(solution)/shard_map/ppermute | solution.py:102
  20.4 3.2 %collective-permute-start.4 = (bf16[2,264,128]{2,1,0:T(8,128)(2,1)}, bf16[2,264,128]{2,1,0:T(8,128)(2,1)}, u32[]{:S(2)}, u32[]{:S(2)}) collective-permute-start(bf16[2,264,128]{2,1,0:T(8,128)(2,1)} %get-tuple-element.26), channel_id=1, source_target_pairs={{0,5},{1,6},{2,7},{3,0},{4,1},{5,2},{6,3},{7,4},{8,13},{9,14},{10,... | collective-permute-start | bytes 405512 | tf_op jit(solution)/shard_map/ppermute | solution.py:102
  25.0 5.6 %fusion.17 = bf16[2,256,8,128]{3,1,2,0:T(8,128)(2,1)} fusion(bf16[2,256,2048]{2,1,0:T(8,128)(2,1)S(1)} %fusion.5, bf16[2048,1024]{1,0:T(8,128)(2,1)} %param.17), kind=kOutput, calls=%fused_computation.23 | convolution fusion | flops 2148007936 | bytes 7340032 | tf_op jit(solution)/shard_map/apd,dhk->hapk/dot_general | solution.py:26
  32.5 3.0 %collective-permute-start.5 = (bf16[2,264,128]{2,1,0:T(8,128)(2,1)S(1)}, bf16[2,264,128]{2,1,0:T(8,128)(2,1)S(1)}, u32[]{:S(2)}, u32[]{:S(2)}) collective-permute-start(bf16[2,264,128]{2,1,0:T(8,128)(2,1)S(1)} %get-tuple-element.25), channel_id=1, source_target_pairs={{0,6},{1,7},{2,0},{3,1},{4,2},{5,3},{6,4},{7,5},{8,14},{9,15},{10,... | collective-permute-start | bytes 405512 | tf_op jit(solution)/shard_map/ppermute | solution.py:102
  38.5 15.8 %collective-permute-start.15 = (bf16[8,256,128]{2,1,0:T(8,128)(2,1)}, bf16[8,256,128]{2,1,0:T(8,128)(2,1)}, u32[]{:S(2)}, u32[]{:S(2)}) collective-permute-start(bf16[8,256,128]{2,1,0:T(8,128)(2,1)} %dynamic-slice_bitcast_fusion.1), channel_id=1, source_target_pairs={{0,8},{8,0},{16,24},{24,16},{32,40},{40,32},{48,56},{56,48},{64,72... | collective-permute-start | bytes 1572872 | tf_op jit(solution)/shard_map/ppermute | solution.py:89
  60.4 2.5 %collective-permute-start.9 = (bf16[2,264,128]{2,1,0:T(8,128)(2,1)}, bf16[2,264,128]{2,1,0:T(8,128)(2,1)S(1)}, u32[]{:S(2)}, u32[]{:S(2)}) collective-permute-start(bf16[2,264,128]{2,1,0:T(8,128)(2,1)} %get-tuple-element.20), channel_id=1, source_target_pairs={{0,48},{8,56},{16,64},{24,72},{32,80},{40,88},{48,96},{56,104},{64... | collective-permute-start | bytes 405512 | tf_op jit(solution)/shard_map/ppermute | solution.py:117
  62.9 3.1 %collective-permute-start.10 = (bf16[2,264,128]{2,1,0:T(8,128)(2,1)}, bf16[2,264,128]{2,1,0:T(8,128)(2,1)S(1)}, u32[]{:S(2)}, u32[]{:S(2)}) collective-permute-start(bf16[2,264,128]{2,1,0:T(8,128)(2,1)} %get-tuple-element.19), channel_id=1, source_target_pairs={{0,64},{8,72},{16,80},{24,88},{32,96},{40,104},{48,112},{56,120},{... | collective-permute-start | bytes 405512 | tf_op jit(solution)/shard_map/ppermute | solution.py:117
  65.9 2.7 %collective-permute-start.11 = (bf16[2,264,128]{2,1,0:T(8,128)(2,1)}, bf16[2,264,128]{2,1,0:T(8,128)(2,1)S(1)}, u32[]{:S(2)}, u32[]{:S(2)}) collective-permute-start(bf16[2,264,128]{2,1,0:T(8,128)(2,1)} %get-tuple-element.18), channel_id=1, source_target_pairs={{0,80},{8,88},{16,96},{24,104},{32,112},{40,120},{48,0},{56,8},{64... | collective-permute-start | bytes 405512 | tf_op jit(solution)/shard_map/ppermute | solution.py:117
  69.7 9.9 %collective-permute-done.9 = bf16[2,264,128]{2,1,0:T(8,128)(2,1)S(1)} collective-permute-done((bf16[2,264,128]{2,1,0:T(8,128)(2,1)}, bf16[2,264,128]{2,1,0:T(8,128)(2,1)S(1)}, u32[]{:S(2)}, u32[]{:S(2)}) %collective-permute-start.9) | collective-permute-done | bytes 135200 | tf_op jit(solution)/shard_map/ppermute | solution.py:117
  81.9 3.6 %collective-permute-start.16 = (bf16[512,128]{1,0:T(8,128)(2,1)S(1)}, bf16[512,128]{1,0:T(8,128)(2,1)S(1)}, u32[]{:S(2)}, u32[]{:S(2)}) collective-permute-start(bf16[512,128]{1,0:T(8,128)(2,1)S(1)} %get-tuple-element.46), channel_id=1, source_target_pairs={{0,1},{1,2},{2,3},{3,4},{4,5},{5,6},{6,7},{7,0},{8,9},{9,10},{10,1... | collective-permute-start | bytes 393224 | tf_op jit(solution)/shard_map/ppermute | solution.py:102
  85.5 2.5 %collective-permute-done.12 = bf16[2,264,128]{2,1,0:T(8,128)(2,1)S(1)} collective-permute-done((bf16[2,264,128]{2,1,0:T(8,128)(2,1)S(1)}, bf16[2,264,128]{2,1,0:T(8,128)(2,1)S(1)}, u32[]{:S(2)}, u32[]{:S(2)}) %collective-permute-start.12) | collective-permute-done | bytes 135200 | tf_op jit(solution)/shard_map/ppermute | solution.py:117
  89.8 3.1 %collective-permute-start.18 = (bf16[512,128]{1,0:T(8,128)(2,1)S(1)}, bf16[512,128]{1,0:T(8,128)(2,1)S(1)}, u32[]{:S(2)}, u32[]{:S(2)}) collective-permute-start(bf16[512,128]{1,0:T(8,128)(2,1)S(1)} %get-tuple-element.44), channel_id=1, source_target_pairs={{0,3},{1,4},{2,5},{3,6},{4,7},{5,0},{6,1},{7,2},{8,11},{9,12},{10,... | collective-permute-start | bytes 393224 | tf_op jit(solution)/shard_map/ppermute | solution.py:102
  92.9 2.8 %collective-permute-start.19 = (bf16[512,128]{1,0:T(8,128)(2,1)S(1)}, bf16[512,128]{1,0:T(8,128)(2,1)S(1)}, u32[]{:S(2)}, u32[]{:S(2)}) collective-permute-start(bf16[512,128]{1,0:T(8,128)(2,1)S(1)} %get-tuple-element.43), channel_id=1, source_target_pairs={{0,4},{1,5},{2,6},{3,7},{4,0},{5,1},{6,2},{7,3},{8,12},{9,13},{10,... | collective-permute-start | bytes 393224 | tf_op jit(solution)/shard_map/ppermute | solution.py:102
  97.6 3.4 %collective-permute-start.21 = (bf16[512,128]{1,0:T(8,128)(2,1)S(1)}, bf16[512,128]{1,0:T(8,128)(2,1)S(1)}, u32[]{:S(2)}, u32[]{:S(2)}) collective-permute-start(bf16[512,128]{1,0:T(8,128)(2,1)S(1)} %get-tuple-element.41), channel_id=1, source_target_pairs={{0,6},{1,7},{2,0},{3,1},{4,2},{5,3},{6,4},{7,5},{8,14},{9,15},{10,... | collective-permute-start | bytes 393224 | tf_op jit(solution)/shard_map/ppermute | solution.py:102
  101.0 6.6 %collective-permute-done.18 = bf16[512,128]{1,0:T(8,128)(2,1)S(1)} collective-permute-done((bf16[512,128]{1,0:T(8,128)(2,1)S(1)}, bf16[512,128]{1,0:T(8,128)(2,1)S(1)}, u32[]{:S(2)}, u32[]{:S(2)}) %collective-permute-start.18) | collective-permute-done | bytes 131104 | tf_op jit(solution)/shard_map/ppermute | solution.py:102
  111.2 6.8 %collective-permute-done.21 = bf16[512,128]{1,0:T(8,128)(2,1)S(1)} collective-permute-done((bf16[512,128]{1,0:T(8,128)(2,1)S(1)}, bf16[512,128]{1,0:T(8,128)(2,1)S(1)}, u32[]{:S(2)}, u32[]{:S(2)}) %collective-permute-start.21) | collective-permute-done | bytes 131104 | tf_op jit(solution)/shard_map/ppermute | solution.py:102
  123.6 3.3 %collective-permute-start.25 = (bf16[512,128]{1,0:T(8,128)(2,1)S(1)}, bf16[512,128]{1,0:T(8,128)(2,1)S(1)}, u32[]{:S(2)}, u32[]{:S(2)}) collective-permute-start(bf16[512,128]{1,0:T(8,128)(2,1)S(1)} %get-tuple-element.36), channel_id=1, source_target_pairs={{0,48},{8,56},{16,64},{24,72},{32,80},{40,88},{48,96},{56,104},{64... | collective-permute-start | bytes 393224 | tf_op jit(solution)/shard_map/ppermute | solution.py:117
  126.9 2.6 %collective-permute-start.26 = (bf16[512,128]{1,0:T(8,128)(2,1)S(1)}, bf16[512,128]{1,0:T(8,128)(2,1)S(1)}, u32[]{:S(2)}, u32[]{:S(2)}) collective-permute-start(bf16[512,128]{1,0:T(8,128)(2,1)S(1)} %get-tuple-element.35), channel_id=1, source_target_pairs={{0,64},{8,72},{16,80},{24,88},{32,96},{40,104},{48,112},{56,120},{... | collective-permute-start | bytes 393224 | tf_op jit(solution)/shard_map/ppermute | solution.py:117
  130.9 2.9 %collective-permute-start.28 = (bf16[512,128]{1,0:T(8,128)(2,1)S(1)}, bf16[512,128]{1,0:T(8,128)(2,1)S(1)}, u32[]{:S(2)}, u32[]{:S(2)}) collective-permute-start(bf16[512,128]{1,0:T(8,128)(2,1)S(1)} %get-tuple-element.33), channel_id=1, source_target_pairs={{0,96},{8,104},{16,112},{24,120},{32,0},{40,8},{48,16},{56,24},{64... | collective-permute-start | bytes 393224 | tf_op jit(solution)/shard_map/ppermute | solution.py:117
  133.8 6.9 %collective-permute-done.25 = bf16[512,128]{1,0:T(8,128)(2,1)S(1)} collective-permute-done((bf16[512,128]{1,0:T(8,128)(2,1)S(1)}, bf16[512,128]{1,0:T(8,128)(2,1)S(1)}, u32[]{:S(2)}, u32[]{:S(2)}) %collective-permute-start.25) | collective-permute-done | bytes 131104 | tf_op jit(solution)/shard_map/ppermute | solution.py:117
  140.8 3.8 %collective-permute-done.26 = bf16[512,128]{1,0:T(8,128)(2,1)S(1)} collective-permute-done((bf16[512,128]{1,0:T(8,128)(2,1)S(1)}, bf16[512,128]{1,0:T(8,128)(2,1)S(1)}, u32[]{:S(2)}, u32[]{:S(2)}) %collective-permute-start.26) | collective-permute-done | bytes 131104 | tf_op jit(solution)/shard_map/ppermute | solution.py:117
  144.7 7.3 %collective-permute-done.28 = bf16[512,128]{1,0:T(8,128)(2,1)S(1)} collective-permute-done((bf16[512,128]{1,0:T(8,128)(2,1)S(1)}, bf16[512,128]{1,0:T(8,128)(2,1)S(1)}, u32[]{:S(2)}, u32[]{:S(2)}) %collective-permute-start.28) | collective-permute-done | bytes 131104 | tf_op jit(solution)/shard_map/ppermute | solution.py:117
  (131 shorter events, 47.7 us)
Async XLA Ops:
  11.5 21.0 %collective-permute-start = (bf16[2,264,128]{2,1,0:T(8,128)(2,1)}, bf16[2,264,128]{2,1,0:T(8,128)(2,1)}, u32[]{:S(2)}, u32[]{:S(2)}) collective-permute-start(bf16[2,264,128]{2,1,0:T(8,128)(2,1)} %get-tuple-element.30), channel_id=1, source_target_pairs={{0,1},{1,2},{2,3},{3,4},{4,5},{5,6},{6,7},{7,0},{8,9},{9,10},{10,1... | collective-permute-start | bytes 405512 | tf_op jit(solution)/shard_map/ppermute | solution.py:102
  13.6 22.8 %collective-permute-start.1 = (bf16[2,264,128]{2,1,0:T(8,128)(2,1)}, bf16[2,264,128]{2,1,0:T(8,128)(2,1)}, u32[]{:S(2)}, u32[]{:S(2)}) collective-permute-start(bf16[2,264,128]{2,1,0:T(8,128)(2,1)} %get-tuple-element.29), channel_id=1, source_target_pairs={{0,2},{1,3},{2,4},{3,5},{4,6},{5,7},{6,0},{7,1},{8,10},{9,11},{10,... | collective-permute-start | bytes 405512 | tf_op jit(solution)/shard_map/ppermute | solution.py:102
  16.0 22.4 %collective-permute-start.2 = (bf16[2,264,128]{2,1,0:T(8,128)(2,1)}, bf16[2,264,128]{2,1,0:T(8,128)(2,1)}, u32[]{:S(2)}, u32[]{:S(2)}) collective-permute-start(bf16[2,264,128]{2,1,0:T(8,128)(2,1)} %get-tuple-element.28), channel_id=1, source_target_pairs={{0,3},{1,4},{2,5},{3,6},{4,7},{5,0},{6,1},{7,2},{8,11},{9,12},{10,... | collective-permute-start | bytes 405512 | tf_op jit(solution)/shard_map/ppermute | solution.py:102
  18.9 36.3 %collective-permute-start.3 = (bf16[2,264,128]{2,1,0:T(8,128)(2,1)}, bf16[2,264,128]{2,1,0:T(8,128)(2,1)}, u32[]{:S(2)}, u32[]{:S(2)}) collective-permute-start(bf16[2,264,128]{2,1,0:T(8,128)(2,1)} %get-tuple-element.27), channel_id=1, source_target_pairs={{0,4},{1,5},{2,6},{3,7},{4,0},{5,1},{6,2},{7,3},{8,12},{9,13},{10,... | collective-permute-start | bytes 405512 | tf_op jit(solution)/shard_map/ppermute | solution.py:102
  20.4 35.8 %collective-permute-start.4 = (bf16[2,264,128]{2,1,0:T(8,128)(2,1)}, bf16[2,264,128]{2,1,0:T(8,128)(2,1)}, u32[]{:S(2)}, u32[]{:S(2)}) collective-permute-start(bf16[2,264,128]{2,1,0:T(8,128)(2,1)} %get-tuple-element.26), channel_id=1, source_target_pairs={{0,5},{1,6},{2,7},{3,0},{4,1},{5,2},{6,3},{7,4},{8,13},{9,14},{10,... | collective-permute-start | bytes 405512 | tf_op jit(solution)/shard_map/ppermute | solution.py:102
  32.5 24.6 %collective-permute-start.5 = (bf16[2,264,128]{2,1,0:T(8,128)(2,1)S(1)}, bf16[2,264,128]{2,1,0:T(8,128)(2,1)S(1)}, u32[]{:S(2)}, u32[]{:S(2)}) collective-permute-start(bf16[2,264,128]{2,1,0:T(8,128)(2,1)S(1)} %get-tuple-element.25), channel_id=1, source_target_pairs={{0,6},{1,7},{2,0},{3,1},{4,2},{5,3},{6,4},{7,5},{8,14},{9,15},{10,... | collective-permute-start | bytes 405512 | tf_op jit(solution)/shard_map/ppermute | solution.py:102
  36.4 20.8 %collective-permute-start.6 = (bf16[2,264,128]{2,1,0:T(8,128)(2,1)S(1)}, bf16[2,264,128]{2,1,0:T(8,128)(2,1)S(1)}, u32[]{:S(2)}, u32[]{:S(2)}) collective-permute-start(bf16[2,264,128]{2,1,0:T(8,128)(2,1)S(1)} %get-tuple-element.24), channel_id=1, source_target_pairs={{0,7},{1,0},{2,1},{3,2},{4,3},{5,4},{6,5},{7,6},{8,15},{9,8},{10,9... | collective-permute-start | bytes 405512 | tf_op jit(solution)/shard_map/ppermute | solution.py:102
  38.5 42.0 %collective-permute-start.15 = (bf16[8,256,128]{2,1,0:T(8,128)(2,1)}, bf16[8,256,128]{2,1,0:T(8,128)(2,1)}, u32[]{:S(2)}, u32[]{:S(2)}) collective-permute-start(bf16[8,256,128]{2,1,0:T(8,128)(2,1)} %dynamic-slice_bitcast_fusion.1), channel_id=1, source_target_pairs={{0,8},{8,0},{16,24},{24,16},{32,40},{40,32},{48,56},{56,48},{64,72... | collective-permute-start | bytes 1572872 | tf_op jit(solution)/shard_map/ppermute | solution.py:89
  60.4 19.2 %collective-permute-start.9 = (bf16[2,264,128]{2,1,0:T(8,128)(2,1)}, bf16[2,264,128]{2,1,0:T(8,128)(2,1)S(1)}, u32[]{:S(2)}, u32[]{:S(2)}) collective-permute-start(bf16[2,264,128]{2,1,0:T(8,128)(2,1)} %get-tuple-element.20), channel_id=1, source_target_pairs={{0,48},{8,56},{16,64},{24,72},{32,80},{40,88},{48,96},{56,104},{64... | collective-permute-start | bytes 405512 | tf_op jit(solution)/shard_map/ppermute | solution.py:117
  62.9 17.6 %collective-permute-start.10 = (bf16[2,264,128]{2,1,0:T(8,128)(2,1)}, bf16[2,264,128]{2,1,0:T(8,128)(2,1)S(1)}, u32[]{:S(2)}, u32[]{:S(2)}) collective-permute-start(bf16[2,264,128]{2,1,0:T(8,128)(2,1)} %get-tuple-element.19), channel_id=1, source_target_pairs={{0,64},{8,72},{16,80},{24,88},{32,96},{40,104},{48,112},{56,120},{... | collective-permute-start | bytes 405512 | tf_op jit(solution)/shard_map/ppermute | solution.py:117
  65.9 14.5 %collective-permute-start.11 = (bf16[2,264,128]{2,1,0:T(8,128)(2,1)}, bf16[2,264,128]{2,1,0:T(8,128)(2,1)S(1)}, u32[]{:S(2)}, u32[]{:S(2)}) collective-permute-start(bf16[2,264,128]{2,1,0:T(8,128)(2,1)} %get-tuple-element.18), channel_id=1, source_target_pairs={{0,80},{8,88},{16,96},{24,104},{32,112},{40,120},{48,0},{56,8},{64... | collective-permute-start | bytes 405512 | tf_op jit(solution)/shard_map/ppermute | solution.py:117
  68.7 19.3 %collective-permute-start.12 = (bf16[2,264,128]{2,1,0:T(8,128)(2,1)S(1)}, bf16[2,264,128]{2,1,0:T(8,128)(2,1)S(1)}, u32[]{:S(2)}, u32[]{:S(2)}) collective-permute-start(bf16[2,264,128]{2,1,0:T(8,128)(2,1)S(1)} %get-tuple-element.17), channel_id=1, source_target_pairs={{0,96},{8,104},{16,112},{24,120},{32,0},{40,8},{48,16},{56,24},{64... | collective-permute-start | bytes 405512 | tf_op jit(solution)/shard_map/ppermute | solution.py:117
  79.6 41.0 %collective-permute-start.13 = (bf16[2,264,128]{2,1,0:T(8,128)(2,1)S(1)}, bf16[2,264,128]{2,1,0:T(8,128)(2,1)S(1)}, u32[]{:S(2)}, u32[]{:S(2)}) collective-permute-start(bf16[2,264,128]{2,1,0:T(8,128)(2,1)S(1)} %get-tuple-element.16), channel_id=1, source_target_pairs={{0,112},{8,120},{16,0},{24,8},{32,16},{40,24},{48,32},{56,40},{64,... | collective-permute-start | bytes 405512 | tf_op jit(solution)/shard_map/ppermute | solution.py:117
  81.9 13.8 %collective-permute-start.16 = (bf16[512,128]{1,0:T(8,128)(2,1)S(1)}, bf16[512,128]{1,0:T(8,128)(2,1)S(1)}, u32[]{:S(2)}, u32[]{:S(2)}) collective-permute-start(bf16[512,128]{1,0:T(8,128)(2,1)S(1)} %get-tuple-element.46), channel_id=1, source_target_pairs={{0,1},{1,2},{2,3},{3,4},{4,5},{5,6},{6,7},{7,0},{8,9},{9,10},{10,1... | collective-permute-start | bytes 393224 | tf_op jit(solution)/shard_map/ppermute | solution.py:102
  89.8 17.8 %collective-permute-start.18 = (bf16[512,128]{1,0:T(8,128)(2,1)S(1)}, bf16[512,128]{1,0:T(8,128)(2,1)S(1)}, u32[]{:S(2)}, u32[]{:S(2)}) collective-permute-start(bf16[512,128]{1,0:T(8,128)(2,1)S(1)} %get-tuple-element.44), channel_id=1, source_target_pairs={{0,3},{1,4},{2,5},{3,6},{4,7},{5,0},{6,1},{7,2},{8,11},{9,12},{10,... | collective-permute-start | bytes 393224 | tf_op jit(solution)/shard_map/ppermute | solution.py:102
  92.9 16.5 %collective-permute-start.19 = (bf16[512,128]{1,0:T(8,128)(2,1)S(1)}, bf16[512,128]{1,0:T(8,128)(2,1)S(1)}, u32[]{:S(2)}, u32[]{:S(2)}) collective-permute-start(bf16[512,128]{1,0:T(8,128)(2,1)S(1)} %get-tuple-element.43), channel_id=1, source_target_pairs={{0,4},{1,5},{2,6},{3,7},{4,0},{5,1},{6,2},{7,3},{8,12},{9,13},{10,... | collective-permute-start | bytes 393224 | tf_op jit(solution)/shard_map/ppermute | solution.py:102
  95.7 15.5 %collective-permute-start.20 = (bf16[512,128]{1,0:T(8,128)(2,1)S(1)}, bf16[512,128]{1,0:T(8,128)(2,1)S(1)}, u32[]{:S(2)}, u32[]{:S(2)}) collective-permute-start(bf16[512,128]{1,0:T(8,128)(2,1)S(1)} %get-tuple-element.42), channel_id=1, source_target_pairs={{0,5},{1,6},{2,7},{3,0},{4,1},{5,2},{6,3},{7,4},{8,13},{9,14},{10,... | collective-permute-start | bytes 393224 | tf_op jit(solution)/shard_map/ppermute | solution.py:102
  97.6 20.4 %collective-permute-start.21 = (bf16[512,128]{1,0:T(8,128)(2,1)S(1)}, bf16[512,128]{1,0:T(8,128)(2,1)S(1)}, u32[]{:S(2)}, u32[]{:S(2)}) collective-permute-start(bf16[512,128]{1,0:T(8,128)(2,1)S(1)} %get-tuple-element.41), channel_id=1, source_target_pairs={{0,6},{1,7},{2,0},{3,1},{4,2},{5,3},{6,4},{7,5},{8,14},{9,15},{10,... | collective-permute-start | bytes 393224 | tf_op jit(solution)/shard_map/ppermute | solution.py:102
  120.7 32.4 %collective-permute-start.14 = (bf16[8,264,128]{2,1,0:T(8,128)(2,1)S(1)}, bf16[8,264,128]{2,1,0:T(8,128)(2,1)S(1)}, u32[]{:S(2)}, u32[]{:S(2)}) collective-permute-start(bf16[8,264,128]{2,1,0:T(8,128)(2,1)S(1)} %dynamic-slice_bitcast_fusion), channel_id=1, source_target_pairs={{0,8},{8,0},{16,24},{24,16},{32,40},{40,32},{48,56},{56,48},{64,72... | collective-permute-start | bytes 1622024 | tf_op jit(solution)/shard_map/ppermute | solution.py:89
  123.6 17.1 %collective-permute-start.25 = (bf16[512,128]{1,0:T(8,128)(2,1)S(1)}, bf16[512,128]{1,0:T(8,128)(2,1)S(1)}, u32[]{:S(2)}, u32[]{:S(2)}) collective-permute-start(bf16[512,128]{1,0:T(8,128)(2,1)S(1)} %get-tuple-element.36), channel_id=1, source_target_pairs={{0,48},{8,56},{16,64},{24,72},{32,80},{40,88},{48,96},{56,104},{64... | collective-permute-start | bytes 393224 | tf_op jit(solution)/shard_map/ppermute | solution.py:117
  126.9 17.7 %collective-permute-start.26 = (bf16[512,128]{1,0:T(8,128)(2,1)S(1)}, bf16[512,128]{1,0:T(8,128)(2,1)S(1)}, u32[]{:S(2)}, u32[]{:S(2)}) collective-permute-start(bf16[512,128]{1,0:T(8,128)(2,1)S(1)} %get-tuple-element.35), channel_id=1, source_target_pairs={{0,64},{8,72},{16,80},{24,88},{32,96},{40,104},{48,112},{56,120},{... | collective-permute-start | bytes 393224 | tf_op jit(solution)/shard_map/ppermute | solution.py:117
  129.5 15.1 %collective-permute-start.27 = (bf16[512,128]{1,0:T(8,128)(2,1)S(1)}, bf16[512,128]{1,0:T(8,128)(2,1)S(1)}, u32[]{:S(2)}, u32[]{:S(2)}) collective-permute-start(bf16[512,128]{1,0:T(8,128)(2,1)S(1)} %get-tuple-element.34), channel_id=1, source_target_pairs={{0,80},{8,88},{16,96},{24,104},{32,112},{40,120},{48,0},{56,8},{64... | collective-permute-start | bytes 393224 | tf_op jit(solution)/shard_map/ppermute | solution.py:117
  130.9 21.1 %collective-permute-start.28 = (bf16[512,128]{1,0:T(8,128)(2,1)S(1)}, bf16[512,128]{1,0:T(8,128)(2,1)S(1)}, u32[]{:S(2)}, u32[]{:S(2)}) collective-permute-start(bf16[512,128]{1,0:T(8,128)(2,1)S(1)} %get-tuple-element.33), channel_id=1, source_target_pairs={{0,96},{8,104},{16,112},{24,120},{32,0},{40,8},{48,16},{56,24},{64... | collective-permute-start | bytes 393224 | tf_op jit(solution)/shard_map/ppermute | solution.py:117
  140.7 12.3 %collective-permute-start.29 = (bf16[512,128]{1,0:T(8,128)(2,1)S(1)}, bf16[512,128]{1,0:T(8,128)(2,1)S(1)}, u32[]{:S(2)}, u32[]{:S(2)}) collective-permute-start(bf16[512,128]{1,0:T(8,128)(2,1)S(1)} %get-tuple-element.32), channel_id=1, source_target_pairs={{0,112},{8,120},{16,0},{24,8},{32,16},{40,24},{48,32},{56,40},{64,... | collective-permute-start | bytes 393224 | tf_op jit(solution)/shard_map/ppermute | solution.py:117
  (18 other events, 135.1 us)

commit v4 on v3

--- a/solution.py
+++ b/solution.py
@@ -1,6 +1,8 @@
 import jax
 import jax.numpy as jnp
 from jax import lax
+from jax.experimental import pallas as pl
+from jax.experimental.pallas import tpu as pltpu
 from jax.sharding import PartitionSpec as P
 
 
@@ -12,25 +14,155 @@
 epsilon = 1e-06
 
 
-def normalise(token_rows, norm_gain):
-    widened = token_rows.astype(jnp.float32)
-    return (
-        widened
-        * lax.rsqrt(jnp.mean(widened * widened, axis=-1, keepdims=True) + epsilon)
-        * norm_gain.astype(jnp.float32)
-    ).astype(jnp.bfloat16)
-
-
-def project(normed, weight):
-    matrix = weight.reshape(weight.shape[0], HEADS, DK)
-    return jnp.einsum(
-        "apd,dhk->hapk", normed, matrix, preferred_element_type=jnp.float32
-    ).astype(jnp.bfloat16)
-
-
-def gate(normed, weight):
-    linear = jnp.einsum("apd,dh->hap", normed, weight, preferred_element_type=jnp.float32)
-    return linear.astype(jnp.bfloat16)
+def project_kernel(place, x_hbm, gain, in_hbm, forget_hbm, key_hbm, value_hbm, *rest):
+    *keys, kept, given, x, gate_weight, weight, normed, gates, x_sem, gate_sem, sem = rest
+    step = pl.program_id(0)
+    seqs, rows, lane = keys[0].shape[0], kept.shape[1], kept.shape[2]
+    lines = rows // lane
+    parts = x_sem.shape[0]
+    part = x.shape[0] // parts
+    chunk = 64
+
+    def column(kind, shift):
+        head = lax.rem(place[0] + shift, HEADS)
+        source = (key_hbm, value_hbm)[kind].at[:, pl.ds(pl.multiple_of(head * lane, lane), lane)]
+        half = shift % 2
+        target = weight.at[kind, shift // 2, :, half * lane : (half + 1) * lane]
+        return pltpu.make_async_copy(source, target, sem.at[kind, shift])
+
+    def arrive(kind):
+        for half in range(2):
+            pltpu.make_async_copy(
+                key_hbm.at[:, :lane],
+                weight.at[kind, step, :, half * lane : (half + 1) * lane],
+                sem.at[kind, 2 * step + half],
+            ).wait()
+
+    @pl.when(step == 0)
+    def _():
+        pieces = [
+            pltpu.make_async_copy(
+                x_hbm.at[n * part : (n + 1) * part], x.at[n * part : (n + 1) * part], x_sem.at[n]
+            )
+            for n in range(parts)
+        ]
+        gate_copies = [
+            pltpu.make_async_copy(ref, gate_weight.at[n], gate_sem.at[n])
+            for n, ref in enumerate((in_hbm, forget_hbm))
+        ]
+        for copy in pieces + gate_copies:
+            copy.start()
+        for shift in range(0, HEADS, 2):
+            for kind in range(2):
+                column(kind, shift).start()
+                column(kind, shift + 1).start()
+        scale = gain[...].astype(jnp.float32)
+        for n in range(parts):
+            pieces[n].wait()
+
+            @pl.loop(0, part // chunk)
+            def _(m):
+                at = pl.ds(pl.multiple_of(n * part + m * chunk, chunk), chunk)
+                wide = x[at, :].astype(jnp.float32)
+                mean = jnp.mean(wide * wide, axis=-1, keepdims=True)
+                normed[at, :] = (wide * lax.rsqrt(mean + epsilon) * scale).astype(jnp.bfloat16)
+
+        for n in range(2):
+            gate_copies[n].wait()
+        both = jnp.concatenate([gate_weight[0], gate_weight[1]], axis=0)
+        gates[...] = lax.dot_general(
+            both, normed[...], (((1,), (1,)), ((), ())), preferred_element_type=jnp.float32
+        )
+
+    def dot(kind):
+        arrive(kind)
+        out = jnp.dot(normed[...], weight[kind, step], preferred_element_type=jnp.float32)
+        return out.astype(jnp.bfloat16)
+
+    key_rows = dot(0)
+    tails = []
+    for j in range(2):
+        head = lax.rem(place[0] + 2 * step + j, HEADS)
+        pair = [gates[pl.ds(head + HEADS * g, 1), :] for g in range(2)]
+        for a in range(seqs):
+            cut = [
+                g[:, (a * lines + n) * lane : (a * lines + n + 1) * lane]
+                for g in pair
+                for n in range(lines)
+            ]
+            spare = jnp.zeros((8 - len(cut), lane), jnp.float32)
+            tails.append(jnp.concatenate(cut + [spare], axis=0).astype(jnp.bfloat16))
+    for c in range(HEADS // 2):
+
+        @pl.when(step == c)
+        def _():
+            for j in range(2):
+                for a in range(seqs):
+                    block = key_rows[a * rows : (a + 1) * rows, j * lane : (j + 1) * lane]
+                    keys[2 * c + j][a, :rows, :] = block
+                    keys[2 * c + j][a, rows:, :] = tails[j * seqs + a]
+
+    value_rows = dot(1)
+    first = place[1] == 0
+    for j in range(2):
+        one = value_rows[:rows, j * lane : (j + 1) * lane]
+        two = value_rows[rows:, j * lane : (j + 1) * lane]
+        kept[j] = jnp.where(first, one, two)
+        given[j] = jnp.where(first, two, one)
+
+
+def project(place, layer_input, norm_gain, key_weight, value_weight, gate_in, gate_forget):
+    seqs, rows, width = layer_input.shape
+    tokens = seqs * rows
+
+    def whole(*shape):
+        return pl.BlockSpec(shape, lambda i, p: (0,) * len(shape))
+
+    def halves():
+        return pl.BlockSpec((2, rows, DK), lambda i, p: (i, 0, 0))
+
+    hbm = pl.BlockSpec(memory_space=pltpu.MemorySpace.HBM)
+    key_shape = (seqs, rows + 8, DK)
+    value_shape = (HEADS, rows, DK)
+    *keys, kept, given = pl.pallas_call(
+        project_kernel,
+        grid_spec=pltpu.PrefetchScalarGridSpec(
+            num_scalar_prefetch=1,
+            grid=(HEADS // 2,),
+            in_specs=[hbm, whole(1, width), hbm, hbm, hbm, hbm],
+            out_specs=[whole(*key_shape)] * HEADS + [halves(), halves()],
+            scratch_shapes=[
+                pltpu.VMEM((tokens, width), jnp.bfloat16),
+                pltpu.VMEM((2, HEADS, width), jnp.bfloat16),
+                pltpu.VMEM((2, HEADS // 2, width, 2 * DK), jnp.bfloat16),
+                pltpu.VMEM((tokens, width), jnp.bfloat16),
+                pltpu.VMEM((2 * HEADS, tokens), jnp.float32),
+                pltpu.SemaphoreType.DMA((4,)),
+                pltpu.SemaphoreType.DMA((2,)),
+                pltpu.SemaphoreType.DMA((2, HEADS)),
+            ],
+        ),
+        out_shape=[jax.ShapeDtypeStruct(key_shape, jnp.bfloat16)] * HEADS
+        + [jax.ShapeDtypeStruct(value_shape, jnp.bfloat16)] * 2,
+        compiler_params=pltpu.CompilerParams(
+            dimension_semantics=("arbitrary",), vmem_limit_bytes=60 * 1024 * 1024
+        ),
+        cost_estimate=pl.CostEstimate(
+            flops=4 * tokens * width * HEADS * DK,
+            bytes_accessed=2 * (tokens * width + 2 * width * HEADS * DK + 2 * tokens * HEADS * DK),
+            transcendentals=tokens,
+        ),
+        name="project",
+    )(
+        place,
+        layer_input.reshape(tokens, width),
+        norm_gain.reshape(1, width),
+        gate_in.T,
+        gate_forget.T,
+        key_weight,
+        value_weight,
+    )
+    return keys, kept, given
 
 
 def convolve(key_linear, tap_weight):
@@ -80,27 +212,19 @@
     return (weight_cache, first_read)
 
 
-def trade(block):
-    pair = block.shape[1]
-    core = lax.axis_index("sp") % pair
-    own = lax.dynamic_index_in_dim(block, core, 1, keepdims=False)
-    other = lax.dynamic_index_in_dim(block, 1 - core, 1, keepdims=False)
+def trade(own, other):
+    first = lax.axis_index("sp") % 2 == 0
     route = [(i, i ^ 1) for i in range(lax.axis_size("sp"))]
     got = lax.ppermute(other, "sp", route)
-    first = core == 0
     return jnp.stack([jnp.where(first, own, got), jnp.where(first, got, own)], axis=1)
 
 
-def rotate(block):
+def rotate(blocks):
     ring = lax.axis_size("tp")
-    here = lax.axis_index("tp")
-    got = []
-    for step in range(ring):
-        mine = lax.dynamic_index_in_dim(block, (here + step) % ring, 0, keepdims=False)
-        if step:
-            route = [(i, (i + step) % ring) for i in range(ring)]
-            mine = lax.ppermute(mine, "tp", route)
-        got.append(mine)
+    got = list(blocks[:1])
+    for step in range(1, ring):
+        route = [(i, (i + step) % ring) for i in range(ring)]
+        got.append(lax.ppermute(blocks[step], "tp", route))
     return jnp.stack(got)
 
 
@@ -137,18 +261,23 @@
 ):
     seqs, rows, _ = layer_input.shape
     lines = rows // DK
-    normed = normalise(layer_input, norm_gain)
-    gates = jnp.stack(
-        [gate(normed, input_gate_weight), gate(normed, forget_gate_weight)], axis=2
-    ).reshape(HEADS, seqs, 2 * lines, DK)
-    gates = jnp.pad(gates, ((0, 0), (0, 0), (0, 8 - 2 * lines), (0, 0)))
-    key_block = jnp.concatenate([project(normed, key_weight), gates], axis=2)
-    normed, key_block = lax.optimization_barrier((normed, key_block))
-    value_block = project(normed, value_weight)
-    value_block = trade(value_block).reshape(HEADS, seqs * rows, DK)
-    mine = trade(spread(rotate(key_block)))
-    mine = mine.reshape((-1,) + mine.shape[2:])
-    values = spread(rotate(value_block))
+    core = lax.axis_index("sp") % 2
+    place = jnp.stack([lax.axis_index("tp"), core]).astype(jnp.int32)
+    key_blocks, kept, given = project(
+        place,
+        layer_input,
+        norm_gain,
+        key_weight,
+        value_weight,
+        input_gate_weight,
+        forget_gate_weight,
+    )
+    value_blocks = trade(kept, given).reshape(HEADS, seqs * rows, DK)
+    mine = spread(rotate(key_blocks))
+    own = lax.dynamic_index_in_dim(mine, core, 1, keepdims=False)
+    other = lax.dynamic_index_in_dim(mine, 1 - core, 1, keepdims=False)
+    mine = trade(own, other).reshape((-1,) + own.shape[1:])
+    values = spread(rotate(value_blocks))
     length = mine.shape[0] * rows
     key_linear = mine[:, :rows].reshape(length, DK)
     values = values.reshape(1, 1, length, DK)

time: 166 us -> 169 us (1.018); the launches traced: 164 us -> 169 us
  Pallas kernels: 0 us -> 17.6 us
  matrix products: 14.2 us -> 2.76 us
  starting transfers between devices: 72.7 us -> 82.7 us
  local copies, waits for them, and re-layouts: 11.3 us -> 5.03 us
  other arithmetic: 11 us -> 6.41 us
    pallas_call x0 -> x1, Pallas kernels: none -> 17.6 us  [project(): pl.pallas_call(project_kernel, grid_spec=pltpu.PrefetchScalarGridSpec(num...]
    dot_general x4 -> x0, matrix products: 11.4 us -> none  [the longest x2 10.1 us: project(): jnp.einsum('apd,dhk->hapk', normed, matrix, preferred_element_type=jnp.fl...]
    ppermute x14, starting transfers between devices: 22 us -> 28.5 us  [spread(): mine = lax.ppermute(mine, 'sp', route)]
    unnamed x36 -> x32, local copies, waits for them, and re-layouts: 5.45 us -> 1.83 us
    squeeze x4 -> x1, local copies, waits for them, and re-layouts: 3.05 us -> 0.05 us  [layer(): other = lax.dynamic_index_in_dim(mine, 1 - core, 1, keepdims=False)]
    ppermute x14, starting transfers between devices: 32.7 us -> 35.1 us  [rotate(): got.append(lax.ppermute(blocks[step], 'tp', route))]
    ppermute x14, waiting for transfers between devices: 17.5 us -> 15.4 us  [rotate(): got.append(lax.ppermute(blocks[step], 'tp', route))]
    reduce_sum x1 -> x0, other arithmetic: 2.07 us -> none  [normalise(): jnp.mean(widened * widened, axis=-1, keepdims=True) + epsilon]
  transfers between devices with their start and end apart: 30 -> 30, of which waited for: 12 -> 11; matrix products, arithmetic and copies ran while one was open for 11% -> 2% of each run, Pallas kernels for 0% -> 0%
where the time goes in v4:
time: 169 us
  starting transfers between devices  82.7 us (49%)
  waiting for transfers between devices  49.3 us (29%)
  Pallas kernels  17.6 us (10%)
  other arithmetic  6.41 us (4%)
  local copies, waits for them, and re-layouts  5.03 us (3%)
  between operations  5.03 us (3%)
  matrix products  2.76 us (2%)
    ppermute x14, starting transfers between devices, rotate(): got.append(lax.ppermute(blocks[step], 'tp', route))  35.1 us
    ppermute x14, waiting for transfers between devices, spread(): mine = lax.ppermute(mine, 'sp', route)  33.9 us
    ppermute x14, starting transfers between devices, spread(): mine = lax.ppermute(mine, 'sp', route)  28.5 us
    ppermute x2, starting transfers between devices, trade(): got = lax.ppermute(other, 'sp', route)  19.1 us
    pallas_call x1, Pallas kernels, project(): pl.pallas_call(project_kernel, grid_spec=pltpu.PrefetchScalarGridSpec(num...  17.6 us
    ppermute x14, waiting for transfers between devices, rotate(): got.append(lax.ppermute(blocks[step], 'tp', route))  15.4 us
  transfers between devices with their start and end apart: 30, of which 11 were waited for; matrix products, arithmetic and copies ran while one was open for 2% of the time, Pallas kernels for 0%

profile of v4, /device:TPU:513, one launch (start us, length us, event | category | flops | bytes accessed | tf_op | source)
XLA Modules:
  0.0 168.9 jit_solution(16875520155568866989)
XLA Ops:
  2.6 17.6 %project.1 = (bf16[2,264,128]{2,1,0:T(8,128)(2,1)}, bf16[2,264,128]{2,1,0:T(8,128)(2,1)}, bf16[2,264,128]{2,1,0:T(8,128)(2,1)}, bf16[2,264,128]{2,1,0:T(8,128)(2...) custom-call(s32[2]{0:T(128)} %pad_add_fusion.place, ...), custom_call_target="tpu_custom_call" | custom-call | flops 4294967296 | bytes 12582912 | tf_op jit(solution)/shard_map/project/pallas_call | solution.py:127
  20.2 2.3 %collective-permute-start = (bf16[2,264,128]{2,1,0:T(8,128)(2,1)}, bf16[2,264,128]{2,1,0:T(8,128)(2,1)S(1)}, u32[]{:S(2)}, u32[]{:S(2)}) collective-permute-start(bf16[2,264,128]{2,1,0:T(8,128)(2,1)} %get-tuple-element.15), channel_id=1, source_target_pairs={{0,1},{1,2},{2,3},{3,4},{4,5},{5,6},{6,7},{7,0},{8,9},{9,10},{10,1... | collective-permute-start | bytes 405512 | tf_op jit(solution)/shard_map/ppermute | solution.py:227
  22.5 2.4 %collective-permute-start.1 = (bf16[2,264,128]{2,1,0:T(8,128)(2,1)}, bf16[2,264,128]{2,1,0:T(8,128)(2,1)S(1)}, u32[]{:S(2)}, u32[]{:S(2)}) collective-permute-start(bf16[2,264,128]{2,1,0:T(8,128)(2,1)} %get-tuple-element.16), channel_id=1, source_target_pairs={{0,2},{1,3},{2,4},{3,5},{4,6},{5,7},{6,0},{7,1},{8,10},{9,11},{10,... | collective-permute-start | bytes 405512 | tf_op jit(solution)/shard_map/ppermute | solution.py:227
  24.9 2.9 %collective-permute-start.2 = (bf16[2,264,128]{2,1,0:T(8,128)(2,1)}, bf16[2,264,128]{2,1,0:T(8,128)(2,1)S(1)}, u32[]{:S(2)}, u32[]{:S(2)}) collective-permute-start(bf16[2,264,128]{2,1,0:T(8,128)(2,1)} %get-tuple-element.17), channel_id=1, source_target_pairs={{0,3},{1,4},{2,5},{3,6},{4,7},{5,0},{6,1},{7,2},{8,11},{9,12},{10,... | collective-permute-start | bytes 405512 | tf_op jit(solution)/shard_map/ppermute | solution.py:227
  29.2 3.2 %collective-permute-start.4 = (bf16[2,264,128]{2,1,0:T(8,128)(2,1)}, bf16[2,264,128]{2,1,0:T(8,128)(2,1)S(1)}, u32[]{:S(2)}, u32[]{:S(2)}) collective-permute-start(bf16[2,264,128]{2,1,0:T(8,128)(2,1)} %get-tuple-element.19), channel_id=1, source_target_pairs={{0,5},{1,6},{2,7},{3,0},{4,1},{5,2},{6,3},{7,4},{8,13},{9,14},{10,... | collective-permute-start | bytes 405512 | tf_op jit(solution)/shard_map/ppermute | solution.py:227
  34.5 3.1 %collective-permute-start.5 = (bf16[2,264,128]{2,1,0:T(8,128)(2,1)}, bf16[2,264,128]{2,1,0:T(8,128)(2,1)S(1)}, u32[]{:S(2)}, u32[]{:S(2)}) collective-permute-start(bf16[2,264,128]{2,1,0:T(8,128)(2,1)} %get-tuple-element.20), channel_id=1, source_target_pairs={{0,6},{1,7},{2,0},{3,1},{4,2},{5,3},{6,4},{7,5},{8,14},{9,15},{10,... | collective-permute-start | bytes 405512 | tf_op jit(solution)/shard_map/ppermute | solution.py:227
  39.0 18.1 %collective-permute-start.15 = (bf16[8,256,128]{2,1,0:T(8,128)(2,1)}, bf16[8,256,128]{2,1,0:T(8,128)(2,1)S(1)}, u32[]{:S(2)}, u32[]{:S(2)}) collective-permute-start(bf16[8,256,128]{2,1,0:T(8,128)(2,1)} %get-tuple-element.23), channel_id=1, source_target_pairs={{0,8},{8,0},{16,24},{24,16},{32,40},{40,32},{48,56},{56,48},{64,72... | collective-permute-start | bytes 1572872 | tf_op jit(solution)/shard_map/ppermute | solution.py:218
  59.8 4.0 %collective-permute-start.8 = (bf16[2,264,128]{2,1,0:T(8,128)(2,1)S(1)}, bf16[2,264,128]{2,1,0:T(8,128)(2,1)S(1)}, u32[]{:S(2)}, u32[]{:S(2)}) collective-permute-start(bf16[2,264,128]{2,1,0:T(8,128)(2,1)S(1)} %get-tuple-element.35), channel_id=1, source_target_pairs={{0,32},{8,40},{16,48},{24,56},{32,64},{40,72},{48,80},{56,88},{64,... | collective-permute-start | bytes 405512 | tf_op jit(solution)/shard_map/ppermute | solution.py:241
  63.9 6.3 %collective-permute-start.9 = (bf16[2,264,128]{2,1,0:T(8,128)(2,1)S(1)}, bf16[2,264,128]{2,1,0:T(8,128)(2,1)S(1)}, u32[]{:S(2)}, u32[]{:S(2)}) collective-permute-start(bf16[2,264,128]{2,1,0:T(8,128)(2,1)S(1)} %get-tuple-element.34), channel_id=1, source_target_pairs={{0,48},{8,56},{16,64},{24,72},{32,80},{40,88},{48,96},{56,104},{64... | collective-permute-start | bytes 405512 | tf_op jit(solution)/shard_map/ppermute | solution.py:241
  71.5 4.5 %collective-permute-start.11 = (bf16[2,264,128]{2,1,0:T(8,128)(2,1)S(1)}, bf16[2,264,128]{2,1,0:T(8,128)(2,1)S(1)}, u32[]{:S(2)}, u32[]{:S(2)}) collective-permute-start(bf16[2,264,128]{2,1,0:T(8,128)(2,1)S(1)} %get-tuple-element.32), channel_id=1, source_target_pairs={{0,80},{8,88},{16,96},{24,104},{32,112},{40,120},{48,0},{56,8},{64... | collective-permute-start | bytes 405512 | tf_op jit(solution)/shard_map/ppermute | solution.py:241
  76.8 11.5 %collective-permute-done.9 = bf16[2,264,128]{2,1,0:T(8,128)(2,1)S(1)} collective-permute-done((bf16[2,264,128]{2,1,0:T(8,128)(2,1)S(1)}, bf16[2,264,128]{2,1,0:T(8,128)(2,1)S(1)}, u32[]{:S(2)}, u32[]{:S(2)}) %collective-permute-start.9) | collective-permute-done | bytes 135200 | tf_op jit(solution)/shard_map/ppermute | solution.py:241
  88.7 2.5 %collective-permute-start.16 = (bf16[512,128]{1,0:T(8,128)(2,1)S(1)}, bf16[512,128]{1,0:T(8,128)(2,1)S(1)}, u32[]{:S(2)}, u32[]{:S(2)}) collective-permute-start(bf16[512,128]{1,0:T(8,128)(2,1)S(1)} %bitcast.194), channel_id=1, source_target_pairs={{0,1},{1,2},{2,3},{3,4},{4,5},{5,6},{6,7},{7,0},{8,9},{9,10},{10,1... | collective-permute-start | bytes 393224 | tf_op jit(solution)/shard_map/ppermute | solution.py:227
  91.2 3.8 %collective-permute-done.12 = bf16[2,264,128]{2,1,0:T(8,128)(2,1)S(1)} collective-permute-done((bf16[2,264,128]{2,1,0:T(8,128)(2,1)S(1)}, bf16[2,264,128]{2,1,0:T(8,128)(2,1)S(1)}, u32[]{:S(2)}, u32[]{:S(2)}) %collective-permute-start.12) | collective-permute-done | bytes 135200 | tf_op jit(solution)/shard_map/ppermute | solution.py:241
  95.0 2.3 %collective-permute-start.17 = (bf16[512,128]{1,0:T(8,128)(2,1)S(1)}, bf16[512,128]{1,0:T(8,128)(2,1)S(1)}, u32[]{:S(2)}, u32[]{:S(2)}) collective-permute-start(bf16[512,128]{1,0:T(8,128)(2,1)S(1)} %bitcast.193), channel_id=1, source_target_pairs={{0,2},{1,3},{2,4},{3,5},{4,6},{5,7},{6,0},{7,1},{8,10},{9,11},{10,... | collective-permute-start | bytes 393224 | tf_op jit(solution)/shard_map/ppermute | solution.py:227
  97.3 2.3 %collective-permute-start.18 = (bf16[512,128]{1,0:T(8,128)(2,1)S(1)}, bf16[512,128]{1,0:T(8,128)(2,1)S(1)}, u32[]{:S(2)}, u32[]{:S(2)}) collective-permute-start(bf16[512,128]{1,0:T(8,128)(2,1)S(1)} %bitcast.192), channel_id=1, source_target_pairs={{0,3},{1,4},{2,5},{3,6},{4,7},{5,0},{6,1},{7,2},{8,11},{9,12},{10,... | collective-permute-start | bytes 393224 | tf_op jit(solution)/shard_map/ppermute | solution.py:227
  99.6 3.6 %collective-permute-start.19 = (bf16[512,128]{1,0:T(8,128)(2,1)S(1)}, bf16[512,128]{1,0:T(8,128)(2,1)S(1)}, u32[]{:S(2)}, u32[]{:S(2)}) collective-permute-start(bf16[512,128]{1,0:T(8,128)(2,1)S(1)} %bitcast.191), channel_id=1, source_target_pairs={{0,4},{1,5},{2,6},{3,7},{4,0},{5,1},{6,2},{7,3},{8,12},{9,13},{10,... | collective-permute-start | bytes 393224 | tf_op jit(solution)/shard_map/ppermute | solution.py:227
  103.5 3.1 %collective-permute-start.21 = (bf16[512,128]{1,0:T(8,128)(2,1)S(1)}, bf16[512,128]{1,0:T(8,128)(2,1)S(1)}, u32[]{:S(2)}, u32[]{:S(2)}) collective-permute-start(bf16[512,128]{1,0:T(8,128)(2,1)S(1)} %bitcast.189), channel_id=1, source_target_pairs={{0,6},{1,7},{2,0},{3,1},{4,2},{5,3},{6,4},{7,5},{8,14},{9,15},{10,... | collective-permute-start | bytes 393224 | tf_op jit(solution)/shard_map/ppermute | solution.py:227
  106.6 2.3 %collective-permute-done.18 = bf16[512,128]{1,0:T(8,128)(2,1)S(1)} collective-permute-done((bf16[512,128]{1,0:T(8,128)(2,1)S(1)}, bf16[512,128]{1,0:T(8,128)(2,1)S(1)}, u32[]{:S(2)}, u32[]{:S(2)}) %collective-permute-start.18) | collective-permute-done | bytes 131104 | tf_op jit(solution)/shard_map/ppermute | solution.py:227
  108.9 4.6 %collective-permute-start.22 = (bf16[512,128]{1,0:T(8,128)(2,1)S(1)}, bf16[512,128]{1,0:T(8,128)(2,1)S(1)}, u32[]{:S(2)}, u32[]{:S(2)}) collective-permute-start(bf16[512,128]{1,0:T(8,128)(2,1)S(1)} %bitcast.188), channel_id=1, source_target_pairs={{0,7},{1,0},{2,1},{3,2},{4,3},{5,4},{6,5},{7,6},{8,15},{9,8},{10,9... | collective-permute-start | bytes 393224 | tf_op jit(solution)/shard_map/ppermute | solution.py:227
  113.5 2.6 %collective-permute-done.19 = bf16[512,128]{1,0:T(8,128)(2,1)S(1)} collective-permute-done((bf16[512,128]{1,0:T(8,128)(2,1)S(1)}, bf16[512,128]{1,0:T(8,128)(2,1)S(1)}, u32[]{:S(2)}, u32[]{:S(2)}) %collective-permute-start.19) | collective-permute-done | bytes 131104 | tf_op jit(solution)/shard_map/ppermute | solution.py:227
  117.0 7.5 %collective-permute-done.21 = bf16[512,128]{1,0:T(8,128)(2,1)S(1)} collective-permute-done((bf16[512,128]{1,0:T(8,128)(2,1)S(1)}, bf16[512,128]{1,0:T(8,128)(2,1)S(1)}, u32[]{:S(2)}, u32[]{:S(2)}) %collective-permute-start.21) | collective-permute-done | bytes 131104 | tf_op jit(solution)/shard_map/ppermute | solution.py:227
  129.1 4.0 %collective-permute-start.25 = (bf16[512,128]{1,0:T(8,128)(2,1)S(1)}, bf16[512,128]{1,0:T(8,128)(2,1)S(1)}, u32[]{:S(2)}, u32[]{:S(2)}) collective-permute-start(bf16[512,128]{1,0:T(8,128)(2,1)S(1)} %get-tuple-element.42), channel_id=1, source_target_pairs={{0,48},{8,56},{16,64},{24,72},{32,80},{40,88},{48,96},{56,104},{64... | collective-permute-start | bytes 393224 | tf_op jit(solution)/shard_map/ppermute | solution.py:241
  139.3 11.2 %collective-permute-done.25 = bf16[512,128]{1,0:T(8,128)(2,1)S(1)} collective-permute-done((bf16[512,128]{1,0:T(8,128)(2,1)S(1)}, bf16[512,128]{1,0:T(8,128)(2,1)S(1)}, u32[]{:S(2)}, u32[]{:S(2)}) %collective-permute-start.25) | collective-permute-done | bytes 131104 | tf_op jit(solution)/shard_map/ppermute | solution.py:241
  150.6 7.0 %collective-permute-done.28 = bf16[512,128]{1,0:T(8,128)(2,1)S(1)} collective-permute-done((bf16[512,128]{1,0:T(8,128)(2,1)S(1)}, bf16[512,128]{1,0:T(8,128)(2,1)S(1)}, u32[]{:S(2)}, u32[]{:S(2)}) %collective-permute-start.28) | collective-permute-done | bytes 131104 | tf_op jit(solution)/shard_map/ppermute | solution.py:241
  (114 shorter events, 31.0 us)
Async XLA Ops:
  20.2 14.2 %collective-permute-start = (bf16[2,264,128]{2,1,0:T(8,128)(2,1)}, bf16[2,264,128]{2,1,0:T(8,128)(2,1)S(1)}, u32[]{:S(2)}, u32[]{:S(2)}) collective-permute-start(bf16[2,264,128]{2,1,0:T(8,128)(2,1)} %get-tuple-element.15), channel_id=1, source_target_pairs={{0,1},{1,2},{2,3},{3,4},{4,5},{5,6},{6,7},{7,0},{8,9},{9,10},{10,1... | collective-permute-start | bytes 405512 | tf_op jit(solution)/shard_map/ppermute | solution.py:227
  22.5 15.1 %collective-permute-start.1 = (bf16[2,264,128]{2,1,0:T(8,128)(2,1)}, bf16[2,264,128]{2,1,0:T(8,128)(2,1)S(1)}, u32[]{:S(2)}, u32[]{:S(2)}) collective-permute-start(bf16[2,264,128]{2,1,0:T(8,128)(2,1)} %get-tuple-element.16), channel_id=1, source_target_pairs={{0,2},{1,3},{2,4},{3,5},{4,6},{5,7},{6,0},{7,1},{8,10},{9,11},{10,... | collective-permute-start | bytes 405512 | tf_op jit(solution)/shard_map/ppermute | solution.py:227
  24.9 14.1 %collective-permute-start.2 = (bf16[2,264,128]{2,1,0:T(8,128)(2,1)}, bf16[2,264,128]{2,1,0:T(8,128)(2,1)S(1)}, u32[]{:S(2)}, u32[]{:S(2)}) collective-permute-start(bf16[2,264,128]{2,1,0:T(8,128)(2,1)} %get-tuple-element.17), channel_id=1, source_target_pairs={{0,3},{1,4},{2,5},{3,6},{4,7},{5,0},{6,1},{7,2},{8,11},{9,12},{10,... | collective-permute-start | bytes 405512 | tf_op jit(solution)/shard_map/ppermute | solution.py:227
  27.8 29.4 %collective-permute-start.3 = (bf16[2,264,128]{2,1,0:T(8,128)(2,1)}, bf16[2,264,128]{2,1,0:T(8,128)(2,1)S(1)}, u32[]{:S(2)}, u32[]{:S(2)}) collective-permute-start(bf16[2,264,128]{2,1,0:T(8,128)(2,1)} %get-tuple-element.18), channel_id=1, source_target_pairs={{0,4},{1,5},{2,6},{3,7},{4,0},{5,1},{6,2},{7,3},{8,12},{9,13},{10,... | collective-permute-start | bytes 405512 | tf_op jit(solution)/shard_map/ppermute | solution.py:227
  29.2 28.0 %collective-permute-start.4 = (bf16[2,264,128]{2,1,0:T(8,128)(2,1)}, bf16[2,264,128]{2,1,0:T(8,128)(2,1)S(1)}, u32[]{:S(2)}, u32[]{:S(2)}) collective-permute-start(bf16[2,264,128]{2,1,0:T(8,128)(2,1)} %get-tuple-element.19), channel_id=1, source_target_pairs={{0,5},{1,6},{2,7},{3,0},{4,1},{5,2},{6,3},{7,4},{8,13},{9,14},{10,... | collective-permute-start | bytes 405512 | tf_op jit(solution)/shard_map/ppermute | solution.py:227
  34.5 22.8 %collective-permute-start.5 = (bf16[2,264,128]{2,1,0:T(8,128)(2,1)}, bf16[2,264,128]{2,1,0:T(8,128)(2,1)S(1)}, u32[]{:S(2)}, u32[]{:S(2)}) collective-permute-start(bf16[2,264,128]{2,1,0:T(8,128)(2,1)} %get-tuple-element.20), channel_id=1, source_target_pairs={{0,6},{1,7},{2,0},{3,1},{4,2},{5,3},{6,4},{7,5},{8,14},{9,15},{10,... | collective-permute-start | bytes 405512 | tf_op jit(solution)/shard_map/ppermute | solution.py:227
  37.6 19.8 %collective-permute-start.6 = (bf16[2,264,128]{2,1,0:T(8,128)(2,1)}, bf16[2,264,128]{2,1,0:T(8,128)(2,1)S(1)}, u32[]{:S(2)}, u32[]{:S(2)}) collective-permute-start(bf16[2,264,128]{2,1,0:T(8,128)(2,1)} %get-tuple-element.21), channel_id=1, source_target_pairs={{0,7},{1,0},{2,1},{3,2},{4,3},{5,4},{6,5},{7,6},{8,15},{9,8},{10,9... | collective-permute-start | bytes 405512 | tf_op jit(solution)/shard_map/ppermute | solution.py:227
  39.0 49.4 %collective-permute-start.15 = (bf16[8,256,128]{2,1,0:T(8,128)(2,1)}, bf16[8,256,128]{2,1,0:T(8,128)(2,1)S(1)}, u32[]{:S(2)}, u32[]{:S(2)}) collective-permute-start(bf16[8,256,128]{2,1,0:T(8,128)(2,1)} %get-tuple-element.23), channel_id=1, source_target_pairs={{0,8},{8,0},{16,24},{24,16},{32,40},{40,32},{48,56},{56,48},{64,72... | collective-permute-start | bytes 1572872 | tf_op jit(solution)/shard_map/ppermute | solution.py:218
  59.8 16.2 %collective-permute-start.8 = (bf16[2,264,128]{2,1,0:T(8,128)(2,1)S(1)}, bf16[2,264,128]{2,1,0:T(8,128)(2,1)S(1)}, u32[]{:S(2)}, u32[]{:S(2)}) collective-permute-start(bf16[2,264,128]{2,1,0:T(8,128)(2,1)S(1)} %get-tuple-element.35), channel_id=1, source_target_pairs={{0,32},{8,40},{16,48},{24,56},{32,64},{40,72},{48,80},{56,88},{64,... | collective-permute-start | bytes 405512 | tf_op jit(solution)/shard_map/ppermute | solution.py:241
  63.9 24.5 %collective-permute-start.9 = (bf16[2,264,128]{2,1,0:T(8,128)(2,1)S(1)}, bf16[2,264,128]{2,1,0:T(8,128)(2,1)S(1)}, u32[]{:S(2)}, u32[]{:S(2)}) collective-permute-start(bf16[2,264,128]{2,1,0:T(8,128)(2,1)S(1)} %get-tuple-element.34), channel_id=1, source_target_pairs={{0,48},{8,56},{16,64},{24,72},{32,80},{40,88},{48,96},{56,104},{64... | collective-permute-start | bytes 405512 | tf_op jit(solution)/shard_map/ppermute | solution.py:241
  70.2 18.2 %collective-permute-start.10 = (bf16[2,264,128]{2,1,0:T(8,128)(2,1)S(1)}, bf16[2,264,128]{2,1,0:T(8,128)(2,1)S(1)}, u32[]{:S(2)}, u32[]{:S(2)}) collective-permute-start(bf16[2,264,128]{2,1,0:T(8,128)(2,1)S(1)} %get-tuple-element.33), channel_id=1, source_target_pairs={{0,64},{8,72},{16,80},{24,88},{32,96},{40,104},{48,112},{56,120},{... | collective-permute-start | bytes 405512 | tf_op jit(solution)/shard_map/ppermute | solution.py:241
  71.5 16.9 %collective-permute-start.11 = (bf16[2,264,128]{2,1,0:T(8,128)(2,1)S(1)}, bf16[2,264,128]{2,1,0:T(8,128)(2,1)S(1)}, u32[]{:S(2)}, u32[]{:S(2)}) collective-permute-start(bf16[2,264,128]{2,1,0:T(8,128)(2,1)S(1)} %get-tuple-element.32), channel_id=1, source_target_pairs={{0,80},{8,88},{16,96},{24,104},{32,112},{40,120},{48,0},{56,8},{64... | collective-permute-start | bytes 405512 | tf_op jit(solution)/shard_map/ppermute | solution.py:241
  76.0 18.9 %collective-permute-start.12 = (bf16[2,264,128]{2,1,0:T(8,128)(2,1)S(1)}, bf16[2,264,128]{2,1,0:T(8,128)(2,1)S(1)}, u32[]{:S(2)}, u32[]{:S(2)}) collective-permute-start(bf16[2,264,128]{2,1,0:T(8,128)(2,1)S(1)} %get-tuple-element.31), channel_id=1, source_target_pairs={{0,96},{8,104},{16,112},{24,120},{32,0},{40,8},{48,16},{56,24},{64... | collective-permute-start | bytes 405512 | tf_op jit(solution)/shard_map/ppermute | solution.py:241
  88.4 38.4 %collective-permute-start.13 = (bf16[2,264,128]{2,1,0:T(8,128)(2,1)S(1)}, bf16[2,264,128]{2,1,0:T(8,128)(2,1)S(1)}, u32[]{:S(2)}, u32[]{:S(2)}) collective-permute-start(bf16[2,264,128]{2,1,0:T(8,128)(2,1)S(1)} %get-tuple-element.30), channel_id=1, source_target_pairs={{0,112},{8,120},{16,0},{24,8},{32,16},{40,24},{48,32},{56,40},{64,... | collective-permute-start | bytes 405512 | tf_op jit(solution)/shard_map/ppermute | solution.py:241
  88.7 14.6 %collective-permute-start.16 = (bf16[512,128]{1,0:T(8,128)(2,1)S(1)}, bf16[512,128]{1,0:T(8,128)(2,1)S(1)}, u32[]{:S(2)}, u32[]{:S(2)}) collective-permute-start(bf16[512,128]{1,0:T(8,128)(2,1)S(1)} %bitcast.194), channel_id=1, source_target_pairs={{0,1},{1,2},{2,3},{3,4},{4,5},{5,6},{6,7},{7,0},{8,9},{9,10},{10,1... | collective-permute-start | bytes 393224 | tf_op jit(solution)/shard_map/ppermute | solution.py:227
  99.6 16.5 %collective-permute-start.19 = (bf16[512,128]{1,0:T(8,128)(2,1)S(1)}, bf16[512,128]{1,0:T(8,128)(2,1)S(1)}, u32[]{:S(2)}, u32[]{:S(2)}) collective-permute-start(bf16[512,128]{1,0:T(8,128)(2,1)S(1)} %bitcast.191), channel_id=1, source_target_pairs={{0,4},{1,5},{2,6},{3,7},{4,0},{5,1},{6,2},{7,3},{8,12},{9,13},{10,... | collective-permute-start | bytes 393224 | tf_op jit(solution)/shard_map/ppermute | solution.py:227
  103.3 13.7 %collective-permute-start.20 = (bf16[512,128]{1,0:T(8,128)(2,1)S(1)}, bf16[512,128]{1,0:T(8,128)(2,1)S(1)}, u32[]{:S(2)}, u32[]{:S(2)}) collective-permute-start(bf16[512,128]{1,0:T(8,128)(2,1)S(1)} %bitcast.190), channel_id=1, source_target_pairs={{0,5},{1,6},{2,7},{3,0},{4,1},{5,2},{6,3},{7,4},{8,13},{9,14},{10,... | collective-permute-start | bytes 393224 | tf_op jit(solution)/shard_map/ppermute | solution.py:227
  103.5 21.1 %collective-permute-start.21 = (bf16[512,128]{1,0:T(8,128)(2,1)S(1)}, bf16[512,128]{1,0:T(8,128)(2,1)S(1)}, u32[]{:S(2)}, u32[]{:S(2)}) collective-permute-start(bf16[512,128]{1,0:T(8,128)(2,1)S(1)} %bitcast.189), channel_id=1, source_target_pairs={{0,6},{1,7},{2,0},{3,1},{4,2},{5,3},{6,4},{7,5},{8,14},{9,15},{10,... | collective-permute-start | bytes 393224 | tf_op jit(solution)/shard_map/ppermute | solution.py:227
  108.9 17.4 %collective-permute-start.22 = (bf16[512,128]{1,0:T(8,128)(2,1)S(1)}, bf16[512,128]{1,0:T(8,128)(2,1)S(1)}, u32[]{:S(2)}, u32[]{:S(2)}) collective-permute-start(bf16[512,128]{1,0:T(8,128)(2,1)S(1)} %bitcast.188), channel_id=1, source_target_pairs={{0,7},{1,0},{2,1},{3,2},{4,3},{5,4},{6,5},{7,6},{8,15},{9,8},{10,9... | collective-permute-start | bytes 393224 | tf_op jit(solution)/shard_map/ppermute | solution.py:227
  126.8 31.3 %collective-permute-start.14 = (bf16[8,264,128]{2,1,0:T(8,128)(2,1)S(1)}, bf16[8,264,128]{2,1,0:T(8,128)(2,1)S(1)}, u32[]{:S(2)}, u32[]{:S(2)}) collective-permute-start(bf16[8,264,128]{2,1,0:T(8,128)(2,1)S(1)} %dynamic-slice_bitcast_fusion), channel_id=1, source_target_pairs={{0,8},{8,0},{16,24},{24,16},{32,40},{40,32},{48,56},{56,48},{64,72... | collective-permute-start | bytes 1622024 | tf_op jit(solution)/shard_map/ppermute | solution.py:218
  129.1 21.4 %collective-permute-start.25 = (bf16[512,128]{1,0:T(8,128)(2,1)S(1)}, bf16[512,128]{1,0:T(8,128)(2,1)S(1)}, u32[]{:S(2)}, u32[]{:S(2)}) collective-permute-start(bf16[512,128]{1,0:T(8,128)(2,1)S(1)} %get-tuple-element.42), channel_id=1, source_target_pairs={{0,48},{8,56},{16,64},{24,72},{32,80},{40,88},{48,96},{56,104},{64... | collective-permute-start | bytes 393224 | tf_op jit(solution)/shard_map/ppermute | solution.py:241
  133.1 17.4 %collective-permute-start.26 = (bf16[512,128]{1,0:T(8,128)(2,1)S(1)}, bf16[512,128]{1,0:T(8,128)(2,1)S(1)}, u32[]{:S(2)}, u32[]{:S(2)}) collective-permute-start(bf16[512,128]{1,0:T(8,128)(2,1)S(1)} %get-tuple-element.41), channel_id=1, source_target_pairs={{0,64},{8,72},{16,80},{24,88},{32,96},{40,104},{48,112},{56,120},{... | collective-permute-start | bytes 393224 | tf_op jit(solution)/shard_map/ppermute | solution.py:241
  135.0 15.6 %collective-permute-start.27 = (bf16[512,128]{1,0:T(8,128)(2,1)S(1)}, bf16[512,128]{1,0:T(8,128)(2,1)S(1)}, u32[]{:S(2)}, u32[]{:S(2)}) collective-permute-start(bf16[512,128]{1,0:T(8,128)(2,1)S(1)} %get-tuple-element.40), channel_id=1, source_target_pairs={{0,80},{8,88},{16,96},{24,104},{32,112},{40,120},{48,0},{56,8},{64... | collective-permute-start | bytes 393224 | tf_op jit(solution)/shard_map/ppermute | solution.py:241
  137.1 20.5 %collective-permute-start.28 = (bf16[512,128]{1,0:T(8,128)(2,1)S(1)}, bf16[512,128]{1,0:T(8,128)(2,1)S(1)}, u32[]{:S(2)}, u32[]{:S(2)}) collective-permute-start(bf16[512,128]{1,0:T(8,128)(2,1)S(1)} %get-tuple-element.39), channel_id=1, source_target_pairs={{0,96},{8,104},{16,112},{24,120},{32,0},{40,8},{48,16},{56,24},{64... | collective-permute-start | bytes 393224 | tf_op jit(solution)/shard_map/ppermute | solution.py:241
  (15 other events, 172.7 us)

commit v5 on v4

--- a/solution.py
+++ b/solution.py
@@ -14,49 +14,35 @@
 epsilon = 1e-06
 
 
-def project_kernel(place, x_hbm, gain, in_hbm, forget_hbm, key_hbm, value_hbm, *rest):
+def project_kernel(x_hbm, gain, in_hbm, forget_hbm, key_hbm, value_hbm, *rest):
     *keys, kept, given, x, gate_weight, weight, normed, gates, x_sem, gate_sem, sem = rest
     step = pl.program_id(0)
     seqs, rows, lane = keys[0].shape[0], kept.shape[1], kept.shape[2]
     lines = rows // lane
     parts = x_sem.shape[0]
     part = x.shape[0] // parts
-    chunk = 64
-
-    def column(kind, shift):
-        head = lax.rem(place[0] + shift, HEADS)
-        source = (key_hbm, value_hbm)[kind].at[:, pl.ds(pl.multiple_of(head * lane, lane), lane)]
-        half = shift % 2
-        target = weight.at[kind, shift // 2, :, half * lane : (half + 1) * lane]
-        return pltpu.make_async_copy(source, target, sem.at[kind, shift])
-
-    def arrive(kind):
-        for half in range(2):
-            pltpu.make_async_copy(
-                key_hbm.at[:, :lane],
-                weight.at[kind, step, :, half * lane : (half + 1) * lane],
-                sem.at[kind, 2 * step + half],
-            ).wait()
+    chunk = 16
+    pieces = [
+        pltpu.make_async_copy(
+            x_hbm.at[n * part : (n + 1) * part], x.at[n * part : (n + 1) * part], x_sem.at[n]
+        )
+        for n in range(parts)
+    ]
+    gate_copies = [
+        pltpu.make_async_copy(ref, gate_weight.at[n], gate_sem.at[n])
+        for n, ref in enumerate((in_hbm, forget_hbm))
+    ]
+    weight_copies = [
+        pltpu.make_async_copy(ref, weight.at[n], sem.at[n])
+        for n, ref in enumerate((key_hbm, value_hbm))
+    ]
 
     @pl.when(step == 0)
     def _():
-        pieces = [
-            pltpu.make_async_copy(
-                x_hbm.at[n * part : (n + 1) * part], x.at[n * part : (n + 1) * part], x_sem.at[n]
-            )
-            for n in range(parts)
-        ]
-        gate_copies = [
-            pltpu.make_async_copy(ref, gate_weight.at[n], gate_sem.at[n])
-            for n, ref in enumerate((in_hbm, forget_hbm))
-        ]
-        for copy in pieces + gate_copies:
+        for copy in pieces + gate_copies + weight_copies:
             copy.start()
-        for shift in range(0, HEADS, 2):
-            for kind in range(2):
-                column(kind, shift).start()
-                column(kind, shift + 1).start()
-        scale = gain[...].astype(jnp.float32)
+        fine = gain[...].astype(jnp.float32)
+        scale = jnp.concatenate([fine[n : n + 1] for n in range(fine.shape[0])], axis=1)
         for n in range(parts):
             pieces[n].wait()
 
@@ -70,19 +56,24 @@
         for n in range(2):
             gate_copies[n].wait()
         both = jnp.concatenate([gate_weight[0], gate_weight[1]], axis=0)
-        gates[...] = lax.dot_general(
-            both, normed[...], (((1,), (1,)), ((), ())), preferred_element_type=jnp.float32
+        across = lax.dot_general(
+            normed[...], both, (((1,), (1,)), ((), ())), preferred_element_type=jnp.float32
         )
+        gates[...] = across.T
+        weight_copies[0].wait()
+
+    heads = [lax.rem(lax.axis_index("tp") + 2 * step + j, HEADS) for j in range(2)]
 
     def dot(kind):
-        arrive(kind)
-        out = jnp.dot(normed[...], weight[kind, step], preferred_element_type=jnp.float32)
+        sides = [weight[kind, :, pl.ds(pl.multiple_of(h * lane, lane), lane)] for h in heads]
+        out = jnp.dot(
+            normed[...], jnp.concatenate(sides, axis=1), preferred_element_type=jnp.float32
+        )
         return out.astype(jnp.bfloat16)
 
     key_rows = dot(0)
     tails = []
-    for j in range(2):
-        head = lax.rem(place[0] + 2 * step + j, HEADS)
+    for head in heads:
         pair = [gates[pl.ds(head + HEADS * g, 1), :] for g in range(2)]
         for a in range(seqs):
             cut = [
@@ -102,8 +93,12 @@
                     keys[2 * c + j][a, :rows, :] = block
                     keys[2 * c + j][a, rows:, :] = tails[j * seqs + a]
 
+    @pl.when(step == 0)
+    def _():
+        weight_copies[1].wait()
+
     value_rows = dot(1)
-    first = place[1] == 0
+    first = lax.rem(lax.axis_index("sp"), 2) == 0
     for j in range(2):
         one = value_rows[:rows, j * lane : (j + 1) * lane]
         two = value_rows[rows:, j * lane : (j + 1) * lane]
@@ -111,37 +106,34 @@
         given[j] = jnp.where(first, two, one)
 
 
-def project(place, layer_input, norm_gain, key_weight, value_weight, gate_in, gate_forget):
+def project(layer_input, norm_gain, key_weight, value_weight, gate_in, gate_forget):
     seqs, rows, width = layer_input.shape
     tokens = seqs * rows
 
     def whole(*shape):
-        return pl.BlockSpec(shape, lambda i, p: (0,) * len(shape))
+        return pl.BlockSpec(shape, lambda i: (0,) * len(shape))
 
     def halves():
-        return pl.BlockSpec((2, rows, DK), lambda i, p: (i, 0, 0))
-
-    hbm = pl.BlockSpec(memory_space=pltpu.MemorySpace.HBM)
+        return pl.BlockSpec((2, rows, DK), lambda i: (i, 0, 0))
+
+    hbm = pl.BlockSpec(memory_space=pl.ANY)
     key_shape = (seqs, rows + 8, DK)
     value_shape = (HEADS, rows, DK)
     *keys, kept, given = pl.pallas_call(
         project_kernel,
-        grid_spec=pltpu.PrefetchScalarGridSpec(
-            num_scalar_prefetch=1,
-            grid=(HEADS // 2,),
-            in_specs=[hbm, whole(1, width), hbm, hbm, hbm, hbm],
-            out_specs=[whole(*key_shape)] * HEADS + [halves(), halves()],
-            scratch_shapes=[
-                pltpu.VMEM((tokens, width), jnp.bfloat16),
-                pltpu.VMEM((2, HEADS, width), jnp.bfloat16),
-                pltpu.VMEM((2, HEADS // 2, width, 2 * DK), jnp.bfloat16),
-                pltpu.VMEM((tokens, width), jnp.bfloat16),
-                pltpu.VMEM((2 * HEADS, tokens), jnp.float32),
-                pltpu.SemaphoreType.DMA((4,)),
-                pltpu.SemaphoreType.DMA((2,)),
-                pltpu.SemaphoreType.DMA((2, HEADS)),
-            ],
-        ),
+        grid=(HEADS // 2,),
+        in_specs=[hbm, whole(width // DK, DK), hbm, hbm, hbm, hbm],
+        out_specs=[whole(*key_shape)] * HEADS + [halves(), halves()],
+        scratch_shapes=[
+            pltpu.VMEM((tokens, width), jnp.bfloat16),
+            pltpu.VMEM((2, HEADS, width), jnp.bfloat16),
+            pltpu.VMEM((2, width, HEADS * DK), jnp.bfloat16),
+            pltpu.VMEM((tokens, width), jnp.bfloat16),
+            pltpu.VMEM((2 * HEADS, tokens), jnp.float32),
+            pltpu.SemaphoreType.DMA((4,)),
+            pltpu.SemaphoreType.DMA((2,)),
+            pltpu.SemaphoreType.DMA((2,)),
+        ],
         out_shape=[jax.ShapeDtypeStruct(key_shape, jnp.bfloat16)] * HEADS
         + [jax.ShapeDtypeStruct(value_shape, jnp.bfloat16)] * 2,
         compiler_params=pltpu.CompilerParams(
@@ -154,15 +146,70 @@
         ),
         name="project",
     )(
-        place,
         layer_input.reshape(tokens, width),
-        norm_gain.reshape(1, width),
+        norm_gain.reshape(width // DK, DK),
         gate_in.T,
         gate_forget.T,
         key_weight,
         value_weight,
     )
     return keys, kept, given
+
+
+def finish_kernel(scores, fresh, bottom, new_value, *rest):
+    chips = scores.shape[0]
+    *blocks, cache, read, held, in_sem, out_sem = rest
+    chip = lax.axis_index("sp") // 2
+    moves = [pltpu.make_async_copy(b, held.at[n], in_sem.at[n]) for n, b in enumerate(blocks)]
+    for move in moves:
+        move.start()
+    total = fresh[0, 0] * new_value[...].astype(jnp.float32)
+    stores = []
+    for n in range(chips):
+        source = lax.rem(chip - n + chips, chips)
+        moves[n].wait()
+        stores.append(pltpu.make_async_copy(held.at[n], cache.at[source], out_sem.at[n]))
+        stores[n].start()
+        block = held[n]
+        row = jnp.broadcast_to(scores[pl.ds(source, 1), :], (8, scores.shape[1]))
+        part = jnp.dot(
+            row.astype(jnp.bfloat16),
+            block.reshape(-1, block.shape[-1]),
+            preferred_element_type=jnp.float32,
+        )
+        total = total + part[:1]
+    read[...] = (total / jnp.maximum(jnp.abs(bottom[0, 0]), 1.0)).astype(jnp.bfloat16)
+    for store in stores:
+        store.wait()
+
+
+def finish(blocks, scores, new_score, denominator, new_value):
+    chips, shape = len(blocks), blocks[0].shape
+    vmem, smem = (pl.BlockSpec(memory_space=m) for m in (pltpu.VMEM, pltpu.SMEM))
+    anywhere = pl.BlockSpec(memory_space=pl.ANY)
+    cache, read = pl.pallas_call(
+        finish_kernel,
+        in_specs=[vmem, smem, smem, vmem] + [anywhere] * chips,
+        out_specs=[anywhere, vmem],
+        scratch_shapes=[
+            pltpu.VMEM((chips,) + shape, jnp.bfloat16),
+            pltpu.SemaphoreType.DMA((chips,)),
+            pltpu.SemaphoreType.DMA((chips,)),
+        ],
+        out_shape=[
+            jax.ShapeDtypeStruct((chips,) + shape, jnp.bfloat16),
+            jax.ShapeDtypeStruct((1, DK), jnp.bfloat16),
+        ],
+        compiler_params=pltpu.CompilerParams(vmem_limit_bytes=60 * 1024 * 1024),
+        name="finish",
+    )(
+        scores.astype(jnp.float32).reshape(chips, -1),
+        new_score.astype(jnp.float32),
+        denominator,
+        new_value.reshape(1, DK),
+        *blocks,
+    )
+    return cache, read
 
 
 def convolve(key_linear, tap_weight):
@@ -202,14 +249,8 @@
     scores = (weight_cache * matched * scaling).astype(jnp.bfloat16)
     denominator = jnp.sum(scores.astype(jnp.float32), axis=2)
     denominator = denominator + new_score.astype(jnp.float32)
-    numerator = jnp.einsum("bhl,bhlk->bhk", scores, values, preferred_element_type=jnp.float32)
-    numerator = numerator + new_score.astype(jnp.float32)[:, :, None] * new_value.astype(
-        jnp.float32
-    )
-    first_read = (numerator / jnp.maximum(jnp.abs(denominator), 1.0)[:, :, None]).astype(
-        jnp.bfloat16
-    )
-    return (weight_cache, first_read)
+    cache, first_read = finish(values, scores, new_score, denominator, new_value)
+    return (cache, weight_cache, first_read)
 
 
 def trade(own, other):
@@ -232,14 +273,23 @@
     ring, chips = lax.axis_size("sp"), stack.shape[0]
     pair = ring // chips
     column, chip = lax.axis_index("tp"), lax.axis_index("sp") // pair
-    whole = jnp.zeros_like(stack)
+    got = []
     for step in range(chips):
         target = (chip + step) % chips
         mine = lax.dynamic_index_in_dim(stack, (column - target) % chips, 0, keepdims=False)
         if step:
             route = [(i, (i // pair + step) % chips * pair + i % pair) for i in range(ring)]
             mine = lax.ppermute(mine, "sp", route)
-        whole = lax.dynamic_update_index_in_dim(whole, mine, (chip - step) % chips, 0)
+        got.append(mine)
+    return got
+
+
+def in_order(blocks):
+    chips = len(blocks)
+    chip = lax.axis_index("sp") * chips // lax.axis_size("sp")
+    whole = jnp.zeros((chips,) + blocks[0].shape, blocks[0].dtype)
+    for step, block in enumerate(blocks):
+        whole = lax.dynamic_update_index_in_dim(whole, block, (chip - step) % chips, 0)
     return whole
 
 
@@ -259,12 +309,10 @@
     new_input,
     new_forget,
 ):
-    seqs, rows, _ = layer_input.shape
+    _, rows, _ = layer_input.shape
     lines = rows // DK
     core = lax.axis_index("sp") % 2
-    place = jnp.stack([lax.axis_index("tp"), core]).astype(jnp.int32)
     key_blocks, kept, given = project(
-        place,
         layer_input,
         norm_gain,
         key_weight,
@@ -272,21 +320,20 @@
         input_gate_weight,
         forget_gate_weight,
     )
-    value_blocks = trade(kept, given).reshape(HEADS, seqs * rows, DK)
-    mine = spread(rotate(key_blocks))
+    value_blocks = trade(kept, given)
+    mine = in_order(spread(rotate(key_blocks)))
     own = lax.dynamic_index_in_dim(mine, core, 1, keepdims=False)
     other = lax.dynamic_index_in_dim(mine, 1 - core, 1, keepdims=False)
     mine = trade(own, other).reshape((-1,) + own.shape[1:])
     values = spread(rotate(value_blocks))
     length = mine.shape[0] * rows
     key_linear = mine[:, :rows].reshape(length, DK)
-    values = values.reshape(1, 1, length, DK)
     input_linear = mine[:, rows : rows + lines].reshape(1, 1, length)
     forget_linear = mine[:, rows + lines : rows + 2 * lines].reshape(1, 1, length)
     head = lax.axis_index("tp")
     tap_weight = lax.dynamic_slice(conv_weight, (0, head * DK), (CONV, DK))
     keys = convolve(key_linear, tap_weight).reshape(1, 1, length, DK)
-    weight_cache, first_read = read_cache(
+    values, weight_cache, first_read = read_cache(
         keys,
         values,
         input_linear,
@@ -299,7 +346,7 @@
         new_input,
         new_forget,
     )
-    return (keys, values, weight_cache, first_read)
+    return (keys, values.reshape(keys.shape), weight_cache, first_read.reshape(new_value.shape))
 
 
 def solution(mesh):

time: 169 us -> 174 us (1.030)
  waiting for transfers between devices: 49.3 us -> 69.9 us
  starting transfers between devices: 82.7 us -> 62.1 us
  Pallas kernels: 17.6 us -> 21 us
    ppermute x14, waiting for transfers between devices: 15.4 us -> 38.8 us  [rotate(): got.append(lax.ppermute(blocks[step], 'tp', route))]
    ppermute x14, starting transfers between devices: 35.1 us -> 21.2 us  [rotate(): got.append(lax.ppermute(blocks[step], 'tp', route))]
    ppermute x14, starting transfers between devices: 28.5 us -> 19.1 us  [spread(): mine = lax.ppermute(mine, 'sp', route)]
    pallas_call x1 -> x2, Pallas kernels: 17.6 us -> 21 us  [the longest x1 17.1 us: project(): pl.pallas_call(project_kernel, grid=(HEADS // 2,), in_specs=[hbm, whole(w...]
    ppermute x14, waiting for transfers between devices: 33.9 us -> 31.1 us  [spread(): mine = lax.ppermute(mine, 'sp', route)]
    ppermute x2, starting transfers between devices: 19.1 us -> 21.8 us  [trade(): got = lax.ppermute(other, 'sp', route)]
  transfers between devices with their start and end apart: 30 -> 30, of which waited for: 11 -> 17; matrix products, arithmetic and copies ran while one was open for 2% -> 7% of each run, Pallas kernels for 0% -> 0%
where the time goes in v5:
time: 174 us; the launch traced here: 172 us
  waiting for transfers between devices  69.9 us (40%)
  starting transfers between devices  62.1 us (36%)
  Pallas kernels  21 us (12%)
  local copies, waits for them, and re-layouts  5.96 us (3%)
  other arithmetic  5.71 us (3%)
  between operations  5.04 us (3%)
  matrix products  2.66 us (2%)
    ppermute x14, waiting for transfers between devices, rotate(): got.append(lax.ppermute(blocks[step], 'tp', route))  38.8 us
    ppermute x14, waiting for transfers between devices, spread(): mine = lax.ppermute(mine, 'sp', route)  31.1 us
    ppermute x2, starting transfers between devices, trade(): got = lax.ppermute(other, 'sp', route)  21.8 us
    ppermute x14, starting transfers between devices, rotate(): got.append(lax.ppermute(blocks[step], 'tp', route))  21.2 us
    ppermute x14, starting transfers between devices, spread(): mine = lax.ppermute(mine, 'sp', route)  19.1 us
    pallas_call x1, Pallas kernels, project(): pl.pallas_call(project_kernel, grid=(HEADS // 2,), in_specs=[hbm, whole(w...  17.1 us
    pallas_call x1, Pallas kernels, finish(): pl.pallas_call(finish_kernel, in_specs=[vmem, smem, smem, vmem] + [anywhe...  3.88 us
  transfers between devices with their start and end apart: 30, of which 17 were waited for; matrix products, arithmetic and copies ran while one was open for 7% of the time, Pallas kernels for 0%

profile of v5, /device:TPU:513, one launch (start us, length us, event | category | flops | bytes accessed | tf_op | source)
XLA Modules:
  0.0 172.3 jit_solution(9894668941538646220)
XLA Ops:
  0.7 17.1 %project.1 = (bf16[2,264,128]{2,1,0:T(8,128)(2,1)}, bf16[2,264,128]{2,1,0:T(8,128)(2,1)}, bf16[2,264,128]{2,1,0:T(8,128)(2,1)}, bf16[2,264,128]{2,1,0:T(8,128)(2...) custom-call(bf16[512,2048]{1,0:T(8,128)(2,1)} %bitcast.184, ...), custom_call_target="tpu_custom_call" | custom-call | flops 4294967296 | bytes 12582912 | tf_op jit(solution)/shard_map/project/pallas_call | solution.py:122
  17.8 20.5 %collective-permute-start.15 = (bf16[8,256,128]{2,1,0:T(8,128)(2,1)}, bf16[8,256,128]{2,1,0:T(8,128)(2,1)S(1)}, u32[]{:S(2)}, u32[]{:S(2)}) collective-permute-start(bf16[8,256,128]{2,1,0:T(8,128)(2,1)} %get-tuple-element.25), channel_id=1, source_target_pairs={{0,8},{8,0},{16,24},{24,16},{32,40},{40,32},{48,56},{56,48},{64,72... | collective-permute-start | bytes 1572872 | tf_op jit(solution)/shard_map/ppermute | solution.py:259
  38.4 5.6 %collective-permute-start.3 = (bf16[2,264,128]{2,1,0:T(8,128)(2,1)}, bf16[2,264,128]{2,1,0:T(8,128)(2,1)S(1)}, u32[]{:S(2)}, u32[]{:S(2)}) collective-permute-start(bf16[2,264,128]{2,1,0:T(8,128)(2,1)} %get-tuple-element.20), channel_id=1, source_target_pairs={{0,4},{1,5},{2,6},{3,7},{4,0},{5,1},{6,2},{7,3},{8,12},{9,13},{10,... | collective-permute-start | bytes 405512 | tf_op jit(solution)/shard_map/ppermute | solution.py:268
  46.2 2.5 %collective-permute-done.1 = bf16[2,264,128]{2,1,0:T(8,128)(2,1)S(1)} collective-permute-done((bf16[2,264,128]{2,1,0:T(8,128)(2,1)}, bf16[2,264,128]{2,1,0:T(8,128)(2,1)S(1)}, u32[]{:S(2)}, u32[]{:S(2)}) %collective-permute-start.1) | collective-permute-done | bytes 135200 | tf_op jit(solution)/shard_map/ppermute | solution.py:268
  50.0 11.2 %collective-permute-done.2 = bf16[2,264,128]{2,1,0:T(8,128)(2,1)S(1)} collective-permute-done((bf16[2,264,128]{2,1,0:T(8,128)(2,1)}, bf16[2,264,128]{2,1,0:T(8,128)(2,1)S(1)}, u32[]{:S(2)}, u32[]{:S(2)}) %collective-permute-start.2) | collective-permute-done | bytes 135200 | tf_op jit(solution)/shard_map/ppermute | solution.py:268
  61.2 3.1 %collective-permute-start.6 = (bf16[2,264,128]{2,1,0:T(8,128)(2,1)S(1)}, bf16[2,264,128]{2,1,0:T(8,128)(2,1)S(1)}, u32[]{:S(2)}, u32[]{:S(2)}) collective-permute-start(bf16[2,264,128]{2,1,0:T(8,128)(2,1)S(1)} %copy-done.7), channel_id=1, source_target_pairs={{0,7},{1,0},{2,1},{3,2},{4,3},{5,4},{6,5},{7,6},{8,15},{9,8},{10,9... | collective-permute-start | bytes 405512 | tf_op jit(solution)/shard_map/ppermute | solution.py:268
  64.7 4.1 %collective-permute-done.6 = bf16[2,264,128]{2,1,0:T(8,128)(2,1)S(1)} collective-permute-done((bf16[2,264,128]{2,1,0:T(8,128)(2,1)S(1)}, bf16[2,264,128]{2,1,0:T(8,128)(2,1)S(1)}, u32[]{:S(2)}, u32[]{:S(2)}) %collective-permute-start.6) | collective-permute-done | bytes 135200 | tf_op jit(solution)/shard_map/ppermute | solution.py:268
  71.3 5.5 %collective-permute-start.10 = (bf16[2,264,128]{2,1,0:T(8,128)(2,1)S(1)}, bf16[2,264,128]{2,1,0:T(8,128)(2,1)S(1)}, u32[]{:S(2)}, u32[]{:S(2)}) collective-permute-start(bf16[2,264,128]{2,1,0:T(8,128)(2,1)S(1)} %get-tuple-element.39), channel_id=1, source_target_pairs={{0,64},{8,72},{16,80},{24,88},{32,96},{40,104},{48,112},{56,120},{... | collective-permute-start | bytes 405512 | tf_op jit(solution)/shard_map/ppermute | solution.py:282
  76.8 5.3 %collective-permute-done.8 = bf16[2,264,128]{2,1,0:T(8,128)(2,1)S(1)} collective-permute-done((bf16[2,264,128]{2,1,0:T(8,128)(2,1)S(1)}, bf16[2,264,128]{2,1,0:T(8,128)(2,1)S(1)}, u32[]{:S(2)}, u32[]{:S(2)}) %collective-permute-start.8) | collective-permute-done | bytes 135200 | tf_op jit(solution)/shard_map/ppermute | solution.py:282
  82.2 11.4 %collective-permute-done.9 = bf16[2,264,128]{2,1,0:T(8,128)(2,1)S(1)} collective-permute-done((bf16[2,264,128]{2,1,0:T(8,128)(2,1)S(1)}, bf16[2,264,128]{2,1,0:T(8,128)(2,1)S(1)}, u32[]{:S(2)}, u32[]{:S(2)}) %collective-permute-start.9) | collective-permute-done | bytes 135200 | tf_op jit(solution)/shard_map/ppermute | solution.py:282
  93.7 4.2 %collective-permute-done.12 = bf16[2,264,128]{2,1,0:T(8,128)(2,1)S(1)} collective-permute-done((bf16[2,264,128]{2,1,0:T(8,128)(2,1)S(1)}, bf16[2,264,128]{2,1,0:T(8,128)(2,1)S(1)}, u32[]{:S(2)}, u32[]{:S(2)}) %collective-permute-start.12) | collective-permute-done | bytes 135200 | tf_op jit(solution)/shard_map/ppermute | solution.py:282
  97.8 3.6 %collective-permute-done.13 = bf16[2,264,128]{2,1,0:T(8,128)(2,1)S(1)} collective-permute-done((bf16[2,264,128]{2,1,0:T(8,128)(2,1)S(1)}, bf16[2,264,128]{2,1,0:T(8,128)(2,1)S(1)}, u32[]{:S(2)}, u32[]{:S(2)}) %collective-permute-start.13) | collective-permute-done | bytes 135200 | tf_op jit(solution)/shard_map/ppermute | solution.py:282
  108.5 2.3 %collective-permute-start.19 = (bf16[2,256,128]{2,1,0:T(8,128)(2,1)S(1)}, bf16[2,256,128]{2,1,0:T(8,128)(2,1)S(1)}, u32[]{:S(2)}, u32[]{:S(2)}) collective-permute-start(bf16[2,256,128]{2,1,0:T(8,128)(2,1)S(1)} %get-tuple-element.56), channel_id=1, source_target_pairs={{0,4},{1,5},{2,6},{3,7},{4,0},{5,1},{6,2},{7,3},{8,12},{9,13},{10,... | collective-permute-start | bytes 393224 | tf_op jit(solution)/shard_map/ppermute | solution.py:268
  112.7 2.4 %collective-permute-done.17 = bf16[2,256,128]{2,1,0:T(8,128)(2,1)S(1)} collective-permute-done((bf16[2,256,128]{2,1,0:T(8,128)(2,1)S(1)}, bf16[2,256,128]{2,1,0:T(8,128)(2,1)S(1)}, u32[]{:S(2)}, u32[]{:S(2)}) %collective-permute-start.17) | collective-permute-done | bytes 131104 | tf_op jit(solution)/shard_map/ppermute | solution.py:268
  116.5 7.4 %collective-permute-done.18 = bf16[2,256,128]{2,1,0:T(8,128)(2,1)S(1)} collective-permute-done((bf16[2,256,128]{2,1,0:T(8,128)(2,1)S(1)}, bf16[2,256,128]{2,1,0:T(8,128)(2,1)S(1)}, u32[]{:S(2)}, u32[]{:S(2)}) %collective-permute-start.18) | collective-permute-done | bytes 131104 | tf_op jit(solution)/shard_map/ppermute | solution.py:268
  123.8 4.2 %collective-permute-done.19 = bf16[2,256,128]{2,1,0:T(8,128)(2,1)S(1)} collective-permute-done((bf16[2,256,128]{2,1,0:T(8,128)(2,1)S(1)}, bf16[2,256,128]{2,1,0:T(8,128)(2,1)S(1)}, u32[]{:S(2)}, u32[]{:S(2)}) %collective-permute-start.19) | collective-permute-done | bytes 131104 | tf_op jit(solution)/shard_map/ppermute | solution.py:268
  128.6 5.6 %collective-permute-done.21 = bf16[2,256,128]{2,1,0:T(8,128)(2,1)S(1)} collective-permute-done((bf16[2,256,128]{2,1,0:T(8,128)(2,1)S(1)}, bf16[2,256,128]{2,1,0:T(8,128)(2,1)S(1)}, u32[]{:S(2)}, u32[]{:S(2)}) %collective-permute-start.21) | collective-permute-done | bytes 131104 | tf_op jit(solution)/shard_map/ppermute | solution.py:268
  138.5 3.0 %collective-permute-start.25 = (bf16[2,256,128]{2,1,0:T(8,128)(2,1)}, bf16[2,256,128]{2,1,0:T(8,128)(2,1)}, u32[]{:S(2)}, u32[]{:S(2)}) collective-permute-start(bf16[2,256,128]{2,1,0:T(8,128)(2,1)} %get-tuple-element.48), channel_id=1, source_target_pairs={{0,48},{8,56},{16,64},{24,72},{32,80},{40,88},{48,96},{56,104},{64... | collective-permute-start | bytes 393224 | tf_op jit(solution)/shard_map/ppermute | solution.py:282
  141.5 2.6 %collective-permute-start.26 = (bf16[2,256,128]{2,1,0:T(8,128)(2,1)}, bf16[2,256,128]{2,1,0:T(8,128)(2,1)}, u32[]{:S(2)}, u32[]{:S(2)}) collective-permute-start(bf16[2,256,128]{2,1,0:T(8,128)(2,1)} %get-tuple-element.47), channel_id=1, source_target_pairs={{0,64},{8,72},{16,80},{24,88},{32,96},{40,104},{48,112},{56,120},{... | collective-permute-start | bytes 393224 | tf_op jit(solution)/shard_map/ppermute | solution.py:282
  150.2 2.3 %fusion.26 = bf16[1,1,4096,128]{3,2,1,0:T(8,128)(2,1)} fusion(f32[4096,128]{1,0:T(8,128)S(1)} %bitcast_convert_fusion, f32[128]{0:T(128)S(1)} %get-tuple-element.62, f32[128]{0:T(128)S(1)} %get-tuple-element.63, f32[128]{0:T(128)S(1)} %get-tuple-element.64, f32[128]{0:T(128)S(1)} %get-tuple-element.61), kind=kLoop, calls=%fused_computation.103 | loop fusion | flops 6291456 | bytes 3147776 | tf_op jit(solution)/shard_map/reshape | solution.py:335
  152.5 3.4 %collective-permute-start.28 = (bf16[2,256,128]{2,1,0:T(8,128)(2,1)S(1)}, bf16[2,256,128]{2,1,0:T(8,128)(2,1)S(1)}, u32[]{:S(2)}, u32[]{:S(2)}) collective-permute-start(bf16[2,256,128]{2,1,0:T(8,128)(2,1)S(1)} %get-tuple-element.45), channel_id=1, source_target_pairs={{0,96},{8,104},{16,112},{24,120},{32,0},{40,8},{48,16},{56,24},{64... | collective-permute-start | bytes 393224 | tf_op jit(solution)/shard_map/ppermute | solution.py:282
  156.4 2.7 %fusion.23 = (f32[]{:T(128)}, f32[4096]{0:T(1024)S(1)}) fusion(f32[]{:T(128)} %broadcast.48, f32[1,1,4096]{2,1,0:T(1,128)S(1)} %subtract_exponential_fusion, bf16[1,1,128]{2,1,0:T(2,128)(2,1)S(1)} %copy-done.10, f32[4096,128]{1,0:T(8,128)S(1)} %bitcast_convert_fusion, f32[128]{0:T(128)S(1)} %get-tuple-element.62, f32[128]{0:T(128)S(1)} %get-tuple-element.63, ...), kind=kOutput, calls=%fused_computation.101 | convolution fusion | flops 7360511 | bytes 2132232 | tf_op jit(solution)/shard_map/bhlk,bhk->bhl/dot_general | solution.py:248
  161.1 5.5 %collective-permute-done.28.rest_6_ = bf16[2,256,128]{2,1,0:T(8,128)(2,1)S(1)} collective-permute-done((bf16[2,256,128]{2,1,0:T(8,128)(2,1)S(1)}, bf16[2,256,128]{2,1,0:T(8,128)(2,1)S(1)}, u32[]{:S(2)}, u32[]{:S(2)}) %collective-permute-start.28) | collective-permute-done | bytes 131104 | tf_op jit(solution)/shard_map/ppermute | solution.py:282
  168.2 3.9 %finish.1 = (bf16[8,2,256,128]{3,2,1,0:T(8,128)(2,1)}, bf16[1,128]{1,0:T(2,128)(2,1)}) custom-call(f32[8,512]{1,0:T(8,128)} %reshape.130.scores, f32[1,1]{1,0:T(1,128)S(6)} %convert_element_type.71.fresh, f32[1,1]{1,0:T(1,128)S(6)} %add.311.bottom, bf16[1,128]{1,0:T(2,128)(2,1)} %bitcast.182, bf16[2,256,128]{2,1,0:T(8,128)(2,1)} %get-tuple-element.51.rest_0_, ...), custom_call_target="tpu_custom_call" | custom-call | tf_op jit(solution)/shard_map/finish/pallas_call | solution.py:190
  (110 shorter events, 27.9 us)
Async XLA Ops:
  17.8 83.6 %collective-permute-start.15 = (bf16[8,256,128]{2,1,0:T(8,128)(2,1)}, bf16[8,256,128]{2,1,0:T(8,128)(2,1)S(1)}, u32[]{:S(2)}, u32[]{:S(2)}) collective-permute-start(bf16[8,256,128]{2,1,0:T(8,128)(2,1)} %get-tuple-element.25), channel_id=1, source_target_pairs={{0,8},{8,0},{16,24},{24,16},{32,40},{40,32},{48,56},{56,48},{64,72... | collective-permute-start | bytes 1572872 | tf_op jit(solution)/shard_map/ppermute | solution.py:259
  38.4 22.8 %collective-permute-start.2 = (bf16[2,264,128]{2,1,0:T(8,128)(2,1)}, bf16[2,264,128]{2,1,0:T(8,128)(2,1)S(1)}, u32[]{:S(2)}, u32[]{:S(2)}) collective-permute-start(bf16[2,264,128]{2,1,0:T(8,128)(2,1)} %get-tuple-element.19), channel_id=1, source_target_pairs={{0,3},{1,4},{2,5},{3,6},{4,7},{5,0},{6,1},{7,2},{8,11},{9,12},{10,... | collective-permute-start | bytes 405512 | tf_op jit(solution)/shard_map/ppermute | solution.py:268
  38.4 25.9 %collective-permute-start.3 = (bf16[2,264,128]{2,1,0:T(8,128)(2,1)}, bf16[2,264,128]{2,1,0:T(8,128)(2,1)S(1)}, u32[]{:S(2)}, u32[]{:S(2)}) collective-permute-start(bf16[2,264,128]{2,1,0:T(8,128)(2,1)} %get-tuple-element.20), channel_id=1, source_target_pairs={{0,4},{1,5},{2,6},{3,7},{4,0},{5,1},{6,2},{7,3},{8,12},{9,13},{10,... | collective-permute-start | bytes 405512 | tf_op jit(solution)/shard_map/ppermute | solution.py:268
  46.1 18.3 %collective-permute-start.4 = (bf16[2,264,128]{2,1,0:T(8,128)(2,1)}, bf16[2,264,128]{2,1,0:T(8,128)(2,1)S(1)}, u32[]{:S(2)}, u32[]{:S(2)}) collective-permute-start(bf16[2,264,128]{2,1,0:T(8,128)(2,1)} %get-tuple-element.21), channel_id=1, source_target_pairs={{0,5},{1,6},{2,7},{3,0},{4,1},{5,2},{6,3},{7,4},{8,13},{9,14},{10,... | collective-permute-start | bytes 405512 | tf_op jit(solution)/shard_map/ppermute | solution.py:268
  48.7 15.9 %collective-permute-start.5 = (bf16[2,264,128]{2,1,0:T(8,128)(2,1)S(1)}, bf16[2,264,128]{2,1,0:T(8,128)(2,1)S(1)}, u32[]{:S(2)}, u32[]{:S(2)}) collective-permute-start(bf16[2,264,128]{2,1,0:T(8,128)(2,1)S(1)} %copy-done.8), channel_id=1, source_target_pairs={{0,6},{1,7},{2,0},{3,1},{4,2},{5,3},{6,4},{7,5},{8,14},{9,15},{10,... | collective-permute-start | bytes 405512 | tf_op jit(solution)/shard_map/ppermute | solution.py:268
  71.3 10.9 %collective-permute-start.8 = (bf16[2,264,128]{2,1,0:T(8,128)(2,1)S(1)}, bf16[2,264,128]{2,1,0:T(8,128)(2,1)S(1)}, u32[]{:S(2)}, u32[]{:S(2)}) collective-permute-start(bf16[2,264,128]{2,1,0:T(8,128)(2,1)S(1)} %get-tuple-element.41), channel_id=1, source_target_pairs={{0,32},{8,40},{16,48},{24,56},{32,64},{40,72},{48,80},{56,88},{64,... | collective-permute-start | bytes 405512 | tf_op jit(solution)/shard_map/ppermute | solution.py:282
  71.3 22.3 %collective-permute-start.9 = (bf16[2,264,128]{2,1,0:T(8,128)(2,1)S(1)}, bf16[2,264,128]{2,1,0:T(8,128)(2,1)S(1)}, u32[]{:S(2)}, u32[]{:S(2)}) collective-permute-start(bf16[2,264,128]{2,1,0:T(8,128)(2,1)S(1)} %get-tuple-element.40), channel_id=1, source_target_pairs={{0,48},{8,56},{16,64},{24,72},{32,80},{40,88},{48,96},{56,104},{64... | collective-permute-start | bytes 405512 | tf_op jit(solution)/shard_map/ppermute | solution.py:282
  71.3 22.3 %collective-permute-start.10 = (bf16[2,264,128]{2,1,0:T(8,128)(2,1)S(1)}, bf16[2,264,128]{2,1,0:T(8,128)(2,1)S(1)}, u32[]{:S(2)}, u32[]{:S(2)}) collective-permute-start(bf16[2,264,128]{2,1,0:T(8,128)(2,1)S(1)} %get-tuple-element.39), channel_id=1, source_target_pairs={{0,64},{8,72},{16,80},{24,88},{32,96},{40,104},{48,112},{56,120},{... | collective-permute-start | bytes 405512 | tf_op jit(solution)/shard_map/ppermute | solution.py:282
  76.8 16.8 %collective-permute-start.11 = (bf16[2,264,128]{2,1,0:T(8,128)(2,1)S(1)}, bf16[2,264,128]{2,1,0:T(8,128)(2,1)S(1)}, u32[]{:S(2)}, u32[]{:S(2)}) collective-permute-start(bf16[2,264,128]{2,1,0:T(8,128)(2,1)S(1)} %get-tuple-element.38), channel_id=1, source_target_pairs={{0,80},{8,88},{16,96},{24,104},{32,112},{40,120},{48,0},{56,8},{64... | collective-permute-start | bytes 405512 | tf_op jit(solution)/shard_map/ppermute | solution.py:282
  82.1 15.7 %collective-permute-start.12 = (bf16[2,264,128]{2,1,0:T(8,128)(2,1)S(1)}, bf16[2,264,128]{2,1,0:T(8,128)(2,1)S(1)}, u32[]{:S(2)}, u32[]{:S(2)}) collective-permute-start(bf16[2,264,128]{2,1,0:T(8,128)(2,1)S(1)} %get-tuple-element.37), channel_id=1, source_target_pairs={{0,96},{8,104},{16,112},{24,120},{32,0},{40,8},{48,16},{56,24},{64... | collective-permute-start | bytes 405512 | tf_op jit(solution)/shard_map/ppermute | solution.py:282
  103.4 40.7 %collective-permute-start.14 = (bf16[8,264,128]{2,1,0:T(8,128)(2,1)S(1)}, bf16[8,264,128]{2,1,0:T(8,128)(2,1)S(1)}, u32[]{:S(2)}, u32[]{:S(2)}) collective-permute-start(bf16[8,264,128]{2,1,0:T(8,128)(2,1)S(1)} %dynamic-slice_bitcast_fusion), channel_id=1, source_target_pairs={{0,8},{8,0},{16,24},{24,16},{32,40},{40,32},{48,56},{56,48},{64,72... | collective-permute-start | bytes 1622024 | tf_op jit(solution)/shard_map/ppermute | solution.py:259
  104.7 10.4 %collective-permute-start.17 = (bf16[2,256,128]{2,1,0:T(8,128)(2,1)S(1)}, bf16[2,256,128]{2,1,0:T(8,128)(2,1)S(1)}, u32[]{:S(2)}, u32[]{:S(2)}) collective-permute-start(bf16[2,256,128]{2,1,0:T(8,128)(2,1)S(1)} %get-tuple-element.54), channel_id=1, source_target_pairs={{0,2},{1,3},{2,4},{3,5},{4,6},{5,7},{6,0},{7,1},{8,10},{9,11},{10,... | collective-permute-start | bytes 393224 | tf_op jit(solution)/shard_map/ppermute | solution.py:268
  106.6 17.2 %collective-permute-start.18 = (bf16[2,256,128]{2,1,0:T(8,128)(2,1)S(1)}, bf16[2,256,128]{2,1,0:T(8,128)(2,1)S(1)}, u32[]{:S(2)}, u32[]{:S(2)}) collective-permute-start(bf16[2,256,128]{2,1,0:T(8,128)(2,1)S(1)} %get-tuple-element.55), channel_id=1, source_target_pairs={{0,3},{1,4},{2,5},{3,6},{4,7},{5,0},{6,1},{7,2},{8,11},{9,12},{10,... | collective-permute-start | bytes 393224 | tf_op jit(solution)/shard_map/ppermute | solution.py:268
  108.5 19.5 %collective-permute-start.19 = (bf16[2,256,128]{2,1,0:T(8,128)(2,1)S(1)}, bf16[2,256,128]{2,1,0:T(8,128)(2,1)S(1)}, u32[]{:S(2)}, u32[]{:S(2)}) collective-permute-start(bf16[2,256,128]{2,1,0:T(8,128)(2,1)S(1)} %get-tuple-element.56), channel_id=1, source_target_pairs={{0,4},{1,5},{2,6},{3,7},{4,0},{5,1},{6,2},{7,3},{8,12},{9,13},{10,... | collective-permute-start | bytes 393224 | tf_op jit(solution)/shard_map/ppermute | solution.py:268
  110.7 17.9 %collective-permute-start.20 = (bf16[2,256,128]{2,1,0:T(8,128)(2,1)S(1)}, bf16[2,256,128]{2,1,0:T(8,128)(2,1)S(1)}, u32[]{:S(2)}, u32[]{:S(2)}) collective-permute-start(bf16[2,256,128]{2,1,0:T(8,128)(2,1)S(1)} %get-tuple-element.57), channel_id=1, source_target_pairs={{0,5},{1,6},{2,7},{3,0},{4,1},{5,2},{6,3},{7,4},{8,13},{9,14},{10,... | collective-permute-start | bytes 393224 | tf_op jit(solution)/shard_map/ppermute | solution.py:268
  115.1 19.2 %collective-permute-start.21 = (bf16[2,256,128]{2,1,0:T(8,128)(2,1)S(1)}, bf16[2,256,128]{2,1,0:T(8,128)(2,1)S(1)}, u32[]{:S(2)}, u32[]{:S(2)}) collective-permute-start(bf16[2,256,128]{2,1,0:T(8,128)(2,1)S(1)} %get-tuple-element.58), channel_id=1, source_target_pairs={{0,6},{1,7},{2,0},{3,1},{4,2},{5,3},{6,4},{7,5},{8,14},{9,15},{10,... | collective-permute-start | bytes 393224 | tf_op jit(solution)/shard_map/ppermute | solution.py:268
  123.8 11.0 %collective-permute-start.22 = (bf16[2,256,128]{2,1,0:T(8,128)(2,1)S(1)}, bf16[2,256,128]{2,1,0:T(8,128)(2,1)S(1)}, u32[]{:S(2)}, u32[]{:S(2)}) collective-permute-start(bf16[2,256,128]{2,1,0:T(8,128)(2,1)S(1)} %get-tuple-element.52), channel_id=1, source_target_pairs={{0,7},{1,0},{2,1},{3,2},{4,3},{5,4},{6,5},{7,6},{8,15},{9,8},{10,9... | collective-permute-start | bytes 393224 | tf_op jit(solution)/shard_map/ppermute | solution.py:268
  135.8 16.7 %collective-permute-start.23 = (bf16[2,256,128]{2,1,0:T(8,128)(2,1)}, bf16[2,256,128]{2,1,0:T(8,128)(2,1)}, u32[]{:S(2)}, u32[]{:S(2)}) collective-permute-start(bf16[2,256,128]{2,1,0:T(8,128)(2,1)} %get-tuple-element.50), channel_id=1, source_target_pairs={{0,16},{8,24},{16,32},{24,40},{32,48},{40,56},{48,64},{56,72},{64,... | collective-permute-start | bytes 393224 | tf_op jit(solution)/shard_map/ppermute | solution.py:282
  137.0 18.9 %collective-permute-start.24 = (bf16[2,256,128]{2,1,0:T(8,128)(2,1)}, bf16[2,256,128]{2,1,0:T(8,128)(2,1)}, u32[]{:S(2)}, u32[]{:S(2)}) collective-permute-start(bf16[2,256,128]{2,1,0:T(8,128)(2,1)} %get-tuple-element.49), channel_id=1, source_target_pairs={{0,32},{8,40},{16,48},{24,56},{32,64},{40,72},{48,80},{56,88},{64,... | collective-permute-start | bytes 393224 | tf_op jit(solution)/shard_map/ppermute | solution.py:282
  138.5 22.5 %collective-permute-start.25 = (bf16[2,256,128]{2,1,0:T(8,128)(2,1)}, bf16[2,256,128]{2,1,0:T(8,128)(2,1)}, u32[]{:S(2)}, u32[]{:S(2)}) collective-permute-start(bf16[2,256,128]{2,1,0:T(8,128)(2,1)} %get-tuple-element.48), channel_id=1, source_target_pairs={{0,48},{8,56},{16,64},{24,72},{32,80},{40,88},{48,96},{56,104},{64... | collective-permute-start | bytes 393224 | tf_op jit(solution)/shard_map/ppermute | solution.py:282
  141.5 19.6 %collective-permute-start.26 = (bf16[2,256,128]{2,1,0:T(8,128)(2,1)}, bf16[2,256,128]{2,1,0:T(8,128)(2,1)}, u32[]{:S(2)}, u32[]{:S(2)}) collective-permute-start(bf16[2,256,128]{2,1,0:T(8,128)(2,1)} %get-tuple-element.47), channel_id=1, source_target_pairs={{0,64},{8,72},{16,80},{24,88},{32,96},{40,104},{48,112},{56,120},{... | collective-permute-start | bytes 393224 | tf_op jit(solution)/shard_map/ppermute | solution.py:282
  144.1 16.9 %collective-permute-start.27 = (bf16[2,256,128]{2,1,0:T(8,128)(2,1)}, bf16[2,256,128]{2,1,0:T(8,128)(2,1)}, u32[]{:S(2)}, u32[]{:S(2)}) collective-permute-start(bf16[2,256,128]{2,1,0:T(8,128)(2,1)} %get-tuple-element.46), channel_id=1, source_target_pairs={{0,80},{8,88},{16,96},{24,104},{32,112},{40,120},{48,0},{56,8},{64... | collective-permute-start | bytes 393224 | tf_op jit(solution)/shard_map/ppermute | solution.py:282
  152.5 14.1 %collective-permute-start.28 = (bf16[2,256,128]{2,1,0:T(8,128)(2,1)S(1)}, bf16[2,256,128]{2,1,0:T(8,128)(2,1)S(1)}, u32[]{:S(2)}, u32[]{:S(2)}) collective-permute-start(bf16[2,256,128]{2,1,0:T(8,128)(2,1)S(1)} %get-tuple-element.45), channel_id=1, source_target_pairs={{0,96},{8,104},{16,112},{24,120},{32,0},{40,8},{48,16},{56,24},{64... | collective-permute-start | bytes 393224 | tf_op jit(solution)/shard_map/ppermute | solution.py:282
  155.9 11.7 %collective-permute-start.29 = (bf16[2,256,128]{2,1,0:T(8,128)(2,1)S(1)}, bf16[2,256,128]{2,1,0:T(8,128)(2,1)S(1)}, u32[]{:S(2)}, u32[]{:S(2)}) collective-permute-start(bf16[2,256,128]{2,1,0:T(8,128)(2,1)S(1)} %get-tuple-element.44), channel_id=1, source_target_pairs={{0,112},{8,120},{16,0},{24,8},{32,16},{40,24},{48,32},{56,40},{64,... | collective-permute-start | bytes 393224 | tf_op jit(solution)/shard_map/ppermute | solution.py:282
  (17 other events, 257.5 us)
